TPU v7x, 512 devices: a 8x2x16 block of a 8x16x16 slice. The times are simulated.
512 devices in a mesh: grp: 2 (over y), kv: 16 (over z), tp: 16 (over x, core).
Axes of the slice: x: 8, y: 2, z: 16, core: 2. Of those that a mesh axis runs over, the one named last changes fastest.
The devices are a block of a 8x16x16 slice.
Arguments:
- tokens: bfloat16 [256, 4096], P('grp', ('kv', 'tp')), parts along dimension 0, may hold values from -8 to 8
- norm_gain: bfloat16 [4096], P('kv'), may hold values from 0.099609375 to 1.8984375
- w_query: bfloat16 [4096, 1024], P('kv', 'tp'), may hold values from -0.09375 to 0.09375
- w_key: bfloat16 [4096, 1024], P('kv', 'tp'), may hold values from -0.09375 to 0.09375
- w_value: bfloat16 [4096, 2048], P('kv', 'tp'), may hold values from -0.09375 to 0.09375
- w_ogate: bfloat16 [4096, 2048], P('kv', 'tp'), may hold values from -0.09375 to 0.09375
- w_igate: bfloat16 [4096, 16], P('kv', 'tp'), may hold values from -0.09375 to 0.09375
- w_fgate: bfloat16 [4096, 16], P('kv', 'tp'), may hold values from -0.09375 to 0.09375
- igate_bias: float32 [16], P('tp'), may hold values from -1 to 1
- fgate_bias: float32 [16], P('tp'), may hold values from -1 to 4
- state_c: float32 [256, 16, 64, 128], P(('grp', 'kv'), 'tp'), parts along dimension 0, may hold values from -1.5 to 1.5
- state_n: float32 [256, 16, 64], P(('grp', 'kv'), 'tp'), parts along dimension 0, may hold values from -1.5 to 1.5
- state_m: float32 [256, 16], P(('grp', 'kv'), 'tp'), parts along dimension 0, may hold values from -3 to 1
- head_gain: bfloat16 [16, 128], P('tp'), may hold values from 0.099609375 to 1.8984375
- w_out: bfloat16 [2048, 4096], P('tp', 'kv'), may hold values from -0.125 to 0.125
- ffn_gain: bfloat16 [4096], P('kv'), may hold values from 0.099609375 to 1.8984375
- w_gate: bfloat16 [4096, 11008], P('kv', 'tp'), may hold values from -0.09375 to 0.09375
- w_up: bfloat16 [4096, 11008], P('kv', 'tp'), may hold values from -0.09375 to 0.09375
- w_down: bfloat16 [11008, 4096], P('tp', 'kv'), may hold values from -0.0546875 to 0.0546875
Outputs:
- out_tokens: bfloat16 [256, 4096], P('grp', ('kv', 'tp')), parts along dimension 0
- new_c: float32 [256, 16, 64, 128], P(('grp', 'kv'), 'tp'), parts along dimension 0
- new_n: float32 [256, 16, 64], P(('grp', 'kv'), 'tp'), parts along dimension 0
- new_m: float32 [256, 16], P(('grp', 'kv'), 'tp'), parts along dimension 0
There are 2 independent parts, one for each index of `grp`. A program takes and returns all parts, laid end to end along the dimension named above; an argument that names none is the same for every part. Nothing has to cross between parts.
All inputs are finite; a program needn't handle non-finite values.
Results may differ from a plain program's by a relative error of at most 0.017.
Values may be sent and summed in bfloat16 or wider, within the bound.
No kernel may reach another device: no remote copies, remote signals or barrier semaphores. Data moves between devices by JAX's collectives and lax.ppermute only.
A program may use at most 64 MiB of HBM per device.

v0:
```python
import math

import jax
import jax.numpy as jnp
from jax import lax
from jax.sharding import PartitionSpec as P

D = 4096
DK = 64
DV = 128


norm_eps = 1e-06
igate_cap = 1.5


def split_up(value, dim, count):
    before, after = (value.shape[:dim], value.shape[dim + 1 :])
    return jnp.moveaxis(value.reshape(*before, count, -1, *after), dim, 0)


def summed_on_arrival(value, axis, dim):
    blocks = split_up(value, dim, lax.axis_size(axis))
    arrived = lax.all_to_all(blocks, axis, split_axis=0, concat_axis=0, tiled=True)
    return arrived.sum(axis=0)


def side_by_side(arrays, axis, dim, along):
    columns = [a.reshape(*a.shape[:along], -1) for a in arrays]
    both = jnp.concatenate(columns, axis=along)
    out, at, finished = (summed_on_arrival(both, axis, dim), 0, [])
    for a, column in zip(arrays, columns):
        section = out[..., at : at + column.shape[along]]
        finished.append(section.reshape(*section.shape[:along], *a.shape[along:]))
        at += column.shape[along]
    return tuple(finished)


def in_order(blocks, dim):
    lengths = list(blocks.shape[1:])
    lengths[dim] *= blocks.shape[0]
    return jnp.moveaxis(blocks, 0, dim).reshape(lengths)


def sent_to_all(value, axis):
    count = lax.axis_size(axis)
    return lax.all_to_all(
        jnp.broadcast_to(value[None], (count, *value.shape)), axis, 0, 0, tiled=True
    )


def gathered_copies(value, axis, dim):
    return in_order(sent_to_all(value, axis), dim)


def sum_at_owner(value, axis, dim):
    blocks = split_up(value, dim, lax.axis_size(axis))
    arrived = lax.all_to_all(blocks, axis, split_axis=0, concat_axis=0, tiled=True)
    return arrived.astype(jnp.float32).sum(axis=0)


def side_by_side_2(arrays, axis, dim, along):
    widths = [math.prod(a.shape[along:]) for a in arrays]
    both = jnp.concatenate(
        [a.reshape(*a.shape[:along], w) for a, w in zip(arrays, widths)], axis=along
    )
    out = sum_at_owner(both, axis, dim)
    blocks = jnp.split(out, [sum(widths[:k]) for k in range(1, len(widths))], axis=along)
    return tuple((b.reshape(*out.shape[:along], *a.shape[along:]) for a, b in zip(arrays, blocks)))


def cell_update(query, key_vec, value_vec, igate, fgate, state_c, state_n, state_m):
    carried = jax.nn.log_sigmoid(fgate) + state_m
    new_m = jnp.maximum(carried, igate)
    keep_weight = jnp.exp(carried - new_m)
    write_weight = jnp.exp(igate - new_m)
    new_c = (
        keep_weight[..., None, None] * state_c
        + write_weight[..., None, None] * key_vec[..., :, None] * value_vec[..., None, :]
    )
    new_n = keep_weight[..., None] * state_n + write_weight[..., None] * key_vec
    numerator = jnp.einsum("bhd,bhde->bhe", query, new_c, precision=lax.Precision.HIGHEST)
    denominator = jnp.sum(query * new_n, axis=-1)
    head_out = numerator / jnp.maximum(jnp.abs(denominator), jnp.exp(-new_m))[..., None]
    return (new_c, new_n, new_m, head_out)


def body(
    tokens,
    norm_gain,
    w_query,
    w_key,
    w_value,
    w_ogate,
    w_igate,
    w_fgate,
    igate_bias,
    fgate_bias,
    state_c,
    state_n,
    state_m,
    head_gain,
    w_out,
    ffn_gain,
    w_gate,
    w_up,
    w_down,
):
    seq_rows = state_c.shape[0]
    heads_here = state_c.shape[1]
    token_cols = lax.all_gather(tokens, "tp", axis=1, tiled=True)
    token_vals = token_cols.astype(jnp.float32)
    normed = (token_vals * norm_gain.astype(jnp.float32)).astype(jnp.bfloat16)
    squares = jnp.sum(token_vals * token_vals, axis=1)
    part_query = jnp.dot(normed, w_query, preferred_element_type=jnp.float32)
    part_key = jnp.dot(normed, w_key, preferred_element_type=jnp.float32)
    part_value = jnp.dot(normed, w_value, preferred_element_type=jnp.float32)
    part_ogate = jnp.dot(normed, w_ogate, preferred_element_type=jnp.float32)
    part_igate = jnp.dot(normed, w_igate, preferred_element_type=jnp.float32)
    part_fgate = jnp.dot(normed, w_fgate, preferred_element_type=jnp.float32)
    sum_query, sum_key, sum_value, sum_ogate, sum_igate, sum_fgate, sum_squares = side_by_side(
        (part_query, part_key, part_value, part_ogate, part_igate, part_fgate, squares), "kv", 0, 1
    )
    row_scale = lax.rsqrt(sum_squares / D + norm_eps)[:, None]
    query = (row_scale * sum_query).reshape(seq_rows, heads_here, DK)
    key_vec = (row_scale * sum_key).reshape(seq_rows, heads_here, DK) * DK ** (-0.5)
    value_vec = (row_scale * sum_value).reshape(seq_rows, heads_here, DV)
    ogate = (row_scale * sum_ogate).reshape(seq_rows, heads_here, DV)
    igate = igate_cap * jnp.tanh((row_scale * sum_igate + igate_bias) / igate_cap)
    fgate = row_scale * sum_fgate + fgate_bias
    new_c, new_n, new_m, head_out = cell_update(
        query, key_vec, value_vec, igate, fgate, state_c, state_n, state_m
    )
    merged = (
        (head_out * head_gain.astype(jnp.float32) * jax.nn.sigmoid(ogate))
        .reshape(seq_rows, heads_here * DV)
        .astype(jnp.bfloat16)
    )
    attn_part = jnp.dot(gathered_copies(merged, "kv", 0), w_out, preferred_element_type=jnp.float32)
    attn_out = sum_at_owner(attn_part.astype(jnp.bfloat16), "tp", 1)
    middle = (tokens.astype(jnp.float32) + attn_out).astype(jnp.bfloat16)
    middle_cols = lax.all_gather(middle, "tp", axis=1, tiled=True)
    middle_vals = middle_cols.astype(jnp.float32)
    normed_two = (middle_vals * ffn_gain.astype(jnp.float32)).astype(jnp.bfloat16)
    squares_two = jnp.sum(middle_vals * middle_vals, axis=1)
    gate_part = jnp.dot(normed_two, w_gate, preferred_element_type=jnp.float32)
    up_part = jnp.dot(normed_two, w_up, preferred_element_type=jnp.float32)
    gate_sum, up_sum, total_two = side_by_side_2(
        (
            gate_part.astype(jnp.bfloat16),
            up_part.astype(jnp.bfloat16),
            squares_two.astype(jnp.bfloat16),
        ),
        "kv",
        0,
        1,
    )
    ffn_scale = lax.rsqrt(total_two / D + norm_eps)[:, None]
    hidden = (jax.nn.silu(ffn_scale * gate_sum) * (ffn_scale * up_sum)).astype(jnp.bfloat16)
    down_part = jnp.dot(
        gathered_copies(hidden, "kv", 0), w_down, preferred_element_type=jnp.float32
    )
    down_out = sum_at_owner(down_part.astype(jnp.bfloat16), "tp", 1)
    out_tokens = (middle.astype(jnp.float32) + down_out).astype(jnp.bfloat16)
    return (out_tokens, new_c, new_n, new_m)


def solution(mesh):
    placed = (
        P("grp", ("kv", "tp")),
        P("kv"),
        P("kv", "tp"),
        P("kv", "tp"),
        P("kv", "tp"),
        P("kv", "tp"),
        P("kv", "tp"),
        P("kv", "tp"),
        P("tp"),
        P("tp"),
        P(("grp", "kv"), "tp", None, None),
        P(("grp", "kv"), "tp", None),
        P(("grp", "kv"), "tp"),
        P("tp", None),
        P("tp", "kv"),
        P("kv"),
        P("kv", "tp"),
        P("kv", "tp"),
        P("tp", "kv"),
    )
    return jax.shard_map(
        body,
        mesh=mesh,
        in_specs=placed,
        out_specs=(
            P("grp", ("kv", "tp")),
            P(("grp", "kv"), "tp", None, None),
            P(("grp", "kv"), "tp", None),
            P(("grp", "kv"), "tp"),
        ),
        check_vma=False,
    )
```

profile of v0, /device:TPU:65, one launch (start us, length us, event | category | flops | bytes accessed | tf_op | source)
XLA Modules:
  0.0 202.4 jit_solution(7340011110046809596)
XLA Ops:
  0.6 0.0 copy-start
  0.6 0.7 convert_element_type.76
  1.4 55.9 %all_gather.6 = bf16[128,256]{0,1:T(8,128)(2,1)S(1)} all-gather(bf16[128,16]{0,1:T(8,128)(2,1)} %param.19), channel_id=1, replica_groups=mesh['grp'=2,'kv'=16,'tp'=16] {'tp'}, dimensions={1}, use_global_device_ids=true | all-gather | bytes 69632 | tf_op jit(solution)/shard_map/all_gather | solution.py:111
  57.3 0.1 copy.69
  57.4 0.1 fusion.4
  57.5 0.0 copy-start.8
  57.5 0.2 concatenate.31
  57.7 0.6 copy-done.8
  58.3 0.1 convolution_bitcast_fusion.4
  58.4 0.7 copy-done.5
  59.1 0.1 convolution_bitcast_fusion.3
  59.3 0.7 copy-done.6
  60.0 0.1 convolution_bitcast_fusion.2
  60.1 0.5 copy-done.12
  60.6 0.1 convolution_bitcast_fusion.1
  60.8 0.5 copy-done.13
  61.3 0.1 convolution_bitcast_fusion
  61.5 0.6 copy-done.9
  62.1 0.1 convolution_bitcast_fusion.5
  62.2 0.9 concatenate.27
  63.1 7.2 %all-to-all-start = ((f32[16,8,387]{2,1,0:T(8,128)}), f32[16,8,387]{2,1,0:T(8,128)S(1)}, u32[]{:S(2)}, u32[]{:S(2)}) async-start(f32[16,8,387]{2,1,0:T(8,128)} %concatenate.27), calls=%async_computation | async-start | bytes 524288 | tf_op jit(solution)/shard_map/all_to_all | solution.py:24
  70.3 0.0 copy-start.4
  71.7 0.1 copy.75
  71.7 0.0 copy-done.15
  71.7 12.5 %all-to-all-done = f32[16,8,387]{2,1,0:T(8,128)S(1)} async-done(((f32[16,8,387]{2,1,0:T(8,128)}), f32[16,8,387]{2,1,0:T(8,128)S(1)}, u32[]{:S(2)}, u32[]{:S(2)}) %all-to-all-start) | async-done | bytes 198176 | tf_op jit(solution)/shard_map/all_to_all | solution.py:24
  84.3 0.3 multiply_reduce_fusion
  84.5 0.1 slice_multiply_fusion.4
  84.6 0.7 copy-done.11
  85.3 0.8 fusion.39
  86.1 0.1 copy.77
  86.2 0.1 maximum_reduce_fusion
  86.3 0.1 multiply_add_fusion
  86.4 0.0 copy-start.1
  86.5 0.3 fusion
  86.8 0.1 fusion.40
  86.9 21.4 %all_to_all.30 = bf16[16,8,128]{2,1,0:T(8,128)(2,1)S(1)} all-to-all(bf16[16,8,128]{2,1,0:T(8,128)(2,1)S(1)} %broadcast_in_dim.4), channel_id=1, replica_groups=mesh['grp'=2,'kv'=16,'tp'=16] {'kv'}, dimensions={0} | all-to-all | bytes 65536 | tf_op jit(solution)/shard_map/all_to_all | solution.py:47
  108.3 0.1 convolution_convert_fusion.3
  108.4 0.7 copy.78
  109.1 6.3 %all-to-all-start.2 = ((bf16[16,128,16]{1,2,0:T(8,128)(2,1)}), bf16[16,128,16]{1,2,0:T(8,128)(2,1)S(1)}, u32[]{:S(2)}, u32[]{:S(2)}) async-start(bf16[16,128,16]{1,2,0:T(8,128)(2,1)} %bitcast.23), calls=%async_computation.2 | async-start | bytes 131072 | tf_op jit(solution)/shard_map/all_to_all | solution.py:58
  115.5 0.0 copy-done.16
  115.5 0.0 copy-start.10
  115.5 7.7 %all-to-all-done.2 = bf16[16,128,16]{1,2,0:T(8,128)(2,1)S(1)} async-done(((bf16[16,128,16]{1,2,0:T(8,128)(2,1)}), bf16[16,128,16]{1,2,0:T(8,128)(2,1)S(1)}, u32[]{:S(2)}, u32[]{:S(2)}) %all-to-all-start.2) | async-done | bytes 65568 | tf_op jit(solution)/shard_map/all_to_all | solution.py:58
  123.3 15.0 %all_gather.7 = bf16[128,256]{0,1:T(8,128)(2,1)S(1)} all-gather(bf16[128,16]{0,1:T(8,128)(2,1)S(1)} %add_convert_fusion.1), channel_id=1, replica_groups=mesh['grp'=2,'kv'=16,'tp'=16] {'tp'}, dimensions={1}, use_global_device_ids=true | all-gather | bytes 69632 | tf_op jit(solution)/shard_map/all_gather | solution.py:142
  138.2 0.1 fusion.6
  138.3 0.2 convert_element_type.95
  138.5 0.0 copy-start.2
  138.5 0.3 convolution_convert_fusion.1
  138.9 0.1 copy.79
  139.0 0.5 copy-done.2
  139.5 0.3 convolution_convert_fusion
  139.8 0.1 copy.80
  140.0 0.2 concatenate.30
  140.2 21.4 %all_to_all.31 = bf16[16,8,1377]{2,1,0:T(8,128)(2,1)S(1)} all-to-all(bf16[16,8,1377]{2,1,0:T(8,128)(2,1)S(1)} %concatenate.30), channel_id=1, replica_groups=mesh['grp'=2,'kv'=16,'tp'=16] {'kv'}, dimensions={0} | all-to-all | bytes 705024 | tf_op jit(solution)/shard_map/all_to_all | solution.py:58
  161.6 0.1 convert_reduce_fusion
  161.7 0.0 copy-start.3
  161.7 0.2 fusion.24
  161.9 0.1 fusion.13
  162.0 22.1 %all_to_all.32 = bf16[16,8,688]{2,1,0:T(8,128)(2,1)S(1)} all-to-all(bf16[16,8,688]{2,1,0:T(8,128)(2,1)S(1)} %broadcast_in_dim.5), channel_id=1, replica_groups=mesh['grp'=2,'kv'=16,'tp'=16] {'kv'}, dimensions={0} | all-to-all | bytes 352256 | tf_op jit(solution)/shard_map/all_to_all | solution.py:47
  184.1 0.2 convolution_convert_fusion.2
  184.3 0.7 copy.82
  185.0 8.9 %all-to-all-start.5 = ((bf16[16,128,16]{1,2,0:T(8,128)(2,1)}), bf16[16,128,16]{1,2,0:T(8,128)(2,1)S(1)}, u32[]{:S(2)}, u32[]{:S(2)}) async-start(bf16[16,128,16]{1,2,0:T(8,128)(2,1)} %bitcast.28), calls=%async_computation.5 | async-start | bytes 131072 | tf_op jit(solution)/shard_map/all_to_all | solution.py:58
  194.0 0.6 copy.84
  194.6 7.2 %all-to-all-done.5 = bf16[16,128,16]{1,2,0:T(8,128)(2,1)S(1)} async-done(((bf16[16,128,16]{1,2,0:T(8,128)(2,1)}), bf16[16,128,16]{1,2,0:T(8,128)(2,1)S(1)}, u32[]{:S(2)}, u32[]{:S(2)}) %all-to-all-start.5) | async-done | bytes 65568 | tf_op jit(solution)/shard_map/all_to_all | solution.py:58
  201.8 0.6 add_convert_fusion
  (26 shorter events, 0.1 us)
Async XLA Ops:
  0.6 137.9 %copy-start = (bf16[256,688]{0,1:T(8,128)(2,1)S(1)}, bf16[256,688]{0,1:T(8,128)(2,1)}, u32[]{:S(2)}) copy-start(bf16[256,688]{0,1:T(8,128)(2,1)} %param.35) | copy-start | bytes 1056772
  57.5 0.8 copy-start.8
  58.3 0.8 copy-start.5
  59.1 0.8 copy-start.6
  60.0 0.7 copy-start.12
  60.6 0.7 copy-start.13
  61.3 0.8 copy-start.9
  63.1 8.6 %copy-start.14 = (f32[8,1]{0,1:T(1,128)S(1)}, f32[8,1]{0,1:T(1,128)}, u32[]{:S(2)}) copy-start(f32[8,1]{0,1:T(1,128)} %param.31) | copy-start | bytes 100
  63.1 8.7 %copy-start.15 = (bf16[1,128]{1,0:T(2,128)(2,1)S(1)}, bf16[1,128]{1,0:T(2,128)(2,1)}, u32[]{:S(2)}) copy-start(bf16[1,128]{1,0:T(2,128)(2,1)} %param.32) | copy-start | bytes 772
  63.1 21.2 %all-to-all-start = ((f32[16,8,387]{2,1,0:T(8,128)}), f32[16,8,387]{2,1,0:T(8,128)S(1)}, u32[]{:S(2)}, u32[]{:S(2)}) async-start(f32[16,8,387]{2,1,0:T(8,128)} %concatenate.27), calls=%async_computation | async-start | bytes 524288 | tf_op jit(solution)/shard_map/all_to_all | solution.py:24
  70.3 16.0 %copy-start.4 = (f32[8,1,64,128]{3,2,1,0:T(8,128)S(1)}, f32[8,1,64,128]{3,2,1,0:T(8,128)}, u32[]{:S(2)}) copy-start(f32[8,1,64,128]{3,2,1,0:T(8,128)} %param.29) | copy-start | bytes 786436
  84.6 0.7 copy-start.11
  86.4 22.0 %copy-start.1 = (f32[8,1,64,128]{3,2,1,0:T(8,128)}, f32[8,1,64,128]{3,2,1,0:T(8,128)S(1)}, u32[]{:S(2)}) copy-start(f32[8,1,64,128]{3,2,1,0:T(8,128)S(1)} %multiply_add_fusion) | copy-start | bytes 786436
  86.8 21.5 %copy-start.7 = (bf16[128,256]{1,0:T(8,128)(2,1)S(1)}, bf16[128,256]{1,0:T(8,128)(2,1)}, u32[]{:S(2)}) copy-start(bf16[128,256]{1,0:T(8,128)(2,1)} %param.33) | copy-start | bytes 196612
  109.1 6.3 %copy-start.16 = (bf16[256]{0:T(256)(128)(2,1)S(1)}, bf16[256]{0:T(256)(128)(2,1)}, u32[]{:S(2)}) copy-start(bf16[256]{0:T(256)(128)(2,1)} %param.34) | copy-start | bytes 1540
  109.1 14.1 %all-to-all-start.2 = ((bf16[16,128,16]{1,2,0:T(8,128)(2,1)}), bf16[16,128,16]{1,2,0:T(8,128)(2,1)S(1)}, u32[]{:S(2)}, u32[]{:S(2)}) async-start(bf16[16,128,16]{1,2,0:T(8,128)(2,1)} %bitcast.23), calls=%async_computation.2 | async-start | bytes 131072 | tf_op jit(solution)/shard_map/all_to_all | solution.py:58
  115.5 7.8 %copy-start.10 = (bf16[128,16]{0,1:T(8,128)(2,1)S(1)}, bf16[128,16]{0,1:T(8,128)(2,1)}, u32[]{:S(2)}) copy-start(bf16[128,16]{0,1:T(8,128)(2,1)} %param.19) | copy-start | bytes 12292
  138.5 1.0 copy-start.2
  161.7 22.4 %copy-start.3 = (bf16[688,256]{1,0:T(8,128)(2,1)S(1)}, bf16[688,256]{1,0:T(8,128)(2,1)}, u32[]{:S(2)}) copy-start(bf16[688,256]{1,0:T(8,128)(2,1)} %param.37) | copy-start | bytes 1056772
  185.0 16.7 %all-to-all-start.5 = ((bf16[16,128,16]{1,2,0:T(8,128)(2,1)}), bf16[16,128,16]{1,2,0:T(8,128)(2,1)S(1)}, u32[]{:S(2)}, u32[]{:S(2)}) async-start(bf16[16,128,16]{1,2,0:T(8,128)(2,1)} %bitcast.28), calls=%async_computation.5 | async-start | bytes 131072 | tf_op jit(solution)/shard_map/all_to_all | solution.py:58
where the time goes:
time: 203 us; the launch traced here: 202 us
  blocking collectives  136 us (67%)
  waiting for transfers between devices  27.4 us (13%)
  starting transfers between devices  22.5 us (11%)
  local copies, waits for them, and re-layouts  9 us (4%)
  other arithmetic  3.32 us (2%)
  between operations  2.24 us (1%)
  matrix products  2.09 us (1%)
    all_gather x1, blocking collectives, body(): token_cols = lax.all_gather(tokens, 'tp', axis=1, tiled=True)  55.9 us
    all_to_all x2, blocking collectives, sent_to_all(): lax.all_to_all(jnp.broadcast_to(value[None], (count, *value.shape)), axis...  43.5 us
    all_to_all x1, blocking collectives, sum_at_owner(): lax.all_to_all(blocks, axis, split_axis=0, concat_axis=0, tiled=True)  21.4 us
    all_to_all x2, starting transfers between devices, sum_at_owner(): lax.all_to_all(blocks, axis, split_axis=0, concat_axis=0, tiled=True)  15.3 us
    all_gather x1, blocking collectives, body(): middle_cols = lax.all_gather(middle, 'tp', axis=1, tiled=True)  15 us
    all_to_all x2, waiting for transfers between devices, sum_at_owner(): lax.all_to_all(blocks, axis, split_axis=0, concat_axis=0, tiled=True)  14.9 us
    all_to_all x1, waiting for transfers between devices, summed_on_arrival(): lax.all_to_all(blocks, axis, split_axis=0, concat_axis=0, tiled=True)  12.5 us
    all_to_all x1, starting transfers between devices, summed_on_arrival(): lax.all_to_all(blocks, axis, split_axis=0, concat_axis=0, tiled=True)  7.23 us
  transfers between devices with their start and end apart: 3, of which 3 were waited for; matrix products, arithmetic and copies ran while one was open for 0% of the time, Pallas kernels for 0%

commit v1 on v0

--- a/solution.py
+++ b/solution.py
@@ -19,16 +19,10 @@
     return jnp.moveaxis(value.reshape(*before, count, -1, *after), dim, 0)
 
 
-def summed_on_arrival(value, axis, dim):
-    blocks = split_up(value, dim, lax.axis_size(axis))
-    arrived = lax.all_to_all(blocks, axis, split_axis=0, concat_axis=0, tiled=True)
-    return arrived.sum(axis=0)
-
-
 def side_by_side(arrays, axis, dim, along):
     columns = [a.reshape(*a.shape[:along], -1) for a in arrays]
-    both = jnp.concatenate(columns, axis=along)
-    out, at, finished = (summed_on_arrival(both, axis, dim), 0, [])
+    both = jnp.concatenate(columns, axis=along).astype(jnp.bfloat16)
+    out, at, finished = (sum_at_owner(both, axis, dim), 0, [])
     for a, column in zip(arrays, columns):
         section = out[..., at : at + column.shape[along]]
         finished.append(section.reshape(*section.shape[:along], *a.shape[along:]))
@@ -108,7 +102,7 @@
 ):
     seq_rows = state_c.shape[0]
     heads_here = state_c.shape[1]
-    token_cols = lax.all_gather(tokens, "tp", axis=1, tiled=True)
+    token_cols = gathered_copies(tokens, "tp", 1)
     token_vals = token_cols.astype(jnp.float32)
     normed = (token_vals * norm_gain.astype(jnp.float32)).astype(jnp.bfloat16)
     squares = jnp.sum(token_vals * token_vals, axis=1)
@@ -139,7 +133,7 @@
     attn_part = jnp.dot(gathered_copies(merged, "kv", 0), w_out, preferred_element_type=jnp.float32)
     attn_out = sum_at_owner(attn_part.astype(jnp.bfloat16), "tp", 1)
     middle = (tokens.astype(jnp.float32) + attn_out).astype(jnp.bfloat16)
-    middle_cols = lax.all_gather(middle, "tp", axis=1, tiled=True)
+    middle_cols = gathered_copies(middle, "tp", 1)
     middle_vals = middle_cols.astype(jnp.float32)
     normed_two = (middle_vals * ffn_gain.astype(jnp.float32)).astype(jnp.bfloat16)
     squares_two = jnp.sum(middle_vals * middle_vals, axis=1)

time: 203 us -> 193 us (0.951)
  blocking collectives: 136 us -> 73.6 us
  starting transfers between devices: 22.5 us -> 64.1 us
  waiting for transfers between devices: 27.4 us -> 33.5 us
  local copies, waits for them, and re-layouts: 9 us -> 13.2 us
    all_gather x2 -> x0, blocking collectives: 70.9 us -> none  [the longest x1 55.9 us: body(): token_cols = lax.all_gather(tokens, 'tp', axis=1, tiled=True)]
    all_to_all x1 -> x2, starting transfers between devices: 7.23 us -> 48.7 us  [sent_to_all(): lax.all_to_all(jnp.broadcast_to(value[None], (count, *value.shape)), axis...]
    all_to_all x1 -> x2, blocking collectives: 21.4 us -> 33.1 us  [sum_at_owner(): lax.all_to_all(blocks, axis, split_axis=0, concat_axis=0, tiled=True)]
    all_to_all x1 -> x2, waiting for transfers between devices: 12.5 us -> 15.7 us  [sent_to_all(): lax.all_to_all(jnp.broadcast_to(value[None], (count, *value.shape)), axis...]
    all_to_all x2, blocking collectives: 43.5 us -> 40.5 us  [sent_to_all(): lax.all_to_all(jnp.broadcast_to(value[None], (count, *value.shape)), axis...]
    all_to_all x2, waiting for transfers between devices: 14.9 us -> 17.8 us  [sum_at_owner(): lax.all_to_all(blocks, axis, split_axis=0, concat_axis=0, tiled=True)]
    unnamed x36 -> x38, local copies, waits for them, and re-layouts: 5.57 us -> 6.1 us
  transfers between devices with their start and end apart: 3 -> 4, of which waited for: 3 -> 4; matrix products, arithmetic and copies ran while one was open for 0% -> 0% of each run, Pallas kernels for 0% -> 0%
where the time goes in v1:
time: 193 us; the launch traced here: 192 us
  blocking collectives  73.6 us (38%)
  starting transfers between devices  64.1 us (33%)
  waiting for transfers between devices  33.5 us (17%)
  local copies, waits for them, and re-layouts  13.2 us (7%)
  other arithmetic  2.75 us (1%)
  between operations  2.28 us (1%)
  matrix products  2.22 us (1%)
    all_to_all x2, starting transfers between devices, sent_to_all(): lax.all_to_all(jnp.broadcast_to(value[None], (count, *value.shape)), axis...  48.7 us
    all_to_all x2, blocking collectives, sent_to_all(): lax.all_to_all(jnp.broadcast_to(value[None], (count, *value.shape)), axis...  40.5 us
    all_to_all x2, blocking collectives, sum_at_owner(): lax.all_to_all(blocks, axis, split_axis=0, concat_axis=0, tiled=True)  33.1 us
    all_to_all x2, waiting for transfers between devices, sum_at_owner(): lax.all_to_all(blocks, axis, split_axis=0, concat_axis=0, tiled=True)  17.8 us
    all_to_all x2, waiting for transfers between devices, sent_to_all(): lax.all_to_all(jnp.broadcast_to(value[None], (count, *value.shape)), axis...  15.7 us
    all_to_all x2, starting transfers between devices, sum_at_owner(): lax.all_to_all(blocks, axis, split_axis=0, concat_axis=0, tiled=True)  15.4 us
    unnamed x38, local copies, waits for them, and re-layouts  6.1 us
  transfers between devices with their start and end apart: 4, of which 4 were waited for; matrix products, arithmetic and copies ran while one was open for 0% of the time, Pallas kernels for 0%

profile of v1, /device:TPU:65, one launch (start us, length us, event | category | flops | bytes accessed | tf_op | source)
XLA Modules:
  0.0 191.6 jit_solution(12194168724781310323)
XLA Ops:
  0.6 1.4 broadcast_in_dim.8
  2.0 44.9 %all-to-all-start = ((bf16[16,128,16]{1,2,0:T(8,128)(2,1)}), bf16[16,128,16]{1,2,0:T(8,128)(2,1)S(1)}, u32[]{:S(2)}, u32[]{:S(2)}) async-start(bf16[16,128,16]{1,2,0:T(8,128)(2,1)} %broadcast_in_dim.8), calls=%async_computation | async-start | bytes 131072 | tf_op jit(solution)/shard_map/all_to_all | solution.py:41
  46.9 0.1 mul.189
  47.0 7.8 %all-to-all-done = bf16[16,128,16]{1,2,0:T(8,128)(2,1)S(1)} async-done(((bf16[16,128,16]{1,2,0:T(8,128)(2,1)}), bf16[16,128,16]{1,2,0:T(8,128)(2,1)S(1)}, u32[]{:S(2)}, u32[]{:S(2)}) %all-to-all-start) | async-done | bytes 65568 | tf_op jit(solution)/shard_map/all_to_all | solution.py:41
  54.8 0.5 copy.66
  55.3 0.4 reshape.213
  55.8 0.8 copy-done.5
  56.6 0.1 convolution_convert_fusion.4
  56.7 0.7 copy-done.6
  57.4 0.1 convolution_convert_fusion.5
  57.6 0.6 copy-done.8
  58.2 0.1 convolution_convert_fusion.6
  58.3 0.6 copy-done.9
  59.0 0.1 convolution_convert_fusion.7
  59.1 0.1 fusion.4
  59.2 0.4 copy.67
  59.7 0.5 dot_general.43
  60.1 0.2 copy-done.12
  60.3 0.2 fusion.40
  60.6 0.1 copy.81
  60.7 0.2 copy.68
  60.8 0.5 copy-done.13
  61.4 0.2 fusion.38
  61.6 0.1 copy.82
  61.7 0.2 copy.69
  61.9 0.2 concatenate.20
  62.1 0.8 concatenate.16
  62.9 7.4 %all-to-all-start.1 = ((bf16[16,8,387]{2,1,0:T(8,128)(2,1)}), bf16[16,8,387]{2,1,0:T(8,128)(2,1)S(1)}, u32[]{:S(2)}, u32[]{:S(2)}) async-start(bf16[16,8,387]{2,1,0:T(8,128)(2,1)} %concatenate.16), calls=%async_computation.1 | async-start | bytes 262144 | tf_op jit(solution)/shard_map/all_to_all | solution.py:52
  70.3 0.1 copy.71
  71.7 10.5 %all-to-all-done.1 = bf16[16,8,387]{2,1,0:T(8,128)(2,1)S(1)} async-done(((bf16[16,8,387]{2,1,0:T(8,128)(2,1)}), bf16[16,8,387]{2,1,0:T(8,128)(2,1)S(1)}, u32[]{:S(2)}, u32[]{:S(2)}) %all-to-all-start.1) | async-done | bytes 99104 | tf_op jit(solution)/shard_map/all_to_all | solution.py:52
  82.2 0.3 multiply_reduce_fusion.1
  82.6 0.7 copy-done.11
  83.3 0.8 fusion.33
  84.1 0.1 copy.73
  84.1 0.1 maximum_reduce_fusion
  84.3 0.1 multiply_add_fusion
  84.4 0.3 fusion
  84.7 0.1 fusion.34
  84.9 17.8 %all_to_all.40 = bf16[16,8,128]{2,1,0:T(8,128)(2,1)S(1)} all-to-all(bf16[16,8,128]{2,1,0:T(8,128)(2,1)S(1)} %broadcast_in_dim.9), channel_id=1, replica_groups=mesh['grp'=2,'kv'=16,'tp'=16] {'kv'}, dimensions={0} | all-to-all | bytes 65536 | tf_op jit(solution)/shard_map/all_to_all | solution.py:41
  102.6 0.1 convolution_convert_fusion.3
  102.8 0.1 copy.74
  102.9 12.3 %all_to_all.41 = bf16[16,128,16]{1,2,0:T(8,128)(2,1)S(1)} all-to-all(bf16[16,128,16]{1,2,0:T(8,128)(2,1)S(1)} %bitcast.95), channel_id=1, replica_groups=mesh['grp'=2,'kv'=16,'tp'=16] {'tp'}, dimensions={0} | all-to-all | bytes 131072 | tf_op jit(solution)/shard_map/all_to_all | solution.py:52
  115.2 0.7 copy-done.10
  115.9 0.6 broadcast_in_dim.10
  116.5 3.8 %all-to-all-start.4 = ((bf16[16,128,16]{1,2,0:T(8,128)(2,1)}), bf16[16,128,16]{1,2,0:T(8,128)(2,1)S(1)}, u32[]{:S(2)}, u32[]{:S(2)}) async-start(bf16[16,128,16]{1,2,0:T(8,128)(2,1)} %broadcast_in_dim.10), calls=%async_computation.4 | async-start | bytes 131072 | tf_op jit(solution)/shard_map/all_to_all | solution.py:41
  120.4 7.9 %all-to-all-done.4 = bf16[16,128,16]{1,2,0:T(8,128)(2,1)S(1)} async-done(((bf16[16,128,16]{1,2,0:T(8,128)(2,1)}), bf16[16,128,16]{1,2,0:T(8,128)(2,1)S(1)}, u32[]{:S(2)}, u32[]{:S(2)}) %all-to-all-start.4) | async-done | bytes 65568 | tf_op jit(solution)/shard_map/all_to_all | solution.py:41
  128.2 0.1 fusion.5
  128.4 0.3 convolution_convert_fusion.1
  128.6 0.1 copy.75
  128.8 0.6 copy-done.2
  129.3 0.2 convolution_convert_fusion
  129.6 0.1 copy.76
  129.8 0.2 convert_element_type.150
  130.0 0.2 concatenate.19
  130.2 20.8 %all_to_all.42 = bf16[16,8,1377]{2,1,0:T(8,128)(2,1)S(1)} all-to-all(bf16[16,8,1377]{2,1,0:T(8,128)(2,1)S(1)} %concatenate.19), channel_id=1, replica_groups=mesh['grp'=2,'kv'=16,'tp'=16] {'kv'}, dimensions={0} | all-to-all | bytes 705024 | tf_op jit(solution)/shard_map/all_to_all | solution.py:52
  151.0 0.2 fusion.18
  151.2 0.1 fusion.13
  151.4 22.8 %all_to_all.43 = bf16[16,8,688]{2,1,0:T(8,128)(2,1)S(1)} all-to-all(bf16[16,8,688]{2,1,0:T(8,128)(2,1)S(1)} %broadcast_in_dim.11), channel_id=1, replica_groups=mesh['grp'=2,'kv'=16,'tp'=16] {'kv'}, dimensions={0} | all-to-all | bytes 352256 | tf_op jit(solution)/shard_map/all_to_all | solution.py:41
  174.1 0.2 convolution_convert_fusion.2
  174.3 0.7 copy.78
  175.1 8.0 %all-to-all-start.7 = ((bf16[16,128,16]{1,2,0:T(8,128)(2,1)}), bf16[16,128,16]{1,2,0:T(8,128)(2,1)S(1)}, u32[]{:S(2)}, u32[]{:S(2)}) async-start(bf16[16,128,16]{1,2,0:T(8,128)(2,1)} %bitcast.31), calls=%async_computation.7 | async-start | bytes 131072 | tf_op jit(solution)/shard_map/all_to_all | solution.py:52
  183.1 0.6 copy.80
  183.7 7.3 %all-to-all-done.7 = bf16[16,128,16]{1,2,0:T(8,128)(2,1)S(1)} async-done(((bf16[16,128,16]{1,2,0:T(8,128)(2,1)}), bf16[16,128,16]{1,2,0:T(8,128)(2,1)S(1)}, u32[]{:S(2)}, u32[]{:S(2)}) %all-to-all-start.7) | async-done | bytes 65568 | tf_op jit(solution)/shard_map/all_to_all | solution.py:52
  191.0 0.6 add_convert_fusion
  (44 shorter events, 0.4 us)
Async XLA Ops:
  0.6 127.7 %copy-start = (bf16[256,688]{0,1:T(8,128)(2,1)S(1)}, bf16[256,688]{0,1:T(8,128)(2,1)}, u32[]{:S(2)}) copy-start(bf16[256,688]{0,1:T(8,128)(2,1)} %param.35) | copy-start | bytes 1056772
  2.0 44.9 %copy-start.14 = (bf16[256]{0:T(256)(128)(2,1)S(1)}, bf16[256]{0:T(256)(128)(2,1)}, u32[]{:S(2)}) copy-start(bf16[256]{0:T(256)(128)(2,1)} %param.20) | copy-start | bytes 1540
  2.0 52.8 %all-to-all-start = ((bf16[16,128,16]{1,2,0:T(8,128)(2,1)}), bf16[16,128,16]{1,2,0:T(8,128)(2,1)S(1)}, u32[]{:S(2)}, u32[]{:S(2)}) async-start(bf16[16,128,16]{1,2,0:T(8,128)(2,1)} %broadcast_in_dim.8), calls=%async_computation | async-start | bytes 131072 | tf_op jit(solution)/shard_map/all_to_all | solution.py:41
  55.8 0.8 copy-start.5
  56.6 0.8 copy-start.6
  57.4 0.8 copy-start.8
  58.2 0.8 copy-start.9
  59.6 0.7 copy-start.12
  60.7 0.7 copy-start.13
  62.1 8.2 %copy-start.15 = (f32[8,1]{0,1:T(1,128)S(1)}, f32[8,1]{0,1:T(1,128)}, u32[]{:S(2)}) copy-start(f32[8,1]{0,1:T(1,128)} %param.31) | copy-start | bytes 100
  62.9 21.4 %copy-start.4 = (f32[8,1,64,128]{3,2,1,0:T(8,128)S(1)}, f32[8,1,64,128]{3,2,1,0:T(8,128)}, u32[]{:S(2)}) copy-start(f32[8,1,64,128]{3,2,1,0:T(8,128)} %param.29) | copy-start | bytes 786436
  62.9 19.3 %all-to-all-start.1 = ((bf16[16,8,387]{2,1,0:T(8,128)(2,1)}), bf16[16,8,387]{2,1,0:T(8,128)(2,1)S(1)}, u32[]{:S(2)}, u32[]{:S(2)}) async-start(bf16[16,8,387]{2,1,0:T(8,128)(2,1)} %concatenate.16), calls=%async_computation.1 | async-start | bytes 262144 | tf_op jit(solution)/shard_map/all_to_all | solution.py:52
  71.1 0.7 copy-start.16
  82.6 0.7 copy-start.11
  84.4 18.4 %copy-start.1 = (f32[8,1,64,128]{3,2,1,0:T(8,128)}, f32[8,1,64,128]{3,2,1,0:T(8,128)S(1)}, u32[]{:S(2)}) copy-start(f32[8,1,64,128]{3,2,1,0:T(8,128)S(1)} %multiply_add_fusion) | copy-start | bytes 786436
  84.7 17.9 %copy-start.7 = (bf16[128,256]{1,0:T(8,128)(2,1)S(1)}, bf16[128,256]{1,0:T(8,128)(2,1)}, u32[]{:S(2)}) copy-start(bf16[128,256]{1,0:T(8,128)(2,1)} %param.33) | copy-start | bytes 196612
  115.2 0.7 copy-start.10
  116.5 3.8 %copy-start.17 = (bf16[256]{0:T(256)(128)(2,1)S(1)}, bf16[256]{0:T(256)(128)(2,1)}, u32[]{:S(2)}) copy-start(bf16[256]{0:T(256)(128)(2,1)} %param.34) | copy-start | bytes 1540
  116.5 11.7 %all-to-all-start.4 = ((bf16[16,128,16]{1,2,0:T(8,128)(2,1)}), bf16[16,128,16]{1,2,0:T(8,128)(2,1)S(1)}, u32[]{:S(2)}, u32[]{:S(2)}) async-start(bf16[16,128,16]{1,2,0:T(8,128)(2,1)} %broadcast_in_dim.10), calls=%async_computation.4 | async-start | bytes 131072 | tf_op jit(solution)/shard_map/all_to_all | solution.py:41
  128.3 1.0 copy-start.2
  151.0 23.1 %copy-start.3 = (bf16[688,256]{1,0:T(8,128)(2,1)S(1)}, bf16[688,256]{1,0:T(8,128)(2,1)}, u32[]{:S(2)}) copy-start(bf16[688,256]{1,0:T(8,128)(2,1)} %param.37) | copy-start | bytes 1056772
  175.1 15.9 %all-to-all-start.7 = ((bf16[16,128,16]{1,2,0:T(8,128)(2,1)}), bf16[16,128,16]{1,2,0:T(8,128)(2,1)S(1)}, u32[]{:S(2)}, u32[]{:S(2)}) async-start(bf16[16,128,16]{1,2,0:T(8,128)(2,1)} %bitcast.31), calls=%async_computation.7 | async-start | bytes 131072 | tf_op jit(solution)/shard_map/all_to_all | solution.py:52

commit v2 on v1

v2 whole, which is shorter than its diff:
```python
import jax
import jax.numpy as jnp
from jax import lax
from jax.experimental import pallas as pl
from jax.experimental.pallas import tpu as pltpu
from jax.sharding import PartitionSpec as P

D = 4096
DK = 64
DV = 128
LANES = 128


norm_eps = 1e-06
igate_cap = 1.5

VMEM = pl.BlockSpec(memory_space=pltpu.VMEM)
ANY = pl.BlockSpec(memory_space=pl.ANY)
HBM = pl.BlockSpec(memory_space=pltpu.HBM)
SMALL = pltpu.CompilerParams(vmem_limit_bytes=8 * 2**20)


def exchanged(blocks, axis):
    return lax.all_to_all(blocks, axis, split_axis=0, concat_axis=0, tiled=True)


def spread_kernel(value_ref, out_ref):
    value = value_ref[...]
    for copy in range(out_ref.shape[0]):
        out_ref[copy] = value


def spread(value, count):
    return pl.pallas_call(
        spread_kernel,
        out_shape=jax.ShapeDtypeStruct((count, *value.shape), value.dtype),
        in_specs=[VMEM],
        out_specs=VMEM,
        compiler_params=SMALL,
        name="spread",
    )(value)


def project_kernel(
    x_ref, gain_ref, query_ref, key_ref, value_ref, ogate_ref, igate_ref, fgate_ref,
    ibias_ref, fbias_ref, out_ref, bias_ref, qk, val, og, biases, sems,
):
    copies = [
        pltpu.make_async_copy(query_ref, qk.at[pl.ds(0, DK)], sems.at[0]),
        pltpu.make_async_copy(key_ref, qk.at[pl.ds(DK, DK)], sems.at[1]),
        pltpu.make_async_copy(value_ref, val, sems.at[2]),
        pltpu.make_async_copy(ogate_ref, og, sems.at[3]),
        pltpu.make_async_copy(ibias_ref, biases.at[0], sems.at[4]),
        pltpu.make_async_copy(fbias_ref, biases.at[1], sems.at[5]),
    ]
    for copy in copies:
        copy.start()
    x = x_ref[...].astype(jnp.float32).T
    normed = (x * gain_ref[...].astype(jnp.float32)[None, :]).astype(jnp.bfloat16)
    wide = normed.astype(jnp.float32)
    squares = jnp.sum(x * x, axis=1, keepdims=True)
    igate = jnp.sum(wide * igate_ref[...].astype(jnp.float32), axis=1, keepdims=True)
    fgate = jnp.sum(wide * fgate_ref[...].astype(jnp.float32), axis=1, keepdims=True)
    lane = lax.broadcasted_iota(jnp.int32, (x.shape[0], LANES), 1)
    tail = jnp.where(lane == 0, igate, jnp.where(lane == 1, fgate, jnp.where(lane == 2, squares, 0.0)))
    out_ref[:, 3 * LANES :] = tail.astype(out_ref.dtype)
    copies[0].wait()
    copies[1].wait()
    both = lax.dot_general(
        normed, qk[...], (((1,), (1,)), ((), ())), preferred_element_type=jnp.float32
    )
    out_ref[:, :LANES] = both.astype(out_ref.dtype)
    copies[2].wait()
    out_ref[:, LANES : 2 * LANES] = jnp.dot(
        normed, val[...], preferred_element_type=jnp.float32
    ).astype(out_ref.dtype)
    copies[3].wait()
    out_ref[:, 2 * LANES : 3 * LANES] = jnp.dot(
        normed, og[...], preferred_element_type=jnp.float32
    ).astype(out_ref.dtype)
    copies[4].wait()
    copies[5].wait()
    row = lax.broadcasted_iota(jnp.int32, bias_ref.shape, 0)
    bias_ref[...] = jnp.where(row == 0, biases[0, 0], biases[1, 0])


def project(
    x, gain, w_query, w_key, w_value, w_ogate, w_igate, w_fgate, igate_bias, fgate_bias
):
    rows, seqs = x.shape
    return pl.pallas_call(
        project_kernel,
        out_shape=(
            jax.ShapeDtypeStruct((seqs, 4 * LANES), jnp.bfloat16),
            jax.ShapeDtypeStruct((8, LANES), jnp.float32),
        ),
        in_specs=[VMEM, VMEM, ANY, ANY, ANY, ANY, VMEM, VMEM, HBM, HBM],
        out_specs=(VMEM, VMEM),
        scratch_shapes=[
            pltpu.VMEM((2 * DK, rows), jnp.bfloat16),
            pltpu.VMEM((rows, DV), jnp.bfloat16),
            pltpu.VMEM((rows, DV), jnp.bfloat16),
            pltpu.SMEM((2, 1), jnp.float32),
            pltpu.SemaphoreType.DMA((6,)),
        ],
        compiler_params=SMALL,
        name="project",
    )(x, gain, w_query.T, w_key.T, w_value, w_ogate, w_igate.T, w_fgate.T,
      igate_bias, fgate_bias)


def cell_kernel(
    parts_ref, bias_ref, c_ref, n_ref, m_ref, gain_ref,
    new_c_out, new_n_ref, new_m_ref, out_ref, new_c_ref, sem,
):
    total = parts_ref[0].astype(jnp.float32)
    for k in range(1, parts_ref.shape[0]):
        total += parts_ref[k].astype(jnp.float32)
    seqs = total.shape[0]
    tail = total[:, 3 * LANES :]
    row_scale = lax.rsqrt(tail[:, 2:3] / D + norm_eps)
    igate = igate_cap * jnp.tanh((row_scale * tail[:, 0:1] + bias_ref[0:1, 0:1]) / igate_cap)
    fgate = row_scale * tail[:, 1:2] + bias_ref[1:2, 0:1]
    diagonal = lax.broadcasted_iota(jnp.int32, (seqs, seqs), 0) == lax.broadcasted_iota(
        jnp.int32, (seqs, seqs), 1
    )
    state_m = jnp.sum(jnp.where(diagonal, m_ref[...], 0.0), axis=1, keepdims=True)
    log_keep = jnp.minimum(fgate, 0.0) - jnp.log1p(jnp.exp(-jnp.abs(fgate)))
    carried = log_keep + state_m
    new_m = jnp.maximum(carried, igate)
    keep = jnp.exp(carried - new_m)
    write = jnp.exp(igate - new_m)
    new_m_ref[...] = jnp.sum(jnp.where(diagonal, new_m, 0.0), axis=0, keepdims=True)
    lane = lax.broadcasted_iota(jnp.int32, (seqs, LANES), 1)
    first = total[:, :LANES]
    query_key = row_scale * jnp.where(lane < DK, first, first * DK ** (-0.5))
    query = query_key[:, :DK]
    key_vec = query_key[:, DK:]
    value_vec = row_scale * total[:, LANES : 2 * LANES]
    ogate = row_scale * total[:, 2 * LANES : 3 * LANES]
    new_n = keep * n_ref[...] + write * key_vec
    new_n_ref[...] = new_n
    denominator = jnp.maximum(
        jnp.abs(jnp.sum(query * new_n, axis=1, keepdims=True)), jnp.exp(-new_m)
    )
    columns = jnp.where(lane < DK, query_key, write * query_key).T
    for b in range(seqs):
        key_b = columns[DK:, b : b + 1]
        new_c_ref[b] = keep[b : b + 1, :] * c_ref[b] + key_b * value_vec[b : b + 1, :]
    copy_out = pltpu.make_async_copy(new_c_ref, new_c_out, sem)
    copy_out.start()
    rows = []
    for b in range(seqs):
        query_b = columns[:DK, b : b + 1]
        rows.append(jnp.sum(query_b * new_c_ref[b], axis=0, keepdims=True))
    head_out = jnp.concatenate(rows, axis=0) / denominator
    merged = head_out * gain_ref[...].astype(jnp.float32) / (1.0 + jnp.exp(-ogate))
    merged = merged.astype(out_ref.dtype)
    for copy in range(out_ref.shape[0]):
        out_ref[copy] = merged
    copy_out.wait()


def cell(parts, biases, state_c, state_n, state_m, head_gain):
    count, seqs, _ = parts.shape
    new_c, new_n, new_m, out = pl.pallas_call(
        cell_kernel,
        out_shape=(
            jax.ShapeDtypeStruct((seqs, DK, DV), jnp.float32),
            jax.ShapeDtypeStruct((seqs, DK), jnp.float32),
            jax.ShapeDtypeStruct((1, seqs), jnp.float32),
            jax.ShapeDtypeStruct((count, seqs, DV), jnp.bfloat16),
        ),
        in_specs=[VMEM] * 6,
        out_specs=(ANY, VMEM, VMEM, VMEM),
        scratch_shapes=[
            pltpu.VMEM((seqs, DK, DV), jnp.float32),
            pltpu.SemaphoreType.DMA,
        ],
        compiler_params=SMALL,
        name="cell",
    )(
        parts, biases, state_c.reshape(seqs, DK, DV),
        state_n.reshape(seqs, DK), state_m.T, head_gain,
    )
    return new_c.reshape(state_c.shape), new_n.reshape(state_n.shape), new_m.T, out


def residual_kernel(parts_ref, tokens_ref, out_ref):
    total = parts_ref[0].astype(jnp.float32)
    for k in range(1, parts_ref.shape[0]):
        total += parts_ref[k].astype(jnp.float32)
    middle = (tokens_ref[0].astype(jnp.float32) + total).astype(out_ref.dtype)
    for copy in range(out_ref.shape[0]):
        out_ref[copy] = middle


def residual(parts, copies):
    return pl.pallas_call(
        residual_kernel,
        out_shape=jax.ShapeDtypeStruct(copies.shape, copies.dtype),
        in_specs=[VMEM, VMEM],
        out_specs=VMEM,
        compiler_params=SMALL,
        name="residual",
    )(parts, copies)


def widen_kernel(x_ref, gain_ref, gate_ref, up_ref, out_ref, weights, sems):
    units = gate_ref.shape[0]
    cols = out_ref.shape[1]
    gate_copy = pltpu.make_async_copy(gate_ref, weights.at[pl.ds(0, units)], sems.at[0])
    up_copy = pltpu.make_async_copy(up_ref, weights.at[pl.ds(units, units)], sems.at[1])
    gate_copy.start()
    up_copy.start()
    weights[2 * units :, :] = jnp.zeros((cols - 2 * units, weights.shape[1]), weights.dtype)
    x = x_ref[...].astype(jnp.float32).T
    normed = (x * gain_ref[...].astype(jnp.float32)[None, :]).astype(jnp.bfloat16)
    squares = jnp.sum(x * x, axis=1, keepdims=True)
    gate_copy.wait()
    start = units // LANES * LANES

    def product(at, size):
        return lax.dot_general(
            normed, weights[at : at + size, :], (((1,), (1,)), ((), ())),
            preferred_element_type=jnp.float32,
        )

    out_ref[:, :start] = product(0, start).astype(out_ref.dtype)
    up_copy.wait()
    last = cols - LANES
    out_ref[:, start:last] = product(start, last - start).astype(out_ref.dtype)
    lane = lax.broadcasted_iota(jnp.int32, (x.shape[0], LANES), 1)
    tail = jnp.where(lane == 2 * units - last, squares, product(last, LANES))
    out_ref[:, last:] = tail.astype(out_ref.dtype)


def widen(x, gain, w_gate, w_up):
    rows, seqs = x.shape
    cols = (2 * w_gate.shape[1] // LANES + 1) * LANES
    return pl.pallas_call(
        widen_kernel,
        out_shape=jax.ShapeDtypeStruct((seqs, cols), jnp.bfloat16),
        in_specs=[VMEM, VMEM, ANY, ANY],
        out_specs=VMEM,
        scratch_shapes=[
            pltpu.VMEM((cols, rows), jnp.bfloat16),
            pltpu.SemaphoreType.DMA((2,)),
        ],
        compiler_params=SMALL,
        name="widen",
    )(x, gain, w_gate.T, w_up.T)


def body(
    tokens,
    norm_gain,
    w_query,
    w_key,
    w_value,
    w_ogate,
    w_igate,
    w_fgate,
    igate_bias,
    fgate_bias,
    state_c,
    state_n,
    state_m,
    head_gain,
    w_out,
    ffn_gain,
    w_gate,
    w_up,
    w_down,
):
    n_kv, n_tp = lax.axis_size("kv"), lax.axis_size("tp")
    seqs, feats = tokens.shape
    units = w_gate.shape[1]
    rows = n_tp * feats
    own_seqs = seqs // n_kv

    token_copies = spread(tokens.T, n_tp)
    token_rows = exchanged(token_copies, "tp").reshape(rows, seqs)
    parts, biases = project(
        token_rows, norm_gain, w_query, w_key, w_value, w_ogate, w_igate, w_fgate,
        igate_bias, fgate_bias,
    )
    arrived = exchanged(parts.reshape(n_kv, own_seqs, -1), "kv")
    new_c, new_n, new_m, merged = cell(
        arrived, biases, state_c, state_n, state_m, head_gain
    )
    merged_all = exchanged(merged, "kv").reshape(seqs, -1)
    attn_part = jnp.dot(merged_all, w_out, preferred_element_type=jnp.float32)
    attn_part = attn_part.astype(jnp.bfloat16).T.reshape(n_tp, feats, seqs)
    middle_copies = residual(exchanged(attn_part, "tp"), token_copies)
    middle_rows = exchanged(middle_copies, "tp").reshape(rows, seqs)
    wide = widen(middle_rows, ffn_gain, w_gate, w_up)
    sums = exchanged(wide.reshape(n_kv, own_seqs, -1), "kv").astype(jnp.float32).sum(axis=0)
    gate_sum, up_sum, total = sums[:, :units], sums[:, units : 2 * units], sums[:, 2 * units]
    ffn_scale = lax.rsqrt(total / D + norm_eps)[:, None]
    hidden = (jax.nn.silu(ffn_scale * gate_sum) * (ffn_scale * up_sum)).astype(jnp.bfloat16)
    hidden_all = exchanged(
        jnp.broadcast_to(hidden[None], (n_kv, *hidden.shape)), "kv"
    ).reshape(seqs, units)
    down_part = jnp.dot(hidden_all, w_down, preferred_element_type=jnp.float32)
    down_part = down_part.astype(jnp.bfloat16).T.reshape(n_tp, feats, seqs)
    down_out = exchanged(down_part, "tp").astype(jnp.float32).sum(axis=0)
    out_tokens = (middle_copies[0].astype(jnp.float32) + down_out).astype(jnp.bfloat16).T
    return (out_tokens, new_c, new_n, new_m)


def solution(mesh):
    placed = (
        P("grp", ("kv", "tp")),
        P("kv"),
        P("kv", "tp"),
        P("kv", "tp"),
        P("kv", "tp"),
        P("kv", "tp"),
        P("kv", "tp"),
        P("kv", "tp"),
        P("tp"),
        P("tp"),
        P(("grp", "kv"), "tp", None, None),
        P(("grp", "kv"), "tp", None),
        P(("grp", "kv"), "tp"),
        P("tp", None),
        P("tp", "kv"),
        P("kv"),
        P("kv", "tp"),
        P("kv", "tp"),
        P("tp", "kv"),
    )
    return jax.shard_map(
        body,
        mesh=mesh,
        in_specs=placed,
        out_specs=(
            P("grp", ("kv", "tp")),
            P(("grp", "kv"), "tp", None, None),
            P(("grp", "kv"), "tp", None),
            P(("grp", "kv"), "tp"),
        ),
        check_vma=False,
    )
```

time: 193 us -> 182 us (0.943)
  blocking collectives: 73.6 us -> 118 us
  waiting for transfers between devices: 33.5 us -> 6.62 us
  starting transfers between devices: 64.1 us -> 44.8 us
  local copies, waits for them, and re-layouts: 13.2 us -> 3.01 us
  Pallas kernels: 0 us -> 5.38 us
    all_to_all x4 -> x7, blocking collectives: 73.6 us -> 118 us  [exchanged(): return lax.all_to_all(blocks, axis, split_axis=0, concat_axis=0, tiled=True)]
    all_to_all x4 -> x1, waiting for transfers between devices: 33.5 us -> 6.62 us  [exchanged(): return lax.all_to_all(blocks, axis, split_axis=0, concat_axis=0, tiled=True)]
    all_to_all x4 -> x1, starting transfers between devices: 64.1 us -> 44.8 us  [exchanged(): return lax.all_to_all(blocks, axis, split_axis=0, concat_axis=0, tiled=True)]
    pallas_call x0 -> x5, Pallas kernels: none -> 5.38 us  [the longest x1 1.82 us: cell(): pl.pallas_call(cell_kernel, out_shape=(jax.ShapeDtypeStruct((seqs, DK, DV...]
    unnamed x38 -> x34, local copies, waits for them, and re-layouts: 6.1 us -> 2.76 us
    convert_element_type x8 -> x2, local copies, waits for them, and re-layouts: 2.71 us -> 0.23 us  [the longest x1 0.12 us: body(): attn_part = attn_part.astype(jnp.bfloat16).T.reshape(n_tp, feats, seqs)]
    broadcast_in_dim x4 -> x1, local copies, waits for them, and re-layouts: 2.04 us -> 0.01 us  [body(): jnp.broadcast_to(hidden[None], (n_kv, *hidden.shape))]
  transfers between devices with their start and end apart: 4 -> 1, of which waited for: 4 -> 1; matrix products, arithmetic and copies ran while one was open for 0% -> 0% of each run, Pallas kernels for 0% -> 0%
where the time goes in v2:
time: 182 us
  blocking collectives  118 us (65%)
  starting transfers between devices  44.8 us (25%)
  waiting for transfers between devices  6.62 us (4%)
  Pallas kernels  5.38 us (3%)
  local copies, waits for them, and re-layouts  3.01 us (2%)
  between operations  2.08 us (1%)
    all_to_all x7, blocking collectives, exchanged(): return lax.all_to_all(blocks, axis, split_axis=0, concat_axis=0, tiled=True)  118 us
    all_to_all x1, starting transfers between devices, exchanged(): return lax.all_to_all(blocks, axis, split_axis=0, concat_axis=0, tiled=True)  44.8 us
    all_to_all x1, waiting for transfers between devices, exchanged(): return lax.all_to_all(blocks, axis, split_axis=0, concat_axis=0, tiled=True)  6.62 us
  transfers between devices with their start and end apart: 1, of which 1 were waited for; matrix products, arithmetic and copies ran while one was open for 0% of the time, Pallas kernels for 0%

profile of v2, /device:TPU:65, one launch (start us, length us, event | category | flops | bytes accessed | tf_op | source)
XLA Modules:
  0.0 181.7 jit_solution(12393305428829306728)
XLA Ops:
  0.6 0.0 copy-start
  0.6 0.0 copy-start.9
  0.7 0.7 copy-done.9
  1.4 0.0 copy-start.6
  1.4 0.0 copy-start.7
  1.4 0.6 spread.1.tokens_ref
  2.0 0.0 copy-start.4
  2.0 0.0 copy-start.5
  2.0 44.8 %all-to-all-start = ((bf16[16,16,128]{2,1,0:T(8,128)(2,1)}), bf16[16,16,128]{2,1,0:T(8,128)(2,1)S(1)}, u32[]{:S(2)}, u32[]{:S(2)}) async-start(bf16[16,16,128]{2,1,0:T(8,128)(2,1)} %spread.1.tokens_ref), calls=%async_computation | async-start | bytes 131072 | tf_op jit(solution)/shard_map/all_to_all | solution.py:24
  48.2 6.6 %all-to-all-done = bf16[16,16,128]{2,1,0:T(8,128)(2,1)S(1)} async-done(((bf16[16,16,128]{2,1,0:T(8,128)(2,1)}), bf16[16,16,128]{2,1,0:T(8,128)(2,1)S(1)}, u32[]{:S(2)}, u32[]{:S(2)}) %all-to-all-start) | async-done | bytes 65568 | tf_op jit(solution)/shard_map/all_to_all | solution.py:24
  54.8 0.0 copy-start.11
  54.8 0.0 copy-start.10
  54.8 0.0 copy-start.12
  54.8 0.0 copy-done.6
  54.8 0.0 copy-done.7
  54.8 0.0 copy-done.4
  54.8 0.0 copy-done.5
  54.8 0.6 copy-done.11
  55.5 0.0 copy-done.10
  55.5 0.0 copy-done.12
  55.5 0.0 copy-start.3
  55.5 1.1 project.1
  56.6 19.0 %all_to_all.40.parts_ref = bf16[16,8,512]{2,1,0:T(8,128)(2,1)S(1)} all-to-all(bf16[16,8,512]{2,1,0:T(8,128)(2,1)S(1)} %bitcast.48), channel_id=1, replica_groups=mesh['grp'=2,'kv'=16,'tp'=16] {'kv'}, dimensions={0} | all-to-all | bytes 262144 | tf_op jit(solution)/shard_map/all_to_all | solution.py:24
  75.6 0.0 copy-start.8
  75.6 0.0 copy-start.13
  75.6 0.0 copy-start.14
  75.6 0.0 copy-done.3
  75.6 0.7 copy-done.8
  76.3 0.0 copy-done.13
  76.3 0.0 copy-done.14
  76.3 1.8 %cell.1 = (f32[8,64,128]{2,1,0:T(8,128)}, f32[8,64]{1,0:T(8,128)}, f32[1,8]{1,0:T(1,128)}, bf16[16,8,128]{2,1,0:T(8,128)(2,1)S(1)}) custom-call(bf16[16,8,512]{2,1,0:T(8,128)(2,1)S(1)} %all_to_all.40.parts_ref, f32[8,128]{1,0:T(8,128)S(1)} %get-tuple-element.11.bias_ref, f32[8,64,128]{2,1,0:T(8,128)S(1)} %bitcast.46, f32[8,64]{1,0:T(8,128)S(1)} %bitcast.51, ...), custom_call_target="tpu_custom_call" | custom-call | tf_op jit(solution)/shard_map/cell/pallas_call | solution.py:166
  78.1 0.0 copy-start.16
  78.1 17.9 %all_to_all.41 = bf16[16,8,128]{2,1,0:T(8,128)(2,1)S(1)} all-to-all(bf16[16,8,128]{2,1,0:T(8,128)(2,1)S(1)} %get-tuple-element.12), channel_id=1, replica_groups=mesh['grp'=2,'kv'=16,'tp'=16] {'kv'}, dimensions={0} | all-to-all | bytes 65536 | tf_op jit(solution)/shard_map/all_to_all | solution.py:24
  96.0 0.0 copy-done.16
  96.0 0.0 copy-start.1
  96.0 0.0 copy-start.2
  96.0 0.1 fusion
  96.2 0.1 copy.36
  96.3 12.3 %all_to_all.42.parts_ref = bf16[16,16,128]{2,1,0:T(8,128)(2,1)S(1)} all-to-all(bf16[16,16,128]{2,1,0:T(8,128)(2,1)S(1)} %bitcast.56), channel_id=1, replica_groups=mesh['grp'=2,'kv'=16,'tp'=16] {'tp'}, dimensions={0} | all-to-all | bytes 131072 | tf_op jit(solution)/shard_map/all_to_all | solution.py:24
  108.6 0.9 residual.1
  109.5 10.7 %all_to_all.43 = bf16[16,16,128]{2,1,0:T(8,128)(2,1)S(1)} all-to-all(bf16[16,16,128]{2,1,0:T(8,128)(2,1)S(1)} %residual.1), channel_id=1, replica_groups=mesh['grp'=2,'kv'=16,'tp'=16] {'tp'}, dimensions={0} | all-to-all | bytes 131072 | tf_op jit(solution)/shard_map/all_to_all | solution.py:24
  120.1 0.0 copy-start.15
  120.1 0.0 copy-done.1
  120.1 0.0 copy-done.2
  120.1 0.6 copy-done.15
  120.8 1.0 widen.1
  121.8 20.8 %all_to_all.44 = bf16[16,8,1408]{2,1,0:T(8,128)(2,1)S(1)} all-to-all(bf16[16,8,1408]{2,1,0:T(8,128)(2,1)S(1)} %bitcast.42), channel_id=1, replica_groups=mesh['grp'=2,'kv'=16,'tp'=16] {'kv'}, dimensions={0} | all-to-all | bytes 720896 | tf_op jit(solution)/shard_map/all_to_all | solution.py:24
  142.5 0.1 convert_reduce_fusion
  142.6 0.2 fusion.10
  142.8 0.1 fusion.5
  142.9 22.8 %all_to_all.45 = bf16[16,8,688]{2,1,0:T(8,128)(2,1)S(1)} all-to-all(bf16[16,8,688]{2,1,0:T(8,128)(2,1)S(1)} %broadcast_in_dim.2), channel_id=1, replica_groups=mesh['grp'=2,'kv'=16,'tp'=16] {'kv'}, dimensions={0} | all-to-all | bytes 352256 | tf_op jit(solution)/shard_map/all_to_all | solution.py:24
  165.7 0.0 copy-done
  165.7 0.2 fusion.1
  165.9 0.1 copy.37
  166.0 15.1 %all_to_all.46 = bf16[16,16,128]{2,1,0:T(8,128)(2,1)S(1)} all-to-all(bf16[16,16,128]{2,1,0:T(8,128)(2,1)S(1)} %bitcast.57), channel_id=1, replica_groups=mesh['grp'=2,'kv'=16,'tp'=16] {'tp'}, dimensions={0} | all-to-all | bytes 131072 | tf_op jit(solution)/shard_map/all_to_all | solution.py:24
  181.1 0.6 fusion.7
  (2 shorter events, 0.0 us)
Async XLA Ops:
  0.6 165.1 %copy-start = (bf16[688,256]{1,0:T(8,128)(2,1)S(1)}, bf16[688,256]{1,0:T(8,128)(2,1)}, u32[]{:S(2)}) copy-start(bf16[688,256]{1,0:T(8,128)(2,1)} %param.37) | copy-start | bytes 1056772
  0.6 0.7 copy-start.9
  1.4 53.4 %copy-start.6 = (bf16[256,64]{0,1:T(8,128)(2,1)S(1)}, bf16[256,64]{0,1:T(8,128)(2,1)}, u32[]{:S(2)}) copy-start(bf16[256,64]{0,1:T(8,128)(2,1)} %param.21) | copy-start | bytes 98308
  1.4 53.4 %copy-start.7 = (bf16[256,64]{0,1:T(8,128)(2,1)S(1)}, bf16[256,64]{0,1:T(8,128)(2,1)}, u32[]{:S(2)}) copy-start(bf16[256,64]{0,1:T(8,128)(2,1)} %param.22) | copy-start | bytes 98308
  2.0 52.8 %copy-start.4 = (bf16[256,128]{1,0:T(8,128)(2,1)S(1)}, bf16[256,128]{1,0:T(8,128)(2,1)}, u32[]{:S(2)}) copy-start(bf16[256,128]{1,0:T(8,128)(2,1)} %value_ref.1) | copy-start | bytes 196612
  2.0 52.8 %copy-start.5 = (bf16[256,128]{1,0:T(8,128)(2,1)S(1)}, bf16[256,128]{1,0:T(8,128)(2,1)}, u32[]{:S(2)}) copy-start(bf16[256,128]{1,0:T(8,128)(2,1)} %ogate_ref.1) | copy-start | bytes 196612
  2.0 52.8 %all-to-all-start = ((bf16[16,16,128]{2,1,0:T(8,128)(2,1)}), bf16[16,16,128]{2,1,0:T(8,128)(2,1)S(1)}, u32[]{:S(2)}, u32[]{:S(2)}) async-start(bf16[16,16,128]{2,1,0:T(8,128)(2,1)} %spread.1.tokens_ref), calls=%async_computation | async-start | bytes 131072 | tf_op jit(solution)/shard_map/all_to_all | solution.py:24
  54.8 0.7 copy-start.11
  54.8 0.7 copy-start.10
  54.8 0.7 copy-start.12
  55.5 20.1 %copy-start.3 = (f32[8,1,64,128]{3,2,1,0:T(8,128)S(1)}, f32[8,1,64,128]{3,2,1,0:T(8,128)}, u32[]{:S(2)}) copy-start(f32[8,1,64,128]{3,2,1,0:T(8,128)} %param.29) | copy-start | bytes 786436
  75.6 0.7 copy-start.8
  75.6 0.7 copy-start.13
  75.6 0.7 copy-start.14
  78.1 17.9 %copy-start.16 = (bf16[128,256]{1,0:T(8,128)(2,1)S(1)}, bf16[128,256]{1,0:T(8,128)(2,1)}, u32[]{:S(2)}) copy-start(bf16[128,256]{1,0:T(8,128)(2,1)} %param.33) | copy-start | bytes 196612
  96.0 24.1 %copy-start.1 = (bf16[256,688]{0,1:T(8,128)(2,1)S(1)}, bf16[256,688]{0,1:T(8,128)(2,1)}, u32[]{:S(2)}) copy-start(bf16[256,688]{0,1:T(8,128)(2,1)} %param.35) | copy-start | bytes 1056772
  96.0 24.1 %copy-start.2 = (bf16[256,688]{0,1:T(8,128)(2,1)S(1)}, bf16[256,688]{0,1:T(8,128)(2,1)}, u32[]{:S(2)}) copy-start(bf16[256,688]{0,1:T(8,128)(2,1)} %param.36) | copy-start | bytes 1056772
  120.1 0.7 copy-start.15

commit v3 on v2

v3 whole, which is shorter than its diff:
```python
import jax
import jax.numpy as jnp
from jax import lax
from jax.experimental import pallas as pl
from jax.experimental.pallas import tpu as pltpu
from jax.sharding import PartitionSpec as P

D = 4096
DK = 64
DV = 128
LANES = 128


norm_eps = 1e-06
igate_cap = 1.5

VMEM = pl.BlockSpec(memory_space=pltpu.VMEM)
ANY = pl.BlockSpec(memory_space=pl.ANY)
SMALL = pltpu.CompilerParams(vmem_limit_bytes=8 * 2**20)


def exchanged(blocks, axis):
    return lax.all_to_all(blocks, axis, split_axis=0, concat_axis=0, tiled=True)


def spread_kernel(value_ref, out_ref, own_ref):
    value = value_ref[...]
    own_ref[...] = value
    for copy in range(out_ref.shape[0]):
        out_ref[copy] = value


def spread(value, count):
    return pl.pallas_call(
        spread_kernel,
        out_shape=(
            jax.ShapeDtypeStruct((count, *value.shape), value.dtype),
            jax.ShapeDtypeStruct(value.shape, value.dtype),
        ),
        in_specs=[VMEM],
        out_specs=(VMEM, VMEM),
        compiler_params=SMALL,
        name="spread",
    )(value)


def transposed_product(x, weight):
    return lax.dot_general(
        x, weight, (((1,), (1,)), ((), ())), preferred_element_type=jnp.float32
    )


def project_kernel(
    x_ref, vectors_ref, small_ref, both_ref, value_ref, ogate_ref, out_ref, handed_ref
):
    handed_ref[...] = small_ref[...]
    x = x_ref[...].astype(jnp.float32).T
    normed = (x * vectors_ref[0:1, :]).astype(jnp.bfloat16)
    out_ref[:, :LANES] = transposed_product(normed, both_ref[...]).astype(out_ref.dtype)
    out_ref[:, LANES : 2 * LANES] = jnp.dot(
        normed, value_ref[...], preferred_element_type=jnp.float32
    ).astype(out_ref.dtype)
    out_ref[:, 2 * LANES : 3 * LANES] = jnp.dot(
        normed, ogate_ref[...], preferred_element_type=jnp.float32
    ).astype(out_ref.dtype)
    wide = normed.astype(jnp.float32)
    squares = jnp.sum(x * x, axis=1, keepdims=True)
    igate = jnp.sum(wide * vectors_ref[1:2, :], axis=1, keepdims=True)
    fgate = jnp.sum(wide * vectors_ref[2:3, :], axis=1, keepdims=True)
    lane = lax.broadcasted_iota(jnp.int32, (x.shape[0], LANES), 1)
    tail = jnp.where(
        lane == 0, igate, jnp.where(lane == 1, fgate, jnp.where(lane == 2, squares, 0.0))
    )
    out_ref[:, 3 * LANES :] = tail.astype(out_ref.dtype)


def project(x, vectors, small, w_both, w_value, w_ogate):
    return pl.pallas_call(
        project_kernel,
        out_shape=(
            jax.ShapeDtypeStruct((x.shape[1], 4 * LANES), jnp.bfloat16),
            jax.ShapeDtypeStruct(small.shape, small.dtype),
        ),
        in_specs=[VMEM] * 6,
        out_specs=(VMEM, VMEM),
        compiler_params=SMALL,
        name="project",
    )(x, vectors, small, w_both, w_value, w_ogate)


def cell_kernel(
    parts_ref, c_ref, small_ref,
    new_c_out, new_n_ref, new_m_ref, out_ref, new_c_ref, sems,
):
    total = parts_ref[0].astype(jnp.float32)
    for k in range(1, parts_ref.shape[0]):
        total += parts_ref[k].astype(jnp.float32)
    seqs = total.shape[0]
    tail = total[:, 3 * LANES :]
    row_scale = lax.rsqrt(tail[:, 2:3] / D + norm_eps)
    igate = igate_cap * jnp.tanh((row_scale * tail[:, 0:1] + small_ref[seqs + 2 : seqs + 3, 0:1]) / igate_cap)
    fgate = row_scale * tail[:, 1:2] + small_ref[seqs + 2 : seqs + 3, 1:2]
    diagonal = lax.broadcasted_iota(jnp.int32, (seqs, seqs), 0) == lax.broadcasted_iota(
        jnp.int32, (seqs, seqs), 1
    )
    state_m = jnp.sum(jnp.where(diagonal, small_ref[seqs : seqs + 1, :seqs], 0.0), axis=1, keepdims=True)
    log_keep = jnp.minimum(fgate, 0.0) - jnp.log1p(jnp.exp(-jnp.abs(fgate)))
    carried = log_keep + state_m
    new_m = jnp.maximum(carried, igate)
    keep = jnp.exp(carried - new_m)
    write = jnp.exp(igate - new_m)
    new_m_ref[...] = jnp.sum(jnp.where(diagonal, new_m, 0.0), axis=0, keepdims=True)
    lane = lax.broadcasted_iota(jnp.int32, (seqs, LANES), 1)
    first = total[:, :LANES]
    query_key = row_scale * jnp.where(lane < DK, first, first * DK ** (-0.5))
    query = query_key[:, :DK]
    key_vec = query_key[:, DK:]
    value_vec = row_scale * total[:, LANES : 2 * LANES]
    ogate = row_scale * total[:, 2 * LANES : 3 * LANES]
    new_n = keep * small_ref[:seqs, :DK] + write * key_vec
    new_n_ref[...] = new_n
    denominator = jnp.maximum(
        jnp.abs(jnp.sum(query * new_n, axis=1, keepdims=True)), jnp.exp(-new_m)
    )
    columns = jnp.where(lane < DK, query_key, write * query_key).T
    copies = []
    for b in range(seqs):
        key_b = columns[DK:, b : b + 1]
        new_c_ref[b] = keep[b : b + 1, :] * c_ref[b] + key_b * value_vec[b : b + 1, :]
        copies.append(pltpu.make_async_copy(new_c_ref.at[b], new_c_out.at[b], sems.at[b]))
        copies[b].start()
    rows = []
    for b in range(seqs):
        query_b = columns[:DK, b : b + 1]
        rows.append(jnp.sum(query_b * new_c_ref[b], axis=0, keepdims=True))
    head_out = jnp.concatenate(rows, axis=0) / denominator
    merged = head_out * small_ref[seqs + 1 : seqs + 2, :] / (1.0 + jnp.exp(-ogate))
    merged = merged.astype(out_ref.dtype)
    for copy in range(out_ref.shape[0]):
        out_ref[copy] = merged
    for copy in copies:
        copy.wait()


def cell(parts, state_c, small):
    count, seqs, _ = parts.shape
    new_c, new_n, new_m, out = pl.pallas_call(
        cell_kernel,
        out_shape=(
            jax.ShapeDtypeStruct((seqs, DK, DV), jnp.float32),
            jax.ShapeDtypeStruct((seqs, DK), jnp.float32),
            jax.ShapeDtypeStruct((1, seqs), jnp.float32),
            jax.ShapeDtypeStruct((count, seqs, DV), jnp.bfloat16),
        ),
        in_specs=[VMEM] * 3,
        out_specs=(ANY, VMEM, VMEM, VMEM),
        scratch_shapes=[
            pltpu.VMEM((seqs, DK, DV), jnp.float32),
            pltpu.SemaphoreType.DMA((seqs,)),
        ],
        compiler_params=SMALL,
        name="cell",
    )(
        parts, state_c.reshape(seqs, DK, DV), small,
    )
    return new_c.reshape(state_c.shape), new_n.reshape(seqs, 1, DK), new_m.T, out


def residual_kernel(parts_ref, tokens_ref, out_ref):
    total = parts_ref[0].astype(jnp.float32)
    for k in range(1, parts_ref.shape[0]):
        total += parts_ref[k].astype(jnp.float32)
    middle = (tokens_ref[...].astype(jnp.float32) + total).astype(out_ref.dtype)
    for copy in range(out_ref.shape[0]):
        out_ref[copy] = middle


def residual(parts, tokens):
    return pl.pallas_call(
        residual_kernel,
        out_shape=jax.ShapeDtypeStruct(parts.shape, parts.dtype),
        in_specs=[VMEM, VMEM],
        out_specs=VMEM,
        compiler_params=SMALL,
        name="residual",
    )(parts, tokens)


def widen_kernel(x_ref, vectors_ref, gate_ref, up_ref, out_ref):
    units = gate_ref.shape[0]
    cols = out_ref.shape[1]
    start = units // LANES * LANES
    taken = (LANES - (units - start)) % LANES
    x = x_ref[...].astype(jnp.float32).T
    normed = (x * vectors_ref[3:4, :]).astype(jnp.bfloat16)
    out_ref[:, :start] = transposed_product(normed, gate_ref[:start, :]).astype(out_ref.dtype)
    if taken:
        mixed = jnp.concatenate([gate_ref[start:, :], up_ref[:taken, :]], axis=0)
        out_ref[:, start : start + LANES] = transposed_product(normed, mixed).astype(
            out_ref.dtype
        )
        start += LANES
    filler = jnp.zeros((cols - 2 * units, gate_ref.shape[1]), gate_ref.dtype)
    rest = transposed_product(normed, jnp.concatenate([up_ref[taken:, :], filler], axis=0))
    lane = lax.broadcasted_iota(jnp.int32, rest.shape, 1)
    squares = jnp.sum(x * x, axis=1, keepdims=True)
    out_ref[:, start:] = jnp.where(lane == 2 * units - start, squares, rest).astype(out_ref.dtype)


def widen(x, vectors, w_gate, w_up):
    cols = (2 * w_gate.shape[1] // LANES + 1) * LANES
    return pl.pallas_call(
        widen_kernel,
        out_shape=jax.ShapeDtypeStruct((x.shape[1], cols), jnp.bfloat16),
        in_specs=[VMEM] * 4,
        out_specs=VMEM,
        compiler_params=SMALL,
        name="widen",
    )(x, vectors, w_gate.T, w_up.T)


def body(
    tokens,
    norm_gain,
    w_query,
    w_key,
    w_value,
    w_ogate,
    w_igate,
    w_fgate,
    igate_bias,
    fgate_bias,
    state_c,
    state_n,
    state_m,
    head_gain,
    w_out,
    ffn_gain,
    w_gate,
    w_up,
    w_down,
):
    n_kv, n_tp = lax.axis_size("kv"), lax.axis_size("tp")
    seqs, feats = tokens.shape
    units = w_gate.shape[1]
    rows = n_tp * feats
    own_seqs = seqs // n_kv

    wide = [norm_gain[None], w_igate.T, w_fgate.T, ffn_gain[None]]
    vectors = jnp.concatenate(wide, axis=0).astype(jnp.float32)
    narrow = [
        state_n.reshape(own_seqs, DK), state_m.T, head_gain.astype(jnp.float32),
        jnp.stack([igate_bias, fgate_bias], axis=1),
    ]
    small = jnp.concatenate(
        [jnp.pad(one, ((0, 0), (0, LANES - one.shape[1]))) for one in narrow], axis=0
    )
    token_copies, own_tokens = spread(tokens.T, n_tp)
    token_rows = exchanged(token_copies, "tp").reshape(rows, seqs)
    w_both = jnp.concatenate([w_query.T, w_key.T], axis=0)
    parts, small = project(token_rows, vectors, small, w_both, w_value, w_ogate)
    arrived = exchanged(parts.reshape(n_kv, own_seqs, -1), "kv")
    new_c, new_n, new_m, merged = cell(arrived, state_c, small)
    merged_all = exchanged(merged, "kv").reshape(seqs, -1)
    attn_part = jnp.dot(merged_all, w_out, preferred_element_type=jnp.float32)
    attn_part = attn_part.astype(jnp.bfloat16).T.reshape(n_tp, feats, seqs)
    middle_copies = residual(exchanged(attn_part, "tp"), own_tokens)
    middle_rows = exchanged(middle_copies, "tp").reshape(rows, seqs)
    spread_out = widen(middle_rows, vectors, w_gate, w_up)
    sums = exchanged(spread_out.reshape(n_kv, own_seqs, -1), "kv").astype(jnp.float32).sum(axis=0)
    gate_sum, up_sum, total = sums[:, :units], sums[:, units : 2 * units], sums[:, 2 * units]
    ffn_scale = lax.rsqrt(total / D + norm_eps)[:, None]
    hidden = (jax.nn.silu(ffn_scale * gate_sum) * (ffn_scale * up_sum)).astype(jnp.bfloat16)
    hidden_all = exchanged(
        jnp.broadcast_to(hidden[None], (n_kv, *hidden.shape)), "kv"
    ).reshape(seqs, units)
    down_part = jnp.dot(hidden_all, w_down, preferred_element_type=jnp.float32)
    down_part = down_part.astype(jnp.bfloat16).T.reshape(n_tp, feats, seqs)
    down_out = exchanged(down_part, "tp").astype(jnp.float32).sum(axis=0)
    out_tokens = (middle_copies[0].astype(jnp.float32) + down_out).astype(jnp.bfloat16).T
    return (out_tokens, new_c, new_n, new_m)


def solution(mesh):
    placed = (
        P("grp", ("kv", "tp")),
        P("kv"),
        P("kv", "tp"),
        P("kv", "tp"),
        P("kv", "tp"),
        P("kv", "tp"),
        P("kv", "tp"),
        P("kv", "tp"),
        P("tp"),
        P("tp"),
        P(("grp", "kv"), "tp", None, None),
        P(("grp", "kv"), "tp", None),
        P(("grp", "kv"), "tp"),
        P("tp", None),
        P("tp", "kv"),
        P("kv"),
        P("kv", "tp"),
        P("kv", "tp"),
        P("tp", "kv"),
    )
    return jax.shard_map(
        body,
        mesh=mesh,
        in_specs=placed,
        out_specs=(
            P("grp", ("kv", "tp")),
            P(("grp", "kv"), "tp", None, None),
            P(("grp", "kv"), "tp", None),
            P(("grp", "kv"), "tp"),
        ),
        check_vma=False,
    )
```

time: 182 us -> 178 us (0.978)
  Pallas kernels: 5.38 us -> 3.18 us
    pallas_call x4, Pallas kernels: 3.56 us -> 1.32 us  [the longest x1 0.64 us: spread(): pl.pallas_call(spread_kernel, out_shape=(jax.ShapeDtypeStruct((count, *va...]
where the time goes in v3:
time: 178 us; the launch traced here: 177 us
  blocking collectives  118 us (66%)
  starting transfers between devices  44.9 us (25%)
  waiting for transfers between devices  5.68 us (3%)
  Pallas kernels  3.18 us (2%)
  between operations  2.17 us (1%)
    all_to_all x7, blocking collectives, exchanged(): return lax.all_to_all(blocks, axis, split_axis=0, concat_axis=0, tiled=True)  118 us
    all_to_all x1, starting transfers between devices, exchanged(): return lax.all_to_all(blocks, axis, split_axis=0, concat_axis=0, tiled=True)  44.9 us
    all_to_all x1, waiting for transfers between devices, exchanged(): return lax.all_to_all(blocks, axis, split_axis=0, concat_axis=0, tiled=True)  5.68 us
  transfers between devices with their start and end apart: 1, of which 1 were waited for; matrix products, arithmetic and copies ran while one was open for 0% of the time, Pallas kernels for 0%

profile of v3, /device:TPU:65, one launch (start us, length us, event | category | flops | bytes accessed | tf_op | source)
XLA Modules:
  0.0 177.5 jit_solution(6875220236536898989)
XLA Ops:
  0.6 0.0 copy-start
  0.6 0.0 copy-start.6
  0.7 0.7 copy-done.6
  1.4 0.6 spread.1
  2.0 0.0 copy-start.14
  2.0 0.0 copy-start.15
  2.0 0.0 copy-start.16
  2.0 0.0 copy-start.10
  2.0 0.0 copy-start.13
  2.0 0.0 copy-start.9
  2.1 44.9 %all-to-all-start = ((bf16[16,16,128]{2,1,0:T(8,128)(2,1)}), bf16[16,16,128]{2,1,0:T(8,128)(2,1)S(1)}, u32[]{:S(2)}, u32[]{:S(2)}) async-start(bf16[16,16,128]{2,1,0:T(8,128)(2,1)} %get-tuple-element.12), calls=%async_computation | async-start | bytes 131072 | tf_op jit(solution)/shard_map/all_to_all | solution.py:23
  46.9 0.0 copy-start.8
  48.2 0.0 copy-done.14
  48.3 0.0 copy-done.15
  48.3 0.0 copy-done.16
  48.3 0.1 fusion.14
  48.4 0.0 copy-done.10
  48.4 0.0 copy-done.13
  48.4 0.0 copy-start.12
  48.4 0.0 copy-start.11
  48.4 0.7 copy-done.12
  49.1 0.0 copy-done.11
  49.1 0.0 copy-done.9
  49.1 0.0 copy-done.8
  49.1 0.0 copy-start.4
  49.1 0.0 copy-start.5
  49.2 5.7 %all-to-all-done = bf16[16,16,128]{2,1,0:T(8,128)(2,1)S(1)} async-done(((bf16[16,16,128]{2,1,0:T(8,128)(2,1)}), bf16[16,16,128]{2,1,0:T(8,128)(2,1)S(1)}, u32[]{:S(2)}, u32[]{:S(2)}) %all-to-all-start) | async-done | bytes 65568 | tf_op jit(solution)/shard_map/all_to_all | solution.py:23
  54.9 0.0 copy-done.4
  54.9 0.0 copy-done.5
  54.9 0.0 copy-start.3
  54.9 0.3 project.1
  55.1 19.0 %all_to_all.40.parts_ref = bf16[16,8,512]{2,1,0:T(8,128)(2,1)S(1)} all-to-all(bf16[16,8,512]{2,1,0:T(8,128)(2,1)S(1)} %bitcast.52), channel_id=1, replica_groups=mesh['grp'=2,'kv'=16,'tp'=16] {'kv'}, dimensions={0} | all-to-all | bytes 262144 | tf_op jit(solution)/shard_map/all_to_all | solution.py:23
  74.1 0.0 copy-done.3
  74.1 0.0 copy-start.7
  74.1 1.9 %cell.1 = (f32[8,64,128]{2,1,0:T(8,128)}, f32[8,64]{1,0:T(8,128)}, f32[1,8]{1,0:T(1,128)}, bf16[16,8,128]{2,1,0:T(8,128)(2,1)S(1)}) custom-call(bf16[16,8,512]{2,1,0:T(8,128)(2,1)S(1)} %all_to_all.40.parts_ref, f32[8,64,128]{2,1,0:T(8,128)S(1)} %bitcast.50, f32[11,128]{1,0:T(8,128)S(1)} %get-tuple-element.14.small_ref), custom_call_target="tpu_custom_call" | custom-call | tf_op jit(solution)/shard_map/cell/pallas_call | solution.py:147
  76.0 0.0 copy-start.2
  76.0 17.9 %all_to_all.41 = bf16[16,8,128]{2,1,0:T(8,128)(2,1)S(1)} all-to-all(bf16[16,8,128]{2,1,0:T(8,128)(2,1)S(1)} %get-tuple-element.15), channel_id=1, replica_groups=mesh['grp'=2,'kv'=16,'tp'=16] {'kv'}, dimensions={0} | all-to-all | bytes 65536 | tf_op jit(solution)/shard_map/all_to_all | solution.py:23
  93.9 0.0 copy-done.7
  93.9 0.0 copy-start.1
  93.9 0.1 fusion
  94.1 0.1 copy.36
  94.2 12.3 %all_to_all.42.parts_ref = bf16[16,16,128]{2,1,0:T(8,128)(2,1)S(1)} all-to-all(bf16[16,16,128]{2,1,0:T(8,128)(2,1)S(1)} %bitcast.54), channel_id=1, replica_groups=mesh['grp'=2,'kv'=16,'tp'=16] {'tp'}, dimensions={0} | all-to-all | bytes 131072 | tf_op jit(solution)/shard_map/all_to_all | solution.py:23
  106.5 10.7 %all_to_all.43 = bf16[16,16,128]{2,1,0:T(8,128)(2,1)S(1)} all-to-all(bf16[16,16,128]{2,1,0:T(8,128)(2,1)S(1)} %residual.1), channel_id=1, replica_groups=mesh['grp'=2,'kv'=16,'tp'=16] {'tp'}, dimensions={0} | all-to-all | bytes 131072 | tf_op jit(solution)/shard_map/all_to_all | solution.py:23
  117.2 0.0 copy-done.2
  117.2 0.0 copy-done.1
  117.2 0.4 widen.1
  117.6 20.8 %all_to_all.44 = bf16[16,8,1408]{2,1,0:T(8,128)(2,1)S(1)} all-to-all(bf16[16,8,1408]{2,1,0:T(8,128)(2,1)S(1)} %bitcast.46), channel_id=1, replica_groups=mesh['grp'=2,'kv'=16,'tp'=16] {'kv'}, dimensions={0} | all-to-all | bytes 720896 | tf_op jit(solution)/shard_map/all_to_all | solution.py:23
  138.3 0.1 convert_reduce_fusion
  138.4 0.2 fusion.13
  138.6 0.1 fusion.5
  138.7 22.8 %all_to_all.45 = bf16[16,8,688]{2,1,0:T(8,128)(2,1)S(1)} all-to-all(bf16[16,8,688]{2,1,0:T(8,128)(2,1)S(1)} %broadcast_in_dim.15), channel_id=1, replica_groups=mesh['grp'=2,'kv'=16,'tp'=16] {'kv'}, dimensions={0} | all-to-all | bytes 352256 | tf_op jit(solution)/shard_map/all_to_all | solution.py:23
  161.5 0.0 copy-done
  161.5 0.2 fusion.1
  161.7 0.1 copy.37
  161.8 15.1 %all_to_all.46 = bf16[16,16,128]{2,1,0:T(8,128)(2,1)S(1)} all-to-all(bf16[16,16,128]{2,1,0:T(8,128)(2,1)S(1)} %bitcast.55), channel_id=1, replica_groups=mesh['grp'=2,'kv'=16,'tp'=16] {'tp'}, dimensions={0} | all-to-all | bytes 131072 | tf_op jit(solution)/shard_map/all_to_all | solution.py:23
  176.9 0.6 fusion.10
  (9 shorter events, 0.1 us)
Async XLA Ops:
  0.6 160.9 %copy-start = (bf16[688,256]{1,0:T(8,128)(2,1)S(1)}, bf16[688,256]{1,0:T(8,128)(2,1)}, u32[]{:S(2)}) copy-start(bf16[688,256]{1,0:T(8,128)(2,1)} %param.37) | copy-start | bytes 1056772
  0.6 0.7 copy-start.6
  2.0 46.2 %copy-start.14 = (bf16[1,128]{1,0:T(2,128)(2,1)S(1)}, bf16[1,128]{1,0:T(2,128)(2,1)}, u32[]{:S(2)}) copy-start(bf16[1,128]{1,0:T(2,128)(2,1)} %param.32) | copy-start | bytes 772
  2.0 46.2 %copy-start.15 = (bf16[256]{0:T(256)(128)(2,1)S(1)}, bf16[256]{0:T(256)(128)(2,1)}, u32[]{:S(2)}) copy-start(bf16[256]{0:T(256)(128)(2,1)} %param.20) | copy-start | bytes 1540
  2.0 46.3 %copy-start.16 = (bf16[256]{0:T(256)(128)(2,1)S(1)}, bf16[256]{0:T(256)(128)(2,1)}, u32[]{:S(2)}) copy-start(bf16[256]{0:T(256)(128)(2,1)} %param.34) | copy-start | bytes 1540
  2.0 46.4 %copy-start.10 = (f32[8,1,64]{2,1,0:T(1,128)S(1)}, f32[8,1,64]{2,1,0:T(1,128)}, u32[]{:S(2)}) copy-start(f32[8,1,64]{2,1,0:T(1,128)} %param.30) | copy-start | bytes 6148
  2.0 46.4 %copy-start.13 = (f32[8,1]{0,1:T(1,128)S(1)}, f32[8,1]{0,1:T(1,128)}, u32[]{:S(2)}) copy-start(f32[8,1]{0,1:T(1,128)} %param.31) | copy-start | bytes 100
  2.0 47.1 %copy-start.9 = (bf16[256,64]{0,1:T(8,128)(2,1)S(1)}, bf16[256,64]{0,1:T(8,128)(2,1)}, u32[]{:S(2)}) copy-start(bf16[256,64]{0,1:T(8,128)(2,1)} %param.21) | copy-start | bytes 98308
  2.1 52.8 %all-to-all-start = ((bf16[16,16,128]{2,1,0:T(8,128)(2,1)}), bf16[16,16,128]{2,1,0:T(8,128)(2,1)S(1)}, u32[]{:S(2)}, u32[]{:S(2)}) async-start(bf16[16,16,128]{2,1,0:T(8,128)(2,1)} %get-tuple-element.12), calls=%async_computation | async-start | bytes 131072 | tf_op jit(solution)/shard_map/all_to_all | solution.py:23
  46.9 2.2 %copy-start.8 = (bf16[256,64]{0,1:T(8,128)(2,1)S(1)}, bf16[256,64]{0,1:T(8,128)(2,1)}, u32[]{:S(2)}) copy-start(bf16[256,64]{0,1:T(8,128)(2,1)} %param.22) | copy-start | bytes 98308
  48.4 0.7 copy-start.12
  48.4 0.7 copy-start.11
  49.1 5.7 %copy-start.4 = (bf16[256,128]{1,0:T(8,128)(2,1)S(1)}, bf16[256,128]{1,0:T(8,128)(2,1)}, u32[]{:S(2)}) copy-start(bf16[256,128]{1,0:T(8,128)(2,1)} %value_ref.1) | copy-start | bytes 196612
  49.1 5.7 %copy-start.5 = (bf16[256,128]{1,0:T(8,128)(2,1)S(1)}, bf16[256,128]{1,0:T(8,128)(2,1)}, u32[]{:S(2)}) copy-start(bf16[256,128]{1,0:T(8,128)(2,1)} %ogate_ref.1) | copy-start | bytes 196612
  54.9 19.3 %copy-start.3 = (f32[8,1,64,128]{3,2,1,0:T(8,128)S(1)}, f32[8,1,64,128]{3,2,1,0:T(8,128)}, u32[]{:S(2)}) copy-start(f32[8,1,64,128]{3,2,1,0:T(8,128)} %param.29) | copy-start | bytes 786436
  74.1 19.8 %copy-start.7 = (bf16[128,256]{1,0:T(8,128)(2,1)S(1)}, bf16[128,256]{1,0:T(8,128)(2,1)}, u32[]{:S(2)}) copy-start(bf16[128,256]{1,0:T(8,128)(2,1)} %param.33) | copy-start | bytes 196612
  76.0 41.2 %copy-start.2 = (bf16[256,688]{0,1:T(8,128)(2,1)S(1)}, bf16[256,688]{0,1:T(8,128)(2,1)}, u32[]{:S(2)}) copy-start(bf16[256,688]{0,1:T(8,128)(2,1)} %param.36) | copy-start | bytes 1056772
  93.9 23.3 %copy-start.1 = (bf16[256,688]{0,1:T(8,128)(2,1)S(1)}, bf16[256,688]{0,1:T(8,128)(2,1)}, u32[]{:S(2)}) copy-start(bf16[256,688]{0,1:T(8,128)(2,1)} %param.35) | copy-start | bytes 1056772

commit v4 on v3

--- a/solution.py
+++ b/solution.py
@@ -90,7 +90,7 @@
 
 def cell_kernel(
     parts_ref, c_ref, small_ref,
-    new_c_out, new_n_ref, new_m_ref, out_ref, new_c_ref, sems,
+    new_c_ref, new_n_ref, new_m_ref, out_ref,
 ):
     total = parts_ref[0].astype(jnp.float32)
     for k in range(1, parts_ref.shape[0]):
@@ -123,23 +123,18 @@
         jnp.abs(jnp.sum(query * new_n, axis=1, keepdims=True)), jnp.exp(-new_m)
     )
     columns = jnp.where(lane < DK, query_key, write * query_key).T
-    copies = []
-    for b in range(seqs):
-        key_b = columns[DK:, b : b + 1]
-        new_c_ref[b] = keep[b : b + 1, :] * c_ref[b] + key_b * value_vec[b : b + 1, :]
-        copies.append(pltpu.make_async_copy(new_c_ref.at[b], new_c_out.at[b], sems.at[b]))
-        copies[b].start()
     rows = []
     for b in range(seqs):
         query_b = columns[:DK, b : b + 1]
-        rows.append(jnp.sum(query_b * new_c_ref[b], axis=0, keepdims=True))
+        key_b = columns[DK:, b : b + 1]
+        new_c = keep[b : b + 1, :] * c_ref[b] + key_b * value_vec[b : b + 1, :]
+        new_c_ref[b] = new_c
+        rows.append(jnp.sum(query_b * new_c, axis=0, keepdims=True))
     head_out = jnp.concatenate(rows, axis=0) / denominator
     merged = head_out * small_ref[seqs + 1 : seqs + 2, :] / (1.0 + jnp.exp(-ogate))
     merged = merged.astype(out_ref.dtype)
     for copy in range(out_ref.shape[0]):
         out_ref[copy] = merged
-    for copy in copies:
-        copy.wait()
 
 
 def cell(parts, state_c, small):
@@ -153,17 +148,13 @@
             jax.ShapeDtypeStruct((count, seqs, DV), jnp.bfloat16),
         ),
         in_specs=[VMEM] * 3,
-        out_specs=(ANY, VMEM, VMEM, VMEM),
-        scratch_shapes=[
-            pltpu.VMEM((seqs, DK, DV), jnp.float32),
-            pltpu.SemaphoreType.DMA((seqs,)),
-        ],
+        out_specs=(VMEM,) * 4,
         compiler_params=SMALL,
         name="cell",
     )(
         parts, state_c.reshape(seqs, DK, DV), small,
     )
-    return new_c.reshape(state_c.shape), new_n.reshape(seqs, 1, DK), new_m.T, out
+    return (new_c, new_n, new_m), out
 
 
 def residual_kernel(parts_ref, tokens_ref, out_ref):
@@ -184,6 +175,44 @@
         compiler_params=SMALL,
         name="residual",
     )(parts, tokens)
+
+
+def finish_kernel(parts_ref, middle_ref, *refs):
+    count = (len(refs) - 3) // 2
+    states, out_ref, targets = refs[:count], refs[count], refs[count + 1 : -2]
+    tokens, sems = refs[-2:]
+    copies = [
+        pltpu.make_async_copy(state, target, sems.at[k])
+        for k, (state, target) in enumerate(zip(states, targets))
+    ]
+    for copy in copies:
+        copy.start()
+    total = parts_ref[0].astype(jnp.float32)
+    for k in range(1, parts_ref.shape[0]):
+        total += parts_ref[k].astype(jnp.float32)
+    tokens[...] = (middle_ref[0].astype(jnp.float32) + total).astype(tokens.dtype)
+    copies.append(pltpu.make_async_copy(tokens, out_ref, sems.at[count]))
+    copies[count].start()
+    for copy in copies:
+        copy.wait()
+
+
+def finish(parts, middle, *states):
+    return pl.pallas_call(
+        finish_kernel,
+        out_shape=(
+            jax.ShapeDtypeStruct(parts.shape[1:], parts.dtype),
+            *(jax.ShapeDtypeStruct(one.shape, one.dtype) for one in states),
+        ),
+        in_specs=[VMEM] * (2 + len(states)),
+        out_specs=(ANY,) * (1 + len(states)),
+        scratch_shapes=[
+            pltpu.VMEM(parts.shape[1:], parts.dtype),
+            pltpu.SemaphoreType.DMA((1 + len(states),)),
+        ],
+        compiler_params=SMALL,
+        name="finish",
+    )(parts, middle, *states)
 
 
 def widen_kernel(x_ref, vectors_ref, gate_ref, up_ref, out_ref):
@@ -260,7 +289,7 @@
     w_both = jnp.concatenate([w_query.T, w_key.T], axis=0)
     parts, small = project(token_rows, vectors, small, w_both, w_value, w_ogate)
     arrived = exchanged(parts.reshape(n_kv, own_seqs, -1), "kv")
-    new_c, new_n, new_m, merged = cell(arrived, state_c, small)
+    states, merged = cell(arrived, state_c, small)
     merged_all = exchanged(merged, "kv").reshape(seqs, -1)
     attn_part = jnp.dot(merged_all, w_out, preferred_element_type=jnp.float32)
     attn_part = attn_part.astype(jnp.bfloat16).T.reshape(n_tp, feats, seqs)
@@ -276,9 +305,11 @@
     ).reshape(seqs, units)
     down_part = jnp.dot(hidden_all, w_down, preferred_element_type=jnp.float32)
     down_part = down_part.astype(jnp.bfloat16).T.reshape(n_tp, feats, seqs)
-    down_out = exchanged(down_part, "tp").astype(jnp.float32).sum(axis=0)
-    out_tokens = (middle_copies[0].astype(jnp.float32) + down_out).astype(jnp.bfloat16).T
-    return (out_tokens, new_c, new_n, new_m)
+    out_tokens, new_c, new_n, new_m = finish(
+        exchanged(down_part, "tp"), middle_copies, *states
+    )
+    new_n = new_n.reshape(own_seqs, 1, DK)
+    return (out_tokens.T, new_c.reshape(state_c.shape), new_n, new_m.T)
 
 
 def solution(mesh):

time: 178 us -> 177 us (level)
  no operation moved by 1% of the time
where the time goes in v4:
time: 177 us; the launch traced here: 176 us
  blocking collectives  118 us (67%)
  starting transfers between devices  44.9 us (25%)
  waiting for transfers between devices  5.68 us (3%)
  Pallas kernels  2.67 us (2%)
  between operations  2.15 us (1%)
    all_to_all x7, blocking collectives, exchanged(): return lax.all_to_all(blocks, axis, split_axis=0, concat_axis=0, tiled=True)  118 us
    all_to_all x1, starting transfers between devices, exchanged(): return lax.all_to_all(blocks, axis, split_axis=0, concat_axis=0, tiled=True)  44.9 us
    all_to_all x1, waiting for transfers between devices, exchanged(): return lax.all_to_all(blocks, axis, split_axis=0, concat_axis=0, tiled=True)  5.68 us
  transfers between devices with their start and end apart: 1, of which 1 were waited for; matrix products, arithmetic and copies ran while one was open for 0% of the time, Pallas kernels for 0%

profile of v4, /device:TPU:65, one launch (start us, length us, event | category | flops | bytes accessed | tf_op | source)
XLA Modules:
  0.0 176.3 jit_solution(15577967064884816930)
XLA Ops:
  0.6 0.0 copy-start
  0.6 0.0 copy-start.6
  0.7 0.7 copy-done.6
  1.4 0.6 spread.1
  2.0 0.0 copy-start.14
  2.0 0.0 copy-start.15
  2.0 0.0 copy-start.16
  2.0 0.0 copy-start.10
  2.0 0.0 copy-start.13
  2.0 0.0 copy-start.9
  2.1 44.9 %all-to-all-start = ((bf16[16,16,128]{2,1,0:T(8,128)(2,1)}), bf16[16,16,128]{2,1,0:T(8,128)(2,1)S(1)}, u32[]{:S(2)}, u32[]{:S(2)}) async-start(bf16[16,16,128]{2,1,0:T(8,128)(2,1)} %get-tuple-element.16), calls=%async_computation | async-start | bytes 131072 | tf_op jit(solution)/shard_map/all_to_all | solution.py:23
  46.9 0.0 copy-start.8
  48.2 0.0 copy-done.14
  48.3 0.0 copy-done.15
  48.3 0.0 copy-done.16
  48.3 0.1 fusion.12
  48.4 0.0 copy-done.10
  48.4 0.0 copy-done.13
  48.4 0.0 copy-start.12
  48.4 0.0 copy-start.11
  48.4 0.7 copy-done.12
  49.1 0.0 copy-done.11
  49.1 0.0 copy-done.9
  49.1 0.0 copy-done.8
  49.1 0.0 copy-start.4
  49.1 0.0 copy-start.5
  49.2 5.7 %all-to-all-done = bf16[16,16,128]{2,1,0:T(8,128)(2,1)S(1)} async-done(((bf16[16,16,128]{2,1,0:T(8,128)(2,1)}), bf16[16,16,128]{2,1,0:T(8,128)(2,1)S(1)}, u32[]{:S(2)}, u32[]{:S(2)}) %all-to-all-start) | async-done | bytes 65568 | tf_op jit(solution)/shard_map/all_to_all | solution.py:23
  54.9 0.0 copy-done.4
  54.9 0.0 copy-done.5
  54.9 0.0 copy-start.3
  54.9 0.3 project.1
  55.1 19.0 %all_to_all.40.parts_ref = bf16[16,8,512]{2,1,0:T(8,128)(2,1)S(1)} all-to-all(bf16[16,8,512]{2,1,0:T(8,128)(2,1)S(1)} %bitcast.46), channel_id=1, replica_groups=mesh['grp'=2,'kv'=16,'tp'=16] {'kv'}, dimensions={0} | all-to-all | bytes 262144 | tf_op jit(solution)/shard_map/all_to_all | solution.py:23
  74.1 0.0 copy-done.3
  74.1 0.0 copy-start.7
  74.1 0.6 cell.1
  74.7 0.0 copy-start.2
  74.7 17.9 %all_to_all.41 = bf16[16,8,128]{2,1,0:T(8,128)(2,1)S(1)} all-to-all(bf16[16,8,128]{2,1,0:T(8,128)(2,1)S(1)} %get-tuple-element.19), channel_id=1, replica_groups=mesh['grp'=2,'kv'=16,'tp'=16] {'kv'}, dimensions={0} | all-to-all | bytes 65536 | tf_op jit(solution)/shard_map/all_to_all | solution.py:23
  92.6 0.0 copy-done.7
  92.7 0.0 copy-start.1
  92.7 0.1 fusion
  92.8 0.1 copy.32
  92.9 12.3 %all_to_all.42.parts_ref = bf16[16,16,128]{2,1,0:T(8,128)(2,1)S(1)} all-to-all(bf16[16,16,128]{2,1,0:T(8,128)(2,1)S(1)} %bitcast.48), channel_id=1, replica_groups=mesh['grp'=2,'kv'=16,'tp'=16] {'tp'}, dimensions={0} | all-to-all | bytes 131072 | tf_op jit(solution)/shard_map/all_to_all | solution.py:23
  105.3 10.7 %all_to_all.43 = bf16[16,16,128]{2,1,0:T(8,128)(2,1)S(1)} all-to-all(bf16[16,16,128]{2,1,0:T(8,128)(2,1)S(1)} %residual.1.middle_ref), channel_id=1, replica_groups=mesh['grp'=2,'kv'=16,'tp'=16] {'tp'}, dimensions={0} | all-to-all | bytes 131072 | tf_op jit(solution)/shard_map/all_to_all | solution.py:23
  115.9 0.0 copy-done.2
  115.9 0.0 copy-done.1
  115.9 0.4 widen.1
  116.3 20.8 %all_to_all.44 = bf16[16,8,1408]{2,1,0:T(8,128)(2,1)S(1)} all-to-all(bf16[16,8,1408]{2,1,0:T(8,128)(2,1)S(1)} %bitcast.40), channel_id=1, replica_groups=mesh['grp'=2,'kv'=16,'tp'=16] {'kv'}, dimensions={0} | all-to-all | bytes 720896 | tf_op jit(solution)/shard_map/all_to_all | solution.py:23
  137.1 0.1 convert_reduce_fusion
  137.1 0.2 fusion.11
  137.3 0.1 fusion.5
  137.4 22.8 %all_to_all.45 = bf16[16,8,688]{2,1,0:T(8,128)(2,1)S(1)} all-to-all(bf16[16,8,688]{2,1,0:T(8,128)(2,1)S(1)} %broadcast_in_dim.15), channel_id=1, replica_groups=mesh['grp'=2,'kv'=16,'tp'=16] {'kv'}, dimensions={0} | all-to-all | bytes 352256 | tf_op jit(solution)/shard_map/all_to_all | solution.py:23
  160.2 0.0 copy-done
  160.2 0.2 fusion.1
  160.4 0.1 copy.33
  160.6 15.1 %all_to_all.46.parts_ref = bf16[16,16,128]{2,1,0:T(8,128)(2,1)S(1)} all-to-all(bf16[16,16,128]{2,1,0:T(8,128)(2,1)S(1)} %bitcast.49), channel_id=1, replica_groups=mesh['grp'=2,'kv'=16,'tp'=16] {'tp'}, dimensions={0} | all-to-all | bytes 131072 | tf_op jit(solution)/shard_map/all_to_all | solution.py:23
  175.6 0.7 finish.1
  (8 shorter events, 0.1 us)
Async XLA Ops:
  0.6 159.6 %copy-start = (bf16[688,256]{1,0:T(8,128)(2,1)S(1)}, bf16[688,256]{1,0:T(8,128)(2,1)}, u32[]{:S(2)}) copy-start(bf16[688,256]{1,0:T(8,128)(2,1)} %param.37) | copy-start | bytes 1056772
  0.6 0.7 copy-start.6
  2.0 46.2 %copy-start.14 = (bf16[1,128]{1,0:T(2,128)(2,1)S(1)}, bf16[1,128]{1,0:T(2,128)(2,1)}, u32[]{:S(2)}) copy-start(bf16[1,128]{1,0:T(2,128)(2,1)} %param.32) | copy-start | bytes 772
  2.0 46.2 %copy-start.15 = (bf16[256]{0:T(256)(128)(2,1)S(1)}, bf16[256]{0:T(256)(128)(2,1)}, u32[]{:S(2)}) copy-start(bf16[256]{0:T(256)(128)(2,1)} %param.20) | copy-start | bytes 1540
  2.0 46.3 %copy-start.16 = (bf16[256]{0:T(256)(128)(2,1)S(1)}, bf16[256]{0:T(256)(128)(2,1)}, u32[]{:S(2)}) copy-start(bf16[256]{0:T(256)(128)(2,1)} %param.34) | copy-start | bytes 1540
  2.0 46.4 %copy-start.10 = (f32[8,1,64]{2,1,0:T(1,128)S(1)}, f32[8,1,64]{2,1,0:T(1,128)}, u32[]{:S(2)}) copy-start(f32[8,1,64]{2,1,0:T(1,128)} %param.30) | copy-start | bytes 6148
  2.0 46.4 %copy-start.13 = (f32[8,1]{0,1:T(1,128)S(1)}, f32[8,1]{0,1:T(1,128)}, u32[]{:S(2)}) copy-start(f32[8,1]{0,1:T(1,128)} %param.31) | copy-start | bytes 100
  2.0 47.1 %copy-start.9 = (bf16[256,64]{0,1:T(8,128)(2,1)S(1)}, bf16[256,64]{0,1:T(8,128)(2,1)}, u32[]{:S(2)}) copy-start(bf16[256,64]{0,1:T(8,128)(2,1)} %param.21) | copy-start | bytes 98308
  2.1 52.8 %all-to-all-start = ((bf16[16,16,128]{2,1,0:T(8,128)(2,1)}), bf16[16,16,128]{2,1,0:T(8,128)(2,1)S(1)}, u32[]{:S(2)}, u32[]{:S(2)}) async-start(bf16[16,16,128]{2,1,0:T(8,128)(2,1)} %get-tuple-element.16), calls=%async_computation | async-start | bytes 131072 | tf_op jit(solution)/shard_map/all_to_all | solution.py:23
  46.9 2.2 %copy-start.8 = (bf16[256,64]{0,1:T(8,128)(2,1)S(1)}, bf16[256,64]{0,1:T(8,128)(2,1)}, u32[]{:S(2)}) copy-start(bf16[256,64]{0,1:T(8,128)(2,1)} %param.22) | copy-start | bytes 98308
  48.4 0.7 copy-start.12
  48.4 0.7 copy-start.11
  49.1 5.7 %copy-start.4 = (bf16[256,128]{1,0:T(8,128)(2,1)S(1)}, bf16[256,128]{1,0:T(8,128)(2,1)}, u32[]{:S(2)}) copy-start(bf16[256,128]{1,0:T(8,128)(2,1)} %value_ref.1) | copy-start | bytes 196612
  49.1 5.7 %copy-start.5 = (bf16[256,128]{1,0:T(8,128)(2,1)S(1)}, bf16[256,128]{1,0:T(8,128)(2,1)}, u32[]{:S(2)}) copy-start(bf16[256,128]{1,0:T(8,128)(2,1)} %ogate_ref.1) | copy-start | bytes 196612
  54.9 19.3 %copy-start.3 = (f32[8,1,64,128]{3,2,1,0:T(8,128)S(1)}, f32[8,1,64,128]{3,2,1,0:T(8,128)}, u32[]{:S(2)}) copy-start(f32[8,1,64,128]{3,2,1,0:T(8,128)} %param.29) | copy-start | bytes 786436
  74.1 18.5 %copy-start.7 = (bf16[128,256]{1,0:T(8,128)(2,1)S(1)}, bf16[128,256]{1,0:T(8,128)(2,1)}, u32[]{:S(2)}) copy-start(bf16[128,256]{1,0:T(8,128)(2,1)} %param.33) | copy-start | bytes 196612
  74.7 41.2 %copy-start.2 = (bf16[256,688]{0,1:T(8,128)(2,1)S(1)}, bf16[256,688]{0,1:T(8,128)(2,1)}, u32[]{:S(2)}) copy-start(bf16[256,688]{0,1:T(8,128)(2,1)} %param.36) | copy-start | bytes 1056772
  92.7 23.3 %copy-start.1 = (bf16[256,688]{0,1:T(8,128)(2,1)S(1)}, bf16[256,688]{0,1:T(8,128)(2,1)}, u32[]{:S(2)}) copy-start(bf16[256,688]{0,1:T(8,128)(2,1)} %param.35) | copy-start | bytes 1056772

commit v5 on v4

--- a/solution.py
+++ b/solution.py
@@ -1,3 +1,5 @@
+import functools
+
 import jax
 import jax.numpy as jnp
 from jax import lax
@@ -19,8 +21,10 @@
 SMALL = pltpu.CompilerParams(vmem_limit_bytes=8 * 2**20)
 
 
-def exchanged(blocks, axis):
-    return lax.all_to_all(blocks, axis, split_axis=0, concat_axis=0, tiled=True)
+def exchanged(blocks, axis, groups=None):
+    return lax.all_to_all(
+        blocks, axis, split_axis=0, concat_axis=0, tiled=True, axis_index_groups=groups
+    )
 
 
 def spread_kernel(value_ref, out_ref, own_ref):
@@ -157,21 +161,34 @@
     return (new_c, new_n, new_m), out
 
 
-def residual_kernel(parts_ref, tokens_ref, out_ref):
+def residual_kernel(parts_ref, tokens_ref, own_ref, out_ref):
     total = parts_ref[0].astype(jnp.float32)
     for k in range(1, parts_ref.shape[0]):
         total += parts_ref[k].astype(jnp.float32)
-    middle = (tokens_ref[...].astype(jnp.float32) + total).astype(out_ref.dtype)
-    for copy in range(out_ref.shape[0]):
-        out_ref[copy] = middle
+    middle = (tokens_ref[...].astype(jnp.float32) + total).astype(own_ref.dtype)
+    own_ref[...] = middle
+    middle = middle.astype(jnp.float32)
+    feats, seqs = middle.shape
+    copies = out_ref.shape[0] // 2
+    for half in range(2):
+        at = half * (seqs // 2)
+        picked = middle[:, at : at + seqs // 2]
+        packed = jnp.concatenate([picked[: feats // 2], picked[feats // 2 :]], axis=1)
+        packed = packed.astype(out_ref.dtype)
+        for copy in range(copies):
+            out_ref[half * copies + copy] = packed
 
 
 def residual(parts, tokens):
+    count, feats, seqs = parts.shape
     return pl.pallas_call(
         residual_kernel,
-        out_shape=jax.ShapeDtypeStruct(parts.shape, parts.dtype),
+        out_shape=(
+            jax.ShapeDtypeStruct((feats, seqs), parts.dtype),
+            jax.ShapeDtypeStruct((2 * count, feats // 2, seqs), parts.dtype),
+        ),
         in_specs=[VMEM, VMEM],
-        out_specs=VMEM,
+        out_specs=(VMEM, VMEM),
         compiler_params=SMALL,
         name="residual",
     )(parts, tokens)
@@ -190,7 +207,7 @@
     total = parts_ref[0].astype(jnp.float32)
     for k in range(1, parts_ref.shape[0]):
         total += parts_ref[k].astype(jnp.float32)
-    tokens[...] = (middle_ref[0].astype(jnp.float32) + total).astype(tokens.dtype)
+    tokens[...] = (middle_ref[...].astype(jnp.float32) + total).astype(tokens.dtype)
     copies.append(pltpu.make_async_copy(tokens, out_ref, sems.at[count]))
     copies[count].start()
     for copy in copies:
@@ -215,37 +232,44 @@
     )(parts, middle, *states)
 
 
-def widen_kernel(x_ref, vectors_ref, gate_ref, up_ref, out_ref):
-    units = gate_ref.shape[0]
+def widen_kernel(units, x_ref, vectors_ref, own_ref, other_ref, out_ref):
+    blocks = x_ref.shape[0] // 2
+    half = x_ref.shape[2] // 2
     cols = out_ref.shape[1]
-    start = units // LANES * LANES
-    taken = (LANES - (units - start)) % LANES
-    x = x_ref[...].astype(jnp.float32).T
-    normed = (x * vectors_ref[3:4, :]).astype(jnp.bfloat16)
-    out_ref[:, :start] = transposed_product(normed, gate_ref[:start, :]).astype(out_ref.dtype)
-    if taken:
-        mixed = jnp.concatenate([gate_ref[start:, :], up_ref[:taken, :]], axis=0)
-        out_ref[:, start : start + LANES] = transposed_product(normed, mixed).astype(
-            out_ref.dtype
-        )
-        start += LANES
-    filler = jnp.zeros((cols - 2 * units, gate_ref.shape[1]), gate_ref.dtype)
-    rest = transposed_product(normed, jnp.concatenate([up_ref[taken:, :], filler], axis=0))
+    place = lax.rem(lax.axis_index("kv"), 2)
+
+    def features(which):
+        packed = x_ref[pl.ds(which * blocks, blocks)].astype(jnp.float32)
+        both = jnp.concatenate([packed[:, :, :half], packed[:, :, half:]], axis=1)
+        return both.reshape(-1, half).T
+
+    last = cols - LANES
+    own, other = features(place), features(1 - place)
+    squares = jnp.sum(own * own, axis=1, keepdims=True) + jnp.sum(
+        other * other, axis=1, keepdims=True
+    )
+    own = (own * vectors_ref[3:4, :]).astype(jnp.bfloat16)
+    gain = other_ref[units : units + 1, :].astype(jnp.float32)
+    other = (other * gain).astype(jnp.bfloat16)
+    out_ref[:, :last] = (
+        transposed_product(own, own_ref[:last, :]) + transposed_product(other, other_ref[:last, :])
+    ).astype(out_ref.dtype)
+    rest = transposed_product(own, own_ref[last:, :]) + transposed_product(
+        other, other_ref[last:, :]
+    )
     lane = lax.broadcasted_iota(jnp.int32, rest.shape, 1)
-    squares = jnp.sum(x * x, axis=1, keepdims=True)
-    out_ref[:, start:] = jnp.where(lane == 2 * units - start, squares, rest).astype(out_ref.dtype)
-
-
-def widen(x, vectors, w_gate, w_up):
-    cols = (2 * w_gate.shape[1] // LANES + 1) * LANES
-    return pl.pallas_call(
-        widen_kernel,
-        out_shape=jax.ShapeDtypeStruct((x.shape[1], cols), jnp.bfloat16),
+    out_ref[:, last:] = jnp.where(lane == units - last, squares, rest).astype(out_ref.dtype)
+
+
+def widen(x, vectors, own, other, units):
+    return pl.pallas_call(
+        functools.partial(widen_kernel, units),
+        out_shape=jax.ShapeDtypeStruct((x.shape[2] // 2, own.shape[0]), jnp.bfloat16),
         in_specs=[VMEM] * 4,
         out_specs=VMEM,
         compiler_params=SMALL,
         name="widen",
-    )(x, vectors, w_gate.T, w_up.T)
+    )(x, vectors, own, other)
 
 
 def body(
@@ -284,29 +308,40 @@
     small = jnp.concatenate(
         [jnp.pad(one, ((0, 0), (0, LANES - one.shape[1]))) for one in narrow], axis=0
     )
+    shared = [w_gate.T, w_up.T, ffn_gain[None]]
+    cols = (2 * units // LANES + 1) * LANES
+    shared.append(jnp.zeros((cols - 2 * units - 1, rows), jnp.bfloat16))
+    own_weights = jnp.concatenate(shared, axis=0)
     token_copies, own_tokens = spread(tokens.T, n_tp)
     token_rows = exchanged(token_copies, "tp").reshape(rows, seqs)
+    token_rows, own_weights = lax.optimization_barrier((token_rows, own_weights))
     w_both = jnp.concatenate([w_query.T, w_key.T], axis=0)
     parts, small = project(token_rows, vectors, small, w_both, w_value, w_ogate)
     arrived = exchanged(parts.reshape(n_kv, own_seqs, -1), "kv")
     states, merged = cell(arrived, state_c, small)
     merged_all = exchanged(merged, "kv").reshape(seqs, -1)
+    merged_all, own_weights = lax.optimization_barrier((merged_all, own_weights))
+    swap = [(k, k + 1 - 2 * (k % 2)) for k in range(n_kv)]
+    other_weights = lax.ppermute(own_weights, "kv", swap)
     attn_part = jnp.dot(merged_all, w_out, preferred_element_type=jnp.float32)
     attn_part = attn_part.astype(jnp.bfloat16).T.reshape(n_tp, feats, seqs)
-    middle_copies = residual(exchanged(attn_part, "tp"), own_tokens)
-    middle_rows = exchanged(middle_copies, "tp").reshape(rows, seqs)
-    spread_out = widen(middle_rows, vectors, w_gate, w_up)
-    sums = exchanged(spread_out.reshape(n_kv, own_seqs, -1), "kv").astype(jnp.float32).sum(axis=0)
+    own_middle, middle_copies = residual(exchanged(attn_part, "tp"), own_tokens)
+    pairs = [[k * n_tp + t for t in range(2 * n_tp)] for k in range(0, n_kv, 2)]
+    middle_rows = exchanged(middle_copies, ("kv", "tp"), pairs)
+    partial = widen(middle_rows, vectors, own_weights, other_weights, 2 * units)
+    halves = [list(range(place, n_kv, 2)) for place in range(2)]
+    arrived = exchanged(partial.reshape(n_kv // 2, own_seqs, -1), "kv", halves)
+    sums = arrived.astype(jnp.float32).sum(axis=0)
     gate_sum, up_sum, total = sums[:, :units], sums[:, units : 2 * units], sums[:, 2 * units]
     ffn_scale = lax.rsqrt(total / D + norm_eps)[:, None]
     hidden = (jax.nn.silu(ffn_scale * gate_sum) * (ffn_scale * up_sum)).astype(jnp.bfloat16)
     hidden_all = exchanged(
-        jnp.broadcast_to(hidden[None], (n_kv, *hidden.shape)), "kv"
+        jnp.broadcast_to(hidden[None], (n_kv, *hidden.shape)), "kv", [halves[0] + halves[1]]
     ).reshape(seqs, units)
     down_part = jnp.dot(hidden_all, w_down, preferred_element_type=jnp.float32)
     down_part = down_part.astype(jnp.bfloat16).T.reshape(n_tp, feats, seqs)
     out_tokens, new_c, new_n, new_m = finish(
-        exchanged(down_part, "tp"), middle_copies, *states
+        exchanged(down_part, "tp"), own_middle, *states
     )
     new_n = new_n.reshape(own_seqs, 1, DK)
     return (out_tokens.T, new_c.reshape(state_c.shape), new_n, new_m.T)

time: 177 us -> 177 us (level)
  local copies, waits for them, and re-layouts: 1.73 us -> 8.33 us
  waiting for transfers between devices: 5.68 us -> 0.01 us
  blocking collectives: 118 us -> 115 us
  starting transfers between devices: 44.9 us -> 47.2 us
    all_to_all x1, waiting for transfers between devices: 5.68 us -> 0.01 us  [exchanged(): lax.all_to_all(blocks, axis, split_axis=0, concat_axis=0, tiled=True, axi...]
    concatenate x0 -> x1, local copies, waits for them, and re-layouts: none -> 3.85 us  [body(): own_weights = jnp.concatenate(shared, axis=0)]
    all_to_all x7, blocking collectives: 118 us -> 115 us  [exchanged(): lax.all_to_all(blocks, axis, split_axis=0, concat_axis=0, tiled=True, axi...]
    unnamed x34 -> x30, local copies, waits for them, and re-layouts: 1.48 us -> 4.22 us
    ppermute x0 -> x1, starting transfers between devices: none -> 2.42 us  [body(): other_weights = lax.ppermute(own_weights, 'kv', swap)]
  transfers between devices with their start and end apart: 1 -> 2, of which waited for: 1 -> 0; matrix products, arithmetic and copies ran while one was open for 0% -> 2% of each run, Pallas kernels for 0% -> 0%
where the time goes in v5:
time: 177 us; the launch traced here: 176 us
  blocking collectives  115 us (65%)
  starting transfers between devices  47.2 us (27%)
  local copies, waits for them, and re-layouts  8.33 us (5%)
  Pallas kernels  3.03 us (2%)
  between operations  2.18 us (1%)
    all_to_all x7, blocking collectives, exchanged(): lax.all_to_all(blocks, axis, split_axis=0, concat_axis=0, tiled=True, axi...  115 us
    all_to_all x1, starting transfers between devices, exchanged(): lax.all_to_all(blocks, axis, split_axis=0, concat_axis=0, tiled=True, axi...  44.7 us
    unnamed x30, local copies, waits for them, and re-layouts  4.22 us
    concatenate x1, local copies, waits for them, and re-layouts, body(): own_weights = jnp.concatenate(shared, axis=0)  3.85 us
  transfers between devices with their start and end apart: 2, of which 0 were waited for; matrix products, arithmetic and copies ran while one was open for 2% of the time, Pallas kernels for 0%

profile of v5, /device:TPU:65, one launch (start us, length us, event | category | flops | bytes accessed | tf_op | source)
XLA Modules:
  0.0 176.4 jit_solution(2480341831691137031)
XLA Ops:
  0.6 0.0 copy-start
  0.6 0.0 copy-start.4
  0.7 0.7 copy-done.4
  1.4 0.6 spread.1
  2.0 44.7 %all-to-all-start = ((bf16[16,16,128]{2,1,0:T(8,128)(2,1)}), bf16[16,16,128]{2,1,0:T(8,128)(2,1)S(1)}, u32[]{:S(2)}, u32[]{:S(2)}) async-start(bf16[16,16,128]{2,1,0:T(8,128)(2,1)} %get-tuple-element.22), calls=%async_computation | async-start | bytes 131072 | tf_op jit(solution)/shard_map/all_to_all | solution.py:25
  47.4 0.0 copy-start.12
  48.1 0.0 copy-done.12
  48.1 0.0 copy-start.13
  48.1 0.6 copy-done.13
  48.7 0.0 copy-start.14
  48.8 0.6 copy-done.14
  49.4 0.0 copy-start.8
  49.4 0.1 fusion.11
  49.5 0.0 copy-start.11
  49.5 0.6 copy-done.8
  50.1 0.0 copy-done.11
  50.2 0.0 copy-start.10
  50.2 0.0 copy-start.9
  50.2 0.7 copy-done.10
  50.8 0.0 copy-done.9
  50.9 0.0 copy-start.6
  50.9 0.0 copy-start.7
  50.9 3.8 %concatenate.12.own_ref = bf16[1408,256]{1,0:T(8,128)(2,1)S(1)} concatenate(bf16[688,256]{1,0:T(8,128)(2,1)} %bitcast.43, bf16[688,256]{1,0:T(8,128)(2,1)} %bitcast.44, bf16[1,256]{1,0:T(2,128)(2,1)S(1)} %broadcast_in_dim.8, bf16[31,256]{1,0:T(8,128)(2,1)S(1)} %broadcast_in_dim.18), dimensions={0} | concatenate | bytes 1441792 | tf_op jit(solution)/shard_map/concatenate | solution.py:314
  54.8 0.0 copy-done.6
  54.8 0.0 copy-done.7
  54.8 0.0 copy-start.2
  54.8 0.0 copy-start.3
  54.8 0.0 all-to-all-done
  54.8 0.8 copy-done.2
  55.6 0.0 copy-done.3
  55.7 0.0 copy-start.1
  55.7 0.3 project.1
  55.9 19.1 %all_to_all.40.parts_ref = bf16[16,8,512]{2,1,0:T(8,128)(2,1)S(1)} all-to-all(bf16[16,8,512]{2,1,0:T(8,128)(2,1)S(1)} %bitcast.41), channel_id=1, replica_groups=mesh['grp'=2,'kv'=16,'tp'=16] {'kv'}, dimensions={0} | all-to-all | bytes 262144 | tf_op jit(solution)/shard_map/all_to_all | solution.py:25
  75.1 0.0 copy-done.1
  75.1 0.6 cell.1
  75.7 0.0 copy-start.5
  75.7 17.9 %all_to_all.41 = bf16[16,8,128]{2,1,0:T(8,128)(2,1)S(1)} all-to-all(bf16[16,8,128]{2,1,0:T(8,128)(2,1)S(1)} %get-tuple-element.26), channel_id=1, replica_groups=mesh['grp'=2,'kv'=16,'tp'=16] {'kv'}, dimensions={0} | all-to-all | bytes 65536 | tf_op jit(solution)/shard_map/all_to_all | solution.py:25
  93.6 2.4 %collective-permute-start = (bf16[1408,256]{1,0:T(8,128)(2,1)S(1)}, bf16[1408,256]{1,0:T(8,128)(2,1)S(1)}, u32[]{:S(2)}, u32[]{:S(2)}) collective-permute-start(bf16[1408,256]{1,0:T(8,128)(2,1)S(1)} %concatenate.12.own_ref), channel_id=1, source_target_pairs={{0,16},{16,0},{32,48},{48,32},{64,80},{80,64},{96,112},{112,96},{1... | collective-permute-start | bytes 2162696 | tf_op jit(solution)/shard_map/ppermute | solution.py:325
  96.0 0.0 copy-done.5
  96.0 0.1 fusion
  96.2 0.1 copy.32
  96.3 16.7 %all_to_all.42.parts_ref = bf16[16,16,128]{2,1,0:T(8,128)(2,1)S(1)} all-to-all(bf16[16,16,128]{2,1,0:T(8,128)(2,1)S(1)} %bitcast.45), channel_id=1, replica_groups=mesh['grp'=2,'kv'=16,'tp'=16] {'tp'}, dimensions={0} | all-to-all | bytes 131072 | tf_op jit(solution)/shard_map/all_to_all | solution.py:25
  113.0 0.1 residual.1
  113.1 11.2 %all_to_all.43.x_ref = bf16[32,8,128]{2,1,0:T(8,128)(2,1)S(1)} all-to-all(bf16[32,8,128]{2,1,0:T(8,128)(2,1)S(1)} %get-tuple-element.30), channel_id=1, replica_groups={{0,1,2,3,4,5,6,7,8,9,10,11,12,13,14,15,16,17,18,19,20,21,22,23,24,25,26..., dimensions={0} | all-to-all | bytes 131072 | tf_op jit(solution)/shard_map/all_to_all | solution.py:25
  124.3 0.0 collective-permute-done.other_ref
  124.3 0.7 widen.1
  124.9 17.3 %all_to_all.44 = bf16[8,8,1408]{2,1,0:T(8,128)(2,1)S(1)} all-to-all(bf16[8,8,1408]{2,1,0:T(8,128)(2,1)S(1)} %bitcast.38), channel_id=1, replica_groups={{0,32,64,96,128,160,192,224},{16,48,80,112,144,176,208,240},{1,33,65,97..., dimensions={0} | all-to-all | bytes 360448 | tf_op jit(solution)/shard_map/all_to_all | solution.py:25
  142.3 0.2 fusion.10
  142.5 0.1 fusion.4
  142.6 18.2 %all_to_all.45 = bf16[16,8,688]{2,1,0:T(8,128)(2,1)S(1)} all-to-all(bf16[16,8,688]{2,1,0:T(8,128)(2,1)S(1)} %broadcast_in_dim.20), channel_id=1, replica_groups={{0,32,64,96,128,160,192,224,16,48,80,112,144,176,208,240},{1,33,65,97,1..., dimensions={0} | all-to-all | bytes 352256 | tf_op jit(solution)/shard_map/all_to_all | solution.py:25
  160.8 0.0 copy-done
  160.8 0.2 fusion.1
  161.1 0.1 copy.33
  161.2 14.5 %all_to_all.46.parts_ref = bf16[16,16,128]{2,1,0:T(8,128)(2,1)S(1)} all-to-all(bf16[16,16,128]{2,1,0:T(8,128)(2,1)S(1)} %bitcast.46), channel_id=1, replica_groups=mesh['grp'=2,'kv'=16,'tp'=16] {'tp'}, dimensions={0} | all-to-all | bytes 131072 | tf_op jit(solution)/shard_map/all_to_all | solution.py:25
  175.7 0.7 finish.1
  (9 shorter events, 0.1 us)
Async XLA Ops:
  0.6 160.2 %copy-start = (bf16[688,256]{1,0:T(8,128)(2,1)S(1)}, bf16[688,256]{1,0:T(8,128)(2,1)}, u32[]{:S(2)}) copy-start(bf16[688,256]{1,0:T(8,128)(2,1)} %param.37) | copy-start | bytes 1056772
  0.6 0.7 copy-start.4
  2.0 52.8 %all-to-all-start = ((bf16[16,16,128]{2,1,0:T(8,128)(2,1)}), bf16[16,16,128]{2,1,0:T(8,128)(2,1)S(1)}, u32[]{:S(2)}, u32[]{:S(2)}) async-start(bf16[16,16,128]{2,1,0:T(8,128)(2,1)} %get-tuple-element.22), calls=%async_computation | async-start | bytes 131072 | tf_op jit(solution)/shard_map/all_to_all | solution.py:25
  47.4 0.7 copy-start.12
  48.1 0.7 copy-start.13
  48.7 0.7 copy-start.14
  49.4 0.7 copy-start.8
  49.5 0.7 copy-start.11
  50.2 0.7 copy-start.10
  50.2 0.7 copy-start.9
  50.9 3.9 %copy-start.6 = (bf16[256,64]{0,1:T(8,128)(2,1)S(1)}, bf16[256,64]{0,1:T(8,128)(2,1)}, u32[]{:S(2)}) copy-start(bf16[256,64]{0,1:T(8,128)(2,1)} %param.22) | copy-start | bytes 98308
  50.9 3.9 %copy-start.7 = (bf16[256,64]{0,1:T(8,128)(2,1)S(1)}, bf16[256,64]{0,1:T(8,128)(2,1)}, u32[]{:S(2)}) copy-start(bf16[256,64]{0,1:T(8,128)(2,1)} %param.21) | copy-start | bytes 98308
  54.8 0.8 copy-start.2
  54.8 0.9 copy-start.3
  55.7 19.4 %copy-start.1 = (f32[8,1,64,128]{3,2,1,0:T(8,128)S(1)}, f32[8,1,64,128]{3,2,1,0:T(8,128)}, u32[]{:S(2)}) copy-start(f32[8,1,64,128]{3,2,1,0:T(8,128)} %param.29) | copy-start | bytes 786436
  75.7 20.3 %copy-start.5 = (bf16[128,256]{1,0:T(8,128)(2,1)S(1)}, bf16[128,256]{1,0:T(8,128)(2,1)}, u32[]{:S(2)}) copy-start(bf16[128,256]{1,0:T(8,128)(2,1)} %param.33) | copy-start | bytes 196612
  93.6 30.7 %collective-permute-start = (bf16[1408,256]{1,0:T(8,128)(2,1)S(1)}, bf16[1408,256]{1,0:T(8,128)(2,1)S(1)}, u32[]{:S(2)}, u32[]{:S(2)}) collective-permute-start(bf16[1408,256]{1,0:T(8,128)(2,1)S(1)} %concatenate.12.own_ref), channel_id=1, source_target_pairs={{0,16},{16,0},{32,48},{48,32},{64,80},{80,64},{96,112},{112,96},{1... | collective-permute-start | bytes 2162696 | tf_op jit(solution)/shard_map/ppermute | solution.py:325

commit v6 on v5

--- a/solution.py
+++ b/solution.py
@@ -75,6 +75,9 @@
     tail = jnp.where(
         lane == 0, igate, jnp.where(lane == 1, fgate, jnp.where(lane == 2, squares, 0.0))
     )
+    own = (small_ref.shape[0] - 3) // 2
+    gain_tile = small_ref[own : 2 * own, :]
+    tail += jnp.concatenate([gain_tile] * (x.shape[0] // own), axis=0)
     out_ref[:, 3 * LANES :] = tail.astype(out_ref.dtype)
 
 
@@ -94,7 +97,7 @@
 
 def cell_kernel(
     parts_ref, c_ref, small_ref,
-    new_c_ref, new_n_ref, new_m_ref, out_ref,
+    new_c_ref, new_n_ref, new_m_ref, other_ref, out_ref,
 ):
     total = parts_ref[0].astype(jnp.float32)
     for k in range(1, parts_ref.shape[0]):
@@ -102,12 +105,12 @@
     seqs = total.shape[0]
     tail = total[:, 3 * LANES :]
     row_scale = lax.rsqrt(tail[:, 2:3] / D + norm_eps)
-    igate = igate_cap * jnp.tanh((row_scale * tail[:, 0:1] + small_ref[seqs + 2 : seqs + 3, 0:1]) / igate_cap)
-    fgate = row_scale * tail[:, 1:2] + small_ref[seqs + 2 : seqs + 3, 1:2]
+    igate = igate_cap * jnp.tanh((row_scale * tail[:, 0:1] + small_ref[2 * seqs + 2 : 2 * seqs + 3, 0:1]) / igate_cap)
+    fgate = row_scale * tail[:, 1:2] + small_ref[2 * seqs + 2 : 2 * seqs + 3, 1:2]
     diagonal = lax.broadcasted_iota(jnp.int32, (seqs, seqs), 0) == lax.broadcasted_iota(
         jnp.int32, (seqs, seqs), 1
     )
-    state_m = jnp.sum(jnp.where(diagonal, small_ref[seqs : seqs + 1, :seqs], 0.0), axis=1, keepdims=True)
+    state_m = jnp.sum(jnp.where(diagonal, small_ref[2 * seqs : 2 * seqs + 1, :seqs], 0.0), axis=1, keepdims=True)
     log_keep = jnp.minimum(fgate, 0.0) - jnp.log1p(jnp.exp(-jnp.abs(fgate)))
     carried = log_keep + state_m
     new_m = jnp.maximum(carried, igate)
@@ -134,31 +137,39 @@
         new_c = keep[b : b + 1, :] * c_ref[b] + key_b * value_vec[b : b + 1, :]
         new_c_ref[b] = new_c
         rows.append(jnp.sum(query_b * new_c, axis=0, keepdims=True))
+    me = lax.axis_index("kv")
+    theirs = parts_ref[pl.ds(me + 1 - 2 * lax.rem(me, 2), 1)][0]
+    theirs = theirs[:, 3 * LANES :].astype(jnp.float32)
+    start, share = LANES // 2, other_ref.shape[1] // seqs
+    other_ref[...] = jnp.concatenate(
+        [theirs[b : b + 1, start : start + share] for b in range(seqs)], axis=1
+    )
     head_out = jnp.concatenate(rows, axis=0) / denominator
-    merged = head_out * small_ref[seqs + 1 : seqs + 2, :] / (1.0 + jnp.exp(-ogate))
+    merged = head_out * small_ref[2 * seqs + 1 : 2 * seqs + 2, :] / (1.0 + jnp.exp(-ogate))
     merged = merged.astype(out_ref.dtype)
     for copy in range(out_ref.shape[0]):
         out_ref[copy] = merged
 
 
-def cell(parts, state_c, small):
+def cell(parts, state_c, small, width):
     count, seqs, _ = parts.shape
-    new_c, new_n, new_m, out = pl.pallas_call(
+    *states, other, out = pl.pallas_call(
         cell_kernel,
         out_shape=(
             jax.ShapeDtypeStruct((seqs, DK, DV), jnp.float32),
             jax.ShapeDtypeStruct((seqs, DK), jnp.float32),
             jax.ShapeDtypeStruct((1, seqs), jnp.float32),
+            jax.ShapeDtypeStruct((1, width), jnp.float32),
             jax.ShapeDtypeStruct((count, seqs, DV), jnp.bfloat16),
         ),
         in_specs=[VMEM] * 3,
-        out_specs=(VMEM,) * 4,
+        out_specs=(VMEM,) * 5,
         compiler_params=SMALL,
         name="cell",
     )(
         parts, state_c.reshape(seqs, DK, DV), small,
     )
-    return (new_c, new_n, new_m), out
+    return states, other, out
 
 
 def residual_kernel(parts_ref, tokens_ref, own_ref, out_ref):
@@ -232,10 +243,15 @@
     )(parts, middle, *states)
 
 
-def widen_kernel(units, x_ref, vectors_ref, own_ref, other_ref, out_ref):
+def widen_kernel(
+    x_ref, vectors_ref, gain_ref, gate_ref, up_ref, other_gate_ref, other_up_ref, out_ref
+):
     blocks = x_ref.shape[0] // 2
     half = x_ref.shape[2] // 2
+    units = gate_ref.shape[0]
     cols = out_ref.shape[1]
+    start = units // LANES * LANES
+    taken = (LANES - (units - start)) % LANES
     place = lax.rem(lax.axis_index("kv"), 2)
 
     def features(which):
@@ -243,33 +259,41 @@
         both = jnp.concatenate([packed[:, :, :half], packed[:, :, half:]], axis=1)
         return both.reshape(-1, half).T
 
-    last = cols - LANES
     own, other = features(place), features(1 - place)
     squares = jnp.sum(own * own, axis=1, keepdims=True) + jnp.sum(
         other * other, axis=1, keepdims=True
     )
     own = (own * vectors_ref[3:4, :]).astype(jnp.bfloat16)
-    gain = other_ref[units : units + 1, :].astype(jnp.float32)
-    other = (other * gain).astype(jnp.bfloat16)
-    out_ref[:, :last] = (
-        transposed_product(own, own_ref[:last, :]) + transposed_product(other, other_ref[:last, :])
-    ).astype(out_ref.dtype)
-    rest = transposed_product(own, own_ref[last:, :]) + transposed_product(
-        other, other_ref[last:, :]
-    )
+    other = (other * gain_ref[...]).astype(jnp.bfloat16)
+
+    def product(pick):
+        return transposed_product(own, pick(gate_ref, up_ref)) + transposed_product(
+            other, pick(other_gate_ref, other_up_ref)
+        )
+
+    out_ref[:, :start] = product(lambda gate, up: gate[:start, :]).astype(out_ref.dtype)
+    if taken:
+        mixed = product(
+            lambda gate, up: jnp.concatenate([gate[start:, :], up[:taken, :]], axis=0)
+        )
+        out_ref[:, start : start + LANES] = mixed.astype(out_ref.dtype)
+        start += LANES
+    filler = jnp.zeros((cols - 2 * units, gate_ref.shape[1]), gate_ref.dtype)
+    rest = product(lambda gate, up: jnp.concatenate([up[taken:, :], filler], axis=0))
     lane = lax.broadcasted_iota(jnp.int32, rest.shape, 1)
-    out_ref[:, last:] = jnp.where(lane == units - last, squares, rest).astype(out_ref.dtype)
-
-
-def widen(x, vectors, own, other, units):
+    out_ref[:, start:] = jnp.where(lane == 2 * units - start, squares, rest).astype(out_ref.dtype)
+
+
+def widen(x, vectors, other_gain, *weights):
+    cols = (2 * weights[0].shape[0] // LANES + 1) * LANES
     return pl.pallas_call(
-        functools.partial(widen_kernel, units),
-        out_shape=jax.ShapeDtypeStruct((x.shape[2] // 2, own.shape[0]), jnp.bfloat16),
-        in_specs=[VMEM] * 4,
+        widen_kernel,
+        out_shape=jax.ShapeDtypeStruct((x.shape[2] // 2, cols), jnp.bfloat16),
+        in_specs=[VMEM] * 7,
         out_specs=VMEM,
         compiler_params=SMALL,
         name="widen",
-    )(x, vectors, own, other)
+    )(x, vectors, other_gain, *weights)
 
 
 def body(
@@ -305,30 +329,31 @@
         state_n.reshape(own_seqs, DK), state_m.T, head_gain.astype(jnp.float32),
         jnp.stack([igate_bias, fgate_bias], axis=1),
     ]
-    small = jnp.concatenate(
-        [jnp.pad(one, ((0, 0), (0, LANES - one.shape[1]))) for one in narrow], axis=0
-    )
-    shared = [w_gate.T, w_up.T, ffn_gain[None]]
-    cols = (2 * units // LANES + 1) * LANES
-    shared.append(jnp.zeros((cols - 2 * units - 1, rows), jnp.bfloat16))
-    own_weights = jnp.concatenate(shared, axis=0)
+    narrow = [jnp.pad(one, ((0, 0), (0, LANES - one.shape[1]))) for one in narrow]
+    share = rows // own_seqs
+    gain_tile = jnp.pad(
+        ffn_gain.astype(jnp.float32).reshape(own_seqs, share),
+        ((0, 0), (LANES // 2, LANES // 2 - share)),
+    )
+    small = jnp.concatenate([narrow[0], gain_tile, *narrow[1:]], axis=0)
     token_copies, own_tokens = spread(tokens.T, n_tp)
     token_rows = exchanged(token_copies, "tp").reshape(rows, seqs)
-    token_rows, own_weights = lax.optimization_barrier((token_rows, own_weights))
     w_both = jnp.concatenate([w_query.T, w_key.T], axis=0)
     parts, small = project(token_rows, vectors, small, w_both, w_value, w_ogate)
     arrived = exchanged(parts.reshape(n_kv, own_seqs, -1), "kv")
-    states, merged = cell(arrived, state_c, small)
+    states, other_gain, merged = cell(arrived, state_c, small, rows)
     merged_all = exchanged(merged, "kv").reshape(seqs, -1)
-    merged_all, own_weights = lax.optimization_barrier((merged_all, own_weights))
+    gate, up = w_gate.T, w_up.T
+    merged_all, sent_gate, sent_up = lax.optimization_barrier((merged_all, gate, up))
     swap = [(k, k + 1 - 2 * (k % 2)) for k in range(n_kv)]
-    other_weights = lax.ppermute(own_weights, "kv", swap)
+    other_gate = lax.ppermute(sent_gate, "kv", swap)
+    other_up = lax.ppermute(sent_up, "kv", swap)
     attn_part = jnp.dot(merged_all, w_out, preferred_element_type=jnp.float32)
     attn_part = attn_part.astype(jnp.bfloat16).T.reshape(n_tp, feats, seqs)
     own_middle, middle_copies = residual(exchanged(attn_part, "tp"), own_tokens)
     pairs = [[k * n_tp + t for t in range(2 * n_tp)] for k in range(0, n_kv, 2)]
     middle_rows = exchanged(middle_copies, ("kv", "tp"), pairs)
-    partial = widen(middle_rows, vectors, own_weights, other_weights, 2 * units)
+    partial = widen(middle_rows, vectors, other_gain, gate, up, other_gate, other_up)
     halves = [list(range(place, n_kv, 2)) for place in range(2)]
     arrived = exchanged(partial.reshape(n_kv // 2, own_seqs, -1), "kv", halves)
     sums = arrived.astype(jnp.float32).sum(axis=0)

time: 177 us -> 177 us (level)
  blocking collectives: 115 us -> 87.3 us
  waiting for transfers between devices: 0.01 us -> 18.5 us
  starting transfers between devices: 47.2 us -> 61.5 us
  local copies, waits for them, and re-layouts: 8.33 us -> 2.31 us
    all_to_all x7 -> x5, blocking collectives: 115 us -> 87.3 us  [exchanged(): lax.all_to_all(blocks, axis, split_axis=0, concat_axis=0, tiled=True, axi...]
    all_to_all x1 -> x3, waiting for transfers between devices: 0.01 us -> 14.6 us  [exchanged(): lax.all_to_all(blocks, axis, split_axis=0, concat_axis=0, tiled=True, axi...]
    all_to_all x1 -> x3, starting transfers between devices: 44.7 us -> 56.2 us  [exchanged(): lax.all_to_all(blocks, axis, split_axis=0, concat_axis=0, tiled=True, axi...]
    ppermute x1 -> x2, waiting for transfers between devices: 0.01 us -> 3.94 us  [the longest x1 3.94 us: body(): other_up = lax.ppermute(sent_up, 'kv', swap)]
    concatenate x1, local copies, waits for them, and re-layouts: 3.85 us -> 0.03 us  [body(): small = jnp.concatenate([narrow[0], gain_tile, *narrow[1:]], axis=0)]
    ppermute x1 -> x2, starting transfers between devices: 2.42 us -> 5.34 us  [the longest x1 2.87 us: body(): other_up = lax.ppermute(sent_up, 'kv', swap)]
    unnamed x30 -> x34, local copies, waits for them, and re-layouts: 4.22 us -> 1.32 us
  transfers between devices with their start and end apart: 2 -> 5, of which waited for: 0 -> 4; matrix products, arithmetic and copies ran while one was open for 2% -> 0% of each run, Pallas kernels for 0% -> 0%
where the time goes in v6:
time: 177 us; the launch traced here: 176 us
  blocking collectives  87.3 us (49%)
  starting transfers between devices  61.5 us (35%)
  waiting for transfers between devices  18.5 us (10%)
  Pallas kernels  3.61 us (2%)
  local copies, waits for them, and re-layouts  2.31 us (1%)
  between operations  2.2 us (1%)
    all_to_all x5, blocking collectives, exchanged(): lax.all_to_all(blocks, axis, split_axis=0, concat_axis=0, tiled=True, axi...  87.3 us
    all_to_all x3, starting transfers between devices, exchanged(): lax.all_to_all(blocks, axis, split_axis=0, concat_axis=0, tiled=True, axi...  56.2 us
    all_to_all x3, waiting for transfers between devices, exchanged(): lax.all_to_all(blocks, axis, split_axis=0, concat_axis=0, tiled=True, axi...  14.6 us
    ppermute x1, waiting for transfers between devices, body(): other_up = lax.ppermute(sent_up, 'kv', swap)  3.94 us
  transfers between devices with their start and end apart: 5, of which 4 were waited for; matrix products, arithmetic and copies ran while one was open for 0% of the time, Pallas kernels for 0%

profile of v6, /device:TPU:65, one launch (start us, length us, event | category | flops | bytes accessed | tf_op | source)
XLA Modules:
  0.0 176.2 jit_solution(7054527207493090574)
XLA Ops:
  0.6 0.0 copy-start
  0.6 0.0 copy-start.6
  0.7 0.7 copy-done.6
  1.4 0.6 spread.1
  2.0 0.0 copy-start.13
  2.0 44.9 %all-to-all-start = ((bf16[16,16,128]{2,1,0:T(8,128)(2,1)}), bf16[16,16,128]{2,1,0:T(8,128)(2,1)S(1)}, u32[]{:S(2)}, u32[]{:S(2)}) async-start(bf16[16,16,128]{2,1,0:T(8,128)(2,1)} %get-tuple-element.22), calls=%async_computation | async-start | bytes 131072 | tf_op jit(solution)/shard_map/all_to_all | solution.py:25
  46.9 0.0 copy-done.13
  46.9 0.0 copy-start.16
  46.9 0.0 copy-start.15
  46.9 0.0 copy-start.11
  46.9 0.0 copy-start.12
  47.0 0.1 reshape.48
  47.0 0.0 copy-start.10
  47.7 0.0 copy-start.14
  48.4 0.0 copy-done.15
  48.4 0.0 copy-start.8
  48.4 0.0 copy-start.9
  48.4 0.1 pad_convert_fusion
  48.5 0.0 copy-done.11
  48.5 0.0 copy-done.12
  48.5 0.1 fusion.8
  48.6 0.0 copy-done.16
  48.6 0.0 copy-done.10
  48.6 0.0 copy-done.14
  48.7 0.5 copy-done.8
  49.2 0.0 copy-done.9
  49.2 0.0 copy-start.4
  49.2 0.0 copy-start.5
  49.2 5.6 %all-to-all-done = bf16[16,16,128]{2,1,0:T(8,128)(2,1)S(1)} async-done(((bf16[16,16,128]{2,1,0:T(8,128)(2,1)}), bf16[16,16,128]{2,1,0:T(8,128)(2,1)S(1)}, u32[]{:S(2)}, u32[]{:S(2)}) %all-to-all-start) | async-done | bytes 65568 | tf_op jit(solution)/shard_map/all_to_all | solution.py:25
  54.8 0.0 copy-done.4
  54.8 0.0 copy-done.5
  54.8 0.0 copy-start.3
  54.8 0.3 project.1
  55.1 0.0 copy-start.7
  55.1 19.1 %all_to_all.40.parts_ref = bf16[16,8,512]{2,1,0:T(8,128)(2,1)S(1)} all-to-all(bf16[16,8,512]{2,1,0:T(8,128)(2,1)S(1)} %bitcast.45), channel_id=1, replica_groups=mesh['grp'=2,'kv'=16,'tp'=16] {'kv'}, dimensions={0} | all-to-all | bytes 262144 | tf_op jit(solution)/shard_map/all_to_all | solution.py:25
  74.2 0.0 copy-done.3
  74.2 0.0 copy-start.1
  74.2 0.0 copy-start.2
  74.2 0.6 cell.1
  74.8 17.8 %all_to_all.41 = bf16[16,8,128]{2,1,0:T(8,128)(2,1)S(1)} all-to-all(bf16[16,8,128]{2,1,0:T(8,128)(2,1)S(1)} %get-tuple-element.25), channel_id=1, replica_groups=mesh['grp'=2,'kv'=16,'tp'=16] {'kv'}, dimensions={0} | all-to-all | bytes 65536 | tf_op jit(solution)/shard_map/all_to_all | solution.py:25
  92.6 0.0 copy-done.7
  92.6 0.1 fusion
  92.8 0.7 copy.32
  93.5 5.3 %all-to-all-start.3 = ((bf16[16,16,128]{2,1,0:T(8,128)(2,1)}), bf16[16,16,128]{2,1,0:T(8,128)(2,1)S(1)}, u32[]{:S(2)}, u32[]{:S(2)}) async-start(bf16[16,16,128]{2,1,0:T(8,128)(2,1)} %bitcast.16), calls=%async_computation.3 | async-start | bytes 131072 | tf_op jit(solution)/shard_map/all_to_all | solution.py:25
  98.8 0.0 copy-done.1
  98.8 2.5 %collective-permute-start = (bf16[688,256]{1,0:T(8,128)(2,1)S(1)}, bf16[688,256]{1,0:T(8,128)(2,1)S(1)}, u32[]{:S(2)}, u32[]{:S(2)}) collective-permute-start(bf16[688,256]{1,0:T(8,128)(2,1)S(1)} %bitcast.39), channel_id=1, source_target_pairs={{0,16},{16,0},{32,48},{48,32},{64,80},{80,64},{96,112},{112,96},{1... | collective-permute-start | bytes 1056776 | tf_op jit(solution)/shard_map/ppermute | solution.py:349
  101.3 0.0 copy-done.2
  101.3 2.9 %collective-permute-start.1 = (bf16[688,256]{1,0:T(8,128)(2,1)S(1)}, bf16[688,256]{1,0:T(8,128)(2,1)S(1)}, u32[]{:S(2)}, u32[]{:S(2)}) collective-permute-start(bf16[688,256]{1,0:T(8,128)(2,1)S(1)} %bitcast.41), channel_id=1, source_target_pairs={{0,16},{16,0},{32,48},{48,32},{64,80},{80,64},{96,112},{112,96},{1... | collective-permute-start | bytes 1056776 | tf_op jit(solution)/shard_map/ppermute | solution.py:350
  104.2 2.5 %all-to-all-done.3.parts_ref = bf16[16,16,128]{2,1,0:T(8,128)(2,1)S(1)} async-done(((bf16[16,16,128]{2,1,0:T(8,128)(2,1)}), bf16[16,16,128]{2,1,0:T(8,128)(2,1)S(1)}, u32[]{:S(2)}, u32[]{:S(2)}) %all-to-all-start.3) | async-done | bytes 65568 | tf_op jit(solution)/shard_map/all_to_all | solution.py:25
  106.7 0.7 residual.1
  107.4 6.0 %all-to-all-start.4 = ((bf16[32,8,128]{2,1,0:T(8,128)(2,1)}), bf16[32,8,128]{2,1,0:T(8,128)(2,1)S(1)}, u32[]{:S(2)}, u32[]{:S(2)}) async-start(bf16[32,8,128]{2,1,0:T(8,128)(2,1)} %get-tuple-element.28), calls=%async_computation.4 | async-start | bytes 131072 | tf_op jit(solution)/shard_map/all_to_all | solution.py:25
  113.5 0.0 collective-permute-done.other_gate_ref
  113.5 3.9 %collective-permute-done.1.other_up_ref = bf16[688,256]{1,0:T(8,128)(2,1)S(1)} collective-permute-done((bf16[688,256]{1,0:T(8,128)(2,1)S(1)}, bf16[688,256]{1,0:T(8,128)(2,1)S(1)}, u32[]{:S(2)}, u32[]{:S(2)}) %collective-permute-start.1) | collective-permute-done | bytes 352288 | tf_op jit(solution)/shard_map/ppermute | solution.py:350
  117.4 6.4 %all-to-all-done.4.x_ref = bf16[32,8,128]{2,1,0:T(8,128)(2,1)S(1)} async-done(((bf16[32,8,128]{2,1,0:T(8,128)(2,1)}), bf16[32,8,128]{2,1,0:T(8,128)(2,1)S(1)}, u32[]{:S(2)}, u32[]{:S(2)}) %all-to-all-start.4) | async-done | bytes 65568 | tf_op jit(solution)/shard_map/all_to_all | solution.py:25
  123.8 0.6 widen.1
  124.5 17.4 %all_to_all.42 = bf16[8,8,1408]{2,1,0:T(8,128)(2,1)S(1)} all-to-all(bf16[8,8,1408]{2,1,0:T(8,128)(2,1)S(1)} %bitcast.38), channel_id=1, replica_groups={{0,32,64,96,128,160,192,224},{16,48,80,112,144,176,208,240},{1,33,65,97..., dimensions={0} | all-to-all | bytes 360448 | tf_op jit(solution)/shard_map/all_to_all | solution.py:25
  141.9 0.2 fusion.7
  142.1 0.1 fusion.4
  142.2 18.0 %all_to_all.43 = bf16[16,8,688]{2,1,0:T(8,128)(2,1)S(1)} all-to-all(bf16[16,8,688]{2,1,0:T(8,128)(2,1)S(1)} %broadcast_in_dim.15), channel_id=1, replica_groups={{0,32,64,96,128,160,192,224,16,48,80,112,144,176,208,240},{1,33,65,97,1..., dimensions={0} | all-to-all | bytes 352256 | tf_op jit(solution)/shard_map/all_to_all | solution.py:25
  160.2 0.0 copy-done
  160.2 0.2 fusion.1
  160.5 0.1 copy.33
  160.6 14.9 %all_to_all.44.parts_ref = bf16[16,16,128]{2,1,0:T(8,128)(2,1)S(1)} all-to-all(bf16[16,16,128]{2,1,0:T(8,128)(2,1)S(1)} %bitcast.47), channel_id=1, replica_groups=mesh['grp'=2,'kv'=16,'tp'=16] {'tp'}, dimensions={0} | all-to-all | bytes 131072 | tf_op jit(solution)/shard_map/all_to_all | solution.py:25
  175.5 0.7 finish.1
  (9 shorter events, 0.1 us)
Async XLA Ops:
  0.6 159.6 %copy-start = (bf16[688,256]{1,0:T(8,128)(2,1)S(1)}, bf16[688,256]{1,0:T(8,128)(2,1)}, u32[]{:S(2)}) copy-start(bf16[688,256]{1,0:T(8,128)(2,1)} %param.37) | copy-start | bytes 1056772
  0.6 0.7 copy-start.6
  2.0 44.9 %copy-start.13 = (bf16[256]{0:T(256)(128)(2,1)S(1)}, bf16[256]{0:T(256)(128)(2,1)}, u32[]{:S(2)}) copy-start(bf16[256]{0:T(256)(128)(2,1)} %param.34) | copy-start | bytes 1540
  2.0 52.8 %all-to-all-start = ((bf16[16,16,128]{2,1,0:T(8,128)(2,1)}), bf16[16,16,128]{2,1,0:T(8,128)(2,1)S(1)}, u32[]{:S(2)}, u32[]{:S(2)}) async-start(bf16[16,16,128]{2,1,0:T(8,128)(2,1)} %get-tuple-element.22), calls=%async_computation | async-start | bytes 131072 | tf_op jit(solution)/shard_map/all_to_all | solution.py:25
  46.9 1.7 copy-start.16
  46.9 1.5 copy-start.15
  46.9 1.6 copy-start.11
  46.9 1.6 copy-start.12
  47.0 1.6 copy-start.10
  47.7 0.9 copy-start.14
  48.4 0.8 copy-start.8
  48.4 0.8 copy-start.9
  49.2 5.6 %copy-start.4 = (bf16[256,128]{1,0:T(8,128)(2,1)S(1)}, bf16[256,128]{1,0:T(8,128)(2,1)}, u32[]{:S(2)}) copy-start(bf16[256,128]{1,0:T(8,128)(2,1)} %value_ref.1) | copy-start | bytes 196612
  49.2 5.6 %copy-start.5 = (bf16[256,128]{1,0:T(8,128)(2,1)S(1)}, bf16[256,128]{1,0:T(8,128)(2,1)}, u32[]{:S(2)}) copy-start(bf16[256,128]{1,0:T(8,128)(2,1)} %ogate_ref.1) | copy-start | bytes 196612
  54.8 19.4 %copy-start.3 = (f32[8,1,64,128]{3,2,1,0:T(8,128)S(1)}, f32[8,1,64,128]{3,2,1,0:T(8,128)}, u32[]{:S(2)}) copy-start(f32[8,1,64,128]{3,2,1,0:T(8,128)} %param.29) | copy-start | bytes 786436
  55.1 37.5 %copy-start.7 = (bf16[128,256]{1,0:T(8,128)(2,1)S(1)}, bf16[128,256]{1,0:T(8,128)(2,1)}, u32[]{:S(2)}) copy-start(bf16[128,256]{1,0:T(8,128)(2,1)} %param.33) | copy-start | bytes 196612
  74.2 24.6 %copy-start.1 = (bf16[256,688]{0,1:T(8,128)(2,1)S(1)}, bf16[256,688]{0,1:T(8,128)(2,1)}, u32[]{:S(2)}) copy-start(bf16[256,688]{0,1:T(8,128)(2,1)} %param.35) | copy-start | bytes 1056772
  74.2 27.1 %copy-start.2 = (bf16[256,688]{0,1:T(8,128)(2,1)S(1)}, bf16[256,688]{0,1:T(8,128)(2,1)}, u32[]{:S(2)}) copy-start(bf16[256,688]{0,1:T(8,128)(2,1)} %param.36) | copy-start | bytes 1056772
  93.5 13.2 %all-to-all-start.3 = ((bf16[16,16,128]{2,1,0:T(8,128)(2,1)}), bf16[16,16,128]{2,1,0:T(8,128)(2,1)S(1)}, u32[]{:S(2)}, u32[]{:S(2)}) async-start(bf16[16,16,128]{2,1,0:T(8,128)(2,1)} %bitcast.16), calls=%async_computation.3 | async-start | bytes 131072 | tf_op jit(solution)/shard_map/all_to_all | solution.py:25
  98.8 14.7 %collective-permute-start = (bf16[688,256]{1,0:T(8,128)(2,1)S(1)}, bf16[688,256]{1,0:T(8,128)(2,1)S(1)}, u32[]{:S(2)}, u32[]{:S(2)}) collective-permute-start(bf16[688,256]{1,0:T(8,128)(2,1)S(1)} %bitcast.39), channel_id=1, source_target_pairs={{0,16},{16,0},{32,48},{48,32},{64,80},{80,64},{96,112},{112,96},{1... | collective-permute-start | bytes 1056776 | tf_op jit(solution)/shard_map/ppermute | solution.py:349
  101.3 16.1 %collective-permute-start.1 = (bf16[688,256]{1,0:T(8,128)(2,1)S(1)}, bf16[688,256]{1,0:T(8,128)(2,1)S(1)}, u32[]{:S(2)}, u32[]{:S(2)}) collective-permute-start(bf16[688,256]{1,0:T(8,128)(2,1)S(1)} %bitcast.41), channel_id=1, source_target_pairs={{0,16},{16,0},{32,48},{48,32},{64,80},{80,64},{96,112},{112,96},{1... | collective-permute-start | bytes 1056776 | tf_op jit(solution)/shard_map/ppermute | solution.py:350
  107.4 16.4 %all-to-all-start.4 = ((bf16[32,8,128]{2,1,0:T(8,128)(2,1)}), bf16[32,8,128]{2,1,0:T(8,128)(2,1)S(1)}, u32[]{:S(2)}, u32[]{:S(2)}) async-start(bf16[32,8,128]{2,1,0:T(8,128)(2,1)} %get-tuple-element.28), calls=%async_computation.4 | async-start | bytes 131072 | tf_op jit(solution)/shard_map/all_to_all | solution.py:25

commit v7 on v6

--- a/solution.py
+++ b/solution.py
@@ -147,8 +147,8 @@
     head_out = jnp.concatenate(rows, axis=0) / denominator
     merged = head_out * small_ref[2 * seqs + 1 : 2 * seqs + 2, :] / (1.0 + jnp.exp(-ogate))
     merged = merged.astype(out_ref.dtype)
-    for copy in range(out_ref.shape[0]):
-        out_ref[copy] = merged
+    for place in range(out_ref.shape[0]):
+        out_ref[place] = merged
 
 
 def cell(parts, state_c, small, width):
@@ -243,15 +243,37 @@
     )(parts, middle, *states)
 
 
-def widen_kernel(
-    x_ref, vectors_ref, gain_ref, gate_ref, up_ref, other_gate_ref, other_up_ref, out_ref
-):
+def pack_kernel(gate_ref, up_ref, out_ref, sems):
+    units = gate_ref.shape[0]
+    copies = [
+        pltpu.make_async_copy(source, out_ref.at[pl.ds(k * units, units)], sems.at[k])
+        for k, source in enumerate((gate_ref, up_ref))
+    ]
+    for copy in copies:
+        copy.start()
+    for copy in copies:
+        copy.wait()
+
+
+def pack(gate, up):
+    units, rows = gate.shape
+    return pl.pallas_call(
+        pack_kernel,
+        out_shape=jax.ShapeDtypeStruct((2 * units, rows), gate.dtype),
+        in_specs=[ANY, ANY],
+        out_specs=VMEM,
+        scratch_shapes=[pltpu.SemaphoreType.DMA((2,))],
+        compiler_params=SMALL,
+        name="pack",
+    )(gate, up)
+
+
+def widen_kernel(x_ref, vectors_ref, gain_ref, own_ref, other_ref, out_ref):
     blocks = x_ref.shape[0] // 2
     half = x_ref.shape[2] // 2
-    units = gate_ref.shape[0]
+    units = own_ref.shape[0]
     cols = out_ref.shape[1]
-    start = units // LANES * LANES
-    taken = (LANES - (units - start)) % LANES
+    last = cols - LANES
     place = lax.rem(lax.axis_index("kv"), 2)
 
     def features(which):
@@ -265,35 +287,27 @@
     )
     own = (own * vectors_ref[3:4, :]).astype(jnp.bfloat16)
     other = (other * gain_ref[...]).astype(jnp.bfloat16)
-
-    def product(pick):
-        return transposed_product(own, pick(gate_ref, up_ref)) + transposed_product(
-            other, pick(other_gate_ref, other_up_ref)
-        )
-
-    out_ref[:, :start] = product(lambda gate, up: gate[:start, :]).astype(out_ref.dtype)
-    if taken:
-        mixed = product(
-            lambda gate, up: jnp.concatenate([gate[start:, :], up[:taken, :]], axis=0)
-        )
-        out_ref[:, start : start + LANES] = mixed.astype(out_ref.dtype)
-        start += LANES
-    filler = jnp.zeros((cols - 2 * units, gate_ref.shape[1]), gate_ref.dtype)
-    rest = product(lambda gate, up: jnp.concatenate([up[taken:, :], filler], axis=0))
+    out_ref[:, :last] = (
+        transposed_product(own, own_ref[:last, :]) + transposed_product(other, other_ref[:last, :])
+    ).astype(out_ref.dtype)
+    filler = jnp.zeros((cols - units, own_ref.shape[1]), own_ref.dtype)
+    rest = transposed_product(
+        own, jnp.concatenate([own_ref[last:, :], filler], axis=0)
+    ) + transposed_product(other, jnp.concatenate([other_ref[last:, :], filler], axis=0))
     lane = lax.broadcasted_iota(jnp.int32, rest.shape, 1)
-    out_ref[:, start:] = jnp.where(lane == 2 * units - start, squares, rest).astype(out_ref.dtype)
-
-
-def widen(x, vectors, other_gain, *weights):
-    cols = (2 * weights[0].shape[0] // LANES + 1) * LANES
+    out_ref[:, last:] = jnp.where(lane == units - last, squares, rest).astype(out_ref.dtype)
+
+
+def widen(x, vectors, other_gain, own, other):
+    cols = (own.shape[0] // LANES + 1) * LANES
     return pl.pallas_call(
         widen_kernel,
         out_shape=jax.ShapeDtypeStruct((x.shape[2] // 2, cols), jnp.bfloat16),
-        in_specs=[VMEM] * 7,
+        in_specs=[VMEM] * 5,
         out_specs=VMEM,
         compiler_params=SMALL,
         name="widen",
-    )(x, vectors, other_gain, *weights)
+    )(x, vectors, other_gain, own, other)
 
 
 def body(
@@ -343,17 +357,16 @@
     arrived = exchanged(parts.reshape(n_kv, own_seqs, -1), "kv")
     states, other_gain, merged = cell(arrived, state_c, small, rows)
     merged_all = exchanged(merged, "kv").reshape(seqs, -1)
-    gate, up = w_gate.T, w_up.T
-    merged_all, sent_gate, sent_up = lax.optimization_barrier((merged_all, gate, up))
+    merged_all, gate, up = lax.optimization_barrier((merged_all, w_gate.T, w_up.T))
+    own_weights = pack(gate, up)
     swap = [(k, k + 1 - 2 * (k % 2)) for k in range(n_kv)]
-    other_gate = lax.ppermute(sent_gate, "kv", swap)
-    other_up = lax.ppermute(sent_up, "kv", swap)
+    other_weights = lax.ppermute(own_weights, "kv", swap)
     attn_part = jnp.dot(merged_all, w_out, preferred_element_type=jnp.float32)
     attn_part = attn_part.astype(jnp.bfloat16).T.reshape(n_tp, feats, seqs)
     own_middle, middle_copies = residual(exchanged(attn_part, "tp"), own_tokens)
     pairs = [[k * n_tp + t for t in range(2 * n_tp)] for k in range(0, n_kv, 2)]
     middle_rows = exchanged(middle_copies, ("kv", "tp"), pairs)
-    partial = widen(middle_rows, vectors, other_gain, gate, up, other_gate, other_up)
+    partial = widen(middle_rows, vectors, other_gain, own_weights, other_weights)
     halves = [list(range(place, n_kv, 2)) for place in range(2)]
     arrived = exchanged(partial.reshape(n_kv // 2, own_seqs, -1), "kv", halves)
     sums = arrived.astype(jnp.float32).sum(axis=0)

time: 177 us -> 172 us (0.972)
  blocking collectives: 87.3 us -> 111 us
  starting transfers between devices: 61.5 us -> 47.3 us
  waiting for transfers between devices: 18.5 us -> 5.63 us
    all_to_all x5 -> x7, blocking collectives: 87.3 us -> 111 us  [exchanged(): lax.all_to_all(blocks, axis, split_axis=0, concat_axis=0, tiled=True, axi...]
    all_to_all x3 -> x1, starting transfers between devices: 56.2 us -> 44.9 us  [exchanged(): lax.all_to_all(blocks, axis, split_axis=0, concat_axis=0, tiled=True, axi...]
    all_to_all x3 -> x1, waiting for transfers between devices: 14.6 us -> 5.63 us  [exchanged(): lax.all_to_all(blocks, axis, split_axis=0, concat_axis=0, tiled=True, axi...]
    ppermute x2 -> x1, waiting for transfers between devices: 3.94 us -> 0.01 us  [body(): other_weights = lax.ppermute(own_weights, 'kv', swap)]
    ppermute x2 -> x1, starting transfers between devices: 5.34 us -> 2.43 us  [body(): other_weights = lax.ppermute(own_weights, 'kv', swap)]
  transfers between devices with their start and end apart: 5 -> 2, of which waited for: 4 -> 1; matrix products, arithmetic and copies ran while one was open for 0% -> 0% of each run, Pallas kernels for 0% -> 0%
where the time goes in v7:
time: 172 us
  blocking collectives  111 us (65%)
  starting transfers between devices  47.3 us (28%)
  waiting for transfers between devices  5.63 us (3%)
  Pallas kernels  3.28 us (2%)
  between operations  2.2 us (1%)
    all_to_all x7, blocking collectives, exchanged(): lax.all_to_all(blocks, axis, split_axis=0, concat_axis=0, tiled=True, axi...  111 us
    all_to_all x1, starting transfers between devices, exchanged(): lax.all_to_all(blocks, axis, split_axis=0, concat_axis=0, tiled=True, axi...  44.9 us
    all_to_all x1, waiting for transfers between devices, exchanged(): lax.all_to_all(blocks, axis, split_axis=0, concat_axis=0, tiled=True, axi...  5.63 us
  transfers between devices with their start and end apart: 2, of which 1 were waited for; matrix products, arithmetic and copies ran while one was open for 0% of the time, Pallas kernels for 0%

profile of v7, /device:TPU:65, one launch (start us, length us, event | category | flops | bytes accessed | tf_op | source)
XLA Modules:
  0.0 171.9 jit_solution(16474435076648971931)
XLA Ops:
  0.6 0.0 copy-start
  0.6 0.0 copy-start.6
  0.7 0.7 copy-done.6
  1.4 0.6 spread.1
  2.0 0.0 copy-start.13
  2.0 44.9 %all-to-all-start = ((bf16[16,16,128]{2,1,0:T(8,128)(2,1)}), bf16[16,16,128]{2,1,0:T(8,128)(2,1)S(1)}, u32[]{:S(2)}, u32[]{:S(2)}) async-start(bf16[16,16,128]{2,1,0:T(8,128)(2,1)} %get-tuple-element.22), calls=%async_computation | async-start | bytes 131072 | tf_op jit(solution)/shard_map/all_to_all | solution.py:25
  46.9 0.0 copy-done.13
  46.9 0.0 copy-start.16
  46.9 0.0 copy-start.15
  46.9 0.0 copy-start.11
  46.9 0.0 copy-start.12
  47.0 0.1 reshape.48
  47.0 0.0 copy-start.10
  47.7 0.0 copy-start.14
  48.4 0.0 copy-done.15
  48.4 0.0 copy-start.8
  48.4 0.0 copy-start.9
  48.4 0.1 pad_convert_fusion
  48.5 0.0 copy-done.11
  48.5 0.0 copy-done.12
  48.5 0.1 fusion.8
  48.6 0.0 copy-done.16
  48.6 0.0 copy-done.10
  48.6 0.0 copy-done.14
  48.7 0.5 copy-done.8
  49.2 0.0 copy-done.9
  49.2 0.0 copy-start.4
  49.2 0.0 copy-start.5
  49.2 5.6 %all-to-all-done = bf16[16,16,128]{2,1,0:T(8,128)(2,1)S(1)} async-done(((bf16[16,16,128]{2,1,0:T(8,128)(2,1)}), bf16[16,16,128]{2,1,0:T(8,128)(2,1)S(1)}, u32[]{:S(2)}, u32[]{:S(2)}) %all-to-all-start) | async-done | bytes 65568 | tf_op jit(solution)/shard_map/all_to_all | solution.py:25
  54.8 0.0 copy-done.4
  54.8 0.0 copy-done.5
  54.8 0.0 copy-start.3
  54.8 0.3 project.1
  55.1 0.0 copy-start.1
  55.1 0.0 copy-start.2
  55.1 19.1 %all_to_all.40.parts_ref = bf16[16,8,512]{2,1,0:T(8,128)(2,1)S(1)} all-to-all(bf16[16,8,512]{2,1,0:T(8,128)(2,1)S(1)} %bitcast.43), channel_id=1, replica_groups=mesh['grp'=2,'kv'=16,'tp'=16] {'kv'}, dimensions={0} | all-to-all | bytes 262144 | tf_op jit(solution)/shard_map/all_to_all | solution.py:25
  74.2 0.0 copy-done.3
  74.2 0.6 cell.1
  74.8 17.8 %all_to_all.41 = bf16[16,8,128]{2,1,0:T(8,128)(2,1)S(1)} all-to-all(bf16[16,8,128]{2,1,0:T(8,128)(2,1)S(1)} %get-tuple-element.25), channel_id=1, replica_groups=mesh['grp'=2,'kv'=16,'tp'=16] {'kv'}, dimensions={0} | all-to-all | bytes 65536 | tf_op jit(solution)/shard_map/all_to_all | solution.py:25
  92.6 0.0 copy-done.1
  92.6 0.0 copy-done.2
  92.6 0.0 copy-start.7
  92.6 0.3 pack.1.own_ref
  92.9 2.4 %collective-permute-start = (bf16[1376,256]{1,0:T(8,128)(2,1)S(1)}, bf16[1376,256]{1,0:T(8,128)(2,1)S(1)}, u32[]{:S(2)}, u32[]{:S(2)}) collective-permute-start(bf16[1376,256]{1,0:T(8,128)(2,1)S(1)} %pack.1.own_ref), channel_id=1, source_target_pairs={{0,16},{16,0},{32,48},{48,32},{64,80},{80,64},{96,112},{112,96},{1... | collective-permute-start | bytes 2113544 | tf_op jit(solution)/shard_map/ppermute | solution.py:363
  95.4 0.0 copy-done.7
  95.4 0.1 fusion
  95.5 0.1 copy.32
  95.7 12.6 %all_to_all.42.parts_ref = bf16[16,16,128]{2,1,0:T(8,128)(2,1)S(1)} all-to-all(bf16[16,16,128]{2,1,0:T(8,128)(2,1)S(1)} %bitcast.45), channel_id=1, replica_groups=mesh['grp'=2,'kv'=16,'tp'=16] {'tp'}, dimensions={0} | all-to-all | bytes 131072 | tf_op jit(solution)/shard_map/all_to_all | solution.py:25
  108.3 0.1 residual.1
  108.4 11.3 %all_to_all.43.x_ref = bf16[32,8,128]{2,1,0:T(8,128)(2,1)S(1)} all-to-all(bf16[32,8,128]{2,1,0:T(8,128)(2,1)S(1)} %get-tuple-element.28), channel_id=1, replica_groups={{0,1,2,3,4,5,6,7,8,9,10,11,12,13,14,15,16,17,18,19,20,21,22,23,24,25,26..., dimensions={0} | all-to-all | bytes 131072 | tf_op jit(solution)/shard_map/all_to_all | solution.py:25
  119.7 0.0 collective-permute-done.other_ref
  119.7 0.6 widen.1
  120.3 17.4 %all_to_all.44 = bf16[8,8,1408]{2,1,0:T(8,128)(2,1)S(1)} all-to-all(bf16[8,8,1408]{2,1,0:T(8,128)(2,1)S(1)} %bitcast.38), channel_id=1, replica_groups={{0,32,64,96,128,160,192,224},{16,48,80,112,144,176,208,240},{1,33,65,97..., dimensions={0} | all-to-all | bytes 360448 | tf_op jit(solution)/shard_map/all_to_all | solution.py:25
  137.7 0.2 fusion.7
  137.9 0.1 fusion.4
  138.0 18.1 %all_to_all.45 = bf16[16,8,688]{2,1,0:T(8,128)(2,1)S(1)} all-to-all(bf16[16,8,688]{2,1,0:T(8,128)(2,1)S(1)} %broadcast_in_dim.15), channel_id=1, replica_groups={{0,32,64,96,128,160,192,224,16,48,80,112,144,176,208,240},{1,33,65,97,1..., dimensions={0} | all-to-all | bytes 352256 | tf_op jit(solution)/shard_map/all_to_all | solution.py:25
  156.2 0.0 copy-done
  156.2 0.2 fusion.1
  156.4 0.1 copy.33
  156.5 14.6 %all_to_all.46.parts_ref = bf16[16,16,128]{2,1,0:T(8,128)(2,1)S(1)} all-to-all(bf16[16,16,128]{2,1,0:T(8,128)(2,1)S(1)} %bitcast.46), channel_id=1, replica_groups=mesh['grp'=2,'kv'=16,'tp'=16] {'tp'}, dimensions={0} | all-to-all | bytes 131072 | tf_op jit(solution)/shard_map/all_to_all | solution.py:25
  171.1 0.7 finish.1
  (9 shorter events, 0.1 us)
Async XLA Ops:
  0.6 155.6 %copy-start = (bf16[688,256]{1,0:T(8,128)(2,1)S(1)}, bf16[688,256]{1,0:T(8,128)(2,1)}, u32[]{:S(2)}) copy-start(bf16[688,256]{1,0:T(8,128)(2,1)} %param.37) | copy-start | bytes 1056772
  0.6 0.7 copy-start.6
  2.0 44.9 %copy-start.13 = (bf16[256]{0:T(256)(128)(2,1)S(1)}, bf16[256]{0:T(256)(128)(2,1)}, u32[]{:S(2)}) copy-start(bf16[256]{0:T(256)(128)(2,1)} %param.34) | copy-start | bytes 1540
  2.0 52.8 %all-to-all-start = ((bf16[16,16,128]{2,1,0:T(8,128)(2,1)}), bf16[16,16,128]{2,1,0:T(8,128)(2,1)S(1)}, u32[]{:S(2)}, u32[]{:S(2)}) async-start(bf16[16,16,128]{2,1,0:T(8,128)(2,1)} %get-tuple-element.22), calls=%async_computation | async-start | bytes 131072 | tf_op jit(solution)/shard_map/all_to_all | solution.py:25
  46.9 1.7 copy-start.16
  46.9 1.5 copy-start.15
  46.9 1.6 copy-start.11
  46.9 1.6 copy-start.12
  47.0 1.6 copy-start.10
  47.7 0.9 copy-start.14
  48.4 0.8 copy-start.8
  48.4 0.8 copy-start.9
  49.2 5.6 %copy-start.4 = (bf16[256,128]{1,0:T(8,128)(2,1)S(1)}, bf16[256,128]{1,0:T(8,128)(2,1)}, u32[]{:S(2)}) copy-start(bf16[256,128]{1,0:T(8,128)(2,1)} %value_ref.1) | copy-start | bytes 196612
  49.2 5.6 %copy-start.5 = (bf16[256,128]{1,0:T(8,128)(2,1)S(1)}, bf16[256,128]{1,0:T(8,128)(2,1)}, u32[]{:S(2)}) copy-start(bf16[256,128]{1,0:T(8,128)(2,1)} %ogate_ref.1) | copy-start | bytes 196612
  54.8 19.4 %copy-start.3 = (f32[8,1,64,128]{3,2,1,0:T(8,128)S(1)}, f32[8,1,64,128]{3,2,1,0:T(8,128)}, u32[]{:S(2)}) copy-start(f32[8,1,64,128]{3,2,1,0:T(8,128)} %param.29) | copy-start | bytes 786436
  55.1 37.5 %copy-start.1 = (bf16[256,688]{0,1:T(8,128)(2,1)S(1)}, bf16[256,688]{0,1:T(8,128)(2,1)}, u32[]{:S(2)}) copy-start(bf16[256,688]{0,1:T(8,128)(2,1)} %param.35) | copy-start | bytes 1056772
  55.1 37.5 %copy-start.2 = (bf16[256,688]{0,1:T(8,128)(2,1)S(1)}, bf16[256,688]{0,1:T(8,128)(2,1)}, u32[]{:S(2)}) copy-start(bf16[256,688]{0,1:T(8,128)(2,1)} %param.36) | copy-start | bytes 1056772
  92.6 2.7 %copy-start.7 = (bf16[128,256]{1,0:T(8,128)(2,1)S(1)}, bf16[128,256]{1,0:T(8,128)(2,1)}, u32[]{:S(2)}) copy-start(bf16[128,256]{1,0:T(8,128)(2,1)} %param.33) | copy-start | bytes 196612
  92.9 26.8 %collective-permute-start = (bf16[1376,256]{1,0:T(8,128)(2,1)S(1)}, bf16[1376,256]{1,0:T(8,128)(2,1)S(1)}, u32[]{:S(2)}, u32[]{:S(2)}) collective-permute-start(bf16[1376,256]{1,0:T(8,128)(2,1)S(1)} %pack.1.own_ref), channel_id=1, source_target_pairs={{0,16},{16,0},{32,48},{48,32},{64,80},{80,64},{96,112},{112,96},{1... | collective-permute-start | bytes 2113544 | tf_op jit(solution)/shard_map/ppermute | solution.py:363

commit v8 on v7

--- a/solution.py
+++ b/solution.py
@@ -356,9 +356,9 @@
     parts, small = project(token_rows, vectors, small, w_both, w_value, w_ogate)
     arrived = exchanged(parts.reshape(n_kv, own_seqs, -1), "kv")
     states, other_gain, merged = cell(arrived, state_c, small, rows)
+    merged, gate, up = lax.optimization_barrier((merged, w_gate.T, w_up.T))
+    own_weights = pack(gate, up)
     merged_all = exchanged(merged, "kv").reshape(seqs, -1)
-    merged_all, gate, up = lax.optimization_barrier((merged_all, w_gate.T, w_up.T))
-    own_weights = pack(gate, up)
     swap = [(k, k + 1 - 2 * (k % 2)) for k in range(n_kv)]
     other_weights = lax.ppermute(own_weights, "kv", swap)
     attn_part = jnp.dot(merged_all, w_out, preferred_element_type=jnp.float32)

time: 172 us -> 170 us (0.988)
  blocking collectives: 111 us -> 92.9 us
  waiting for transfers between devices: 5.63 us -> 13.6 us
  starting transfers between devices: 47.3 us -> 54.7 us
    all_to_all x7 -> x6, blocking collectives: 111 us -> 92.9 us  [exchanged(): lax.all_to_all(blocks, axis, split_axis=0, concat_axis=0, tiled=True, axi...]
    all_to_all x1 -> x2, waiting for transfers between devices: 5.63 us -> 13.6 us  [exchanged(): lax.all_to_all(blocks, axis, split_axis=0, concat_axis=0, tiled=True, axi...]
    all_to_all x1 -> x2, starting transfers between devices: 44.9 us -> 51.6 us  [exchanged(): lax.all_to_all(blocks, axis, split_axis=0, concat_axis=0, tiled=True, axi...]
  transfers between devices with their start and end apart: 2 -> 3, of which waited for: 1 -> 2; matrix products, arithmetic and copies ran while one was open for 0% -> 0% of each run, Pallas kernels for 0% -> 0%
where the time goes in v8:
time: 170 us
  blocking collectives  92.9 us (55%)
  starting transfers between devices  54.7 us (32%)
  waiting for transfers between devices  13.6 us (8%)
  Pallas kernels  3.9 us (2%)
  between operations  2.22 us (1%)
    all_to_all x6, blocking collectives, exchanged(): lax.all_to_all(blocks, axis, split_axis=0, concat_axis=0, tiled=True, axi...  92.9 us
    all_to_all x2, starting transfers between devices, exchanged(): lax.all_to_all(blocks, axis, split_axis=0, concat_axis=0, tiled=True, axi...  51.6 us
    all_to_all x2, waiting for transfers between devices, exchanged(): lax.all_to_all(blocks, axis, split_axis=0, concat_axis=0, tiled=True, axi...  13.6 us
  transfers between devices with their start and end apart: 3, of which 2 were waited for; matrix products, arithmetic and copies ran while one was open for 0% of the time, Pallas kernels for 0%

profile of v8, /device:TPU:65, one launch (start us, length us, event | category | flops | bytes accessed | tf_op | source)
XLA Modules:
  0.0 169.8 jit_solution(17254988320925647500)
XLA Ops:
  0.6 0.0 copy-start
  0.6 0.0 copy-start.6
  0.7 0.7 copy-done.6
  1.4 0.6 spread.1
  2.0 0.0 copy-start.13
  2.0 44.9 %all-to-all-start = ((bf16[16,16,128]{2,1,0:T(8,128)(2,1)}), bf16[16,16,128]{2,1,0:T(8,128)(2,1)S(1)}, u32[]{:S(2)}, u32[]{:S(2)}) async-start(bf16[16,16,128]{2,1,0:T(8,128)(2,1)} %get-tuple-element.22), calls=%async_computation | async-start | bytes 131072 | tf_op jit(solution)/shard_map/all_to_all | solution.py:25
  46.9 0.0 copy-done.13
  46.9 0.0 copy-start.16
  46.9 0.0 copy-start.15
  46.9 0.0 copy-start.11
  46.9 0.0 copy-start.12
  47.0 0.1 reshape.48
  47.0 0.0 copy-start.10
  47.7 0.0 copy-start.14
  48.4 0.0 copy-done.15
  48.4 0.0 copy-start.8
  48.4 0.0 copy-start.9
  48.4 0.1 pad_convert_fusion
  48.5 0.0 copy-done.11
  48.5 0.0 copy-done.12
  48.5 0.1 fusion.9
  48.6 0.0 copy-done.16
  48.6 0.0 copy-done.10
  48.6 0.0 copy-done.14
  48.7 0.5 copy-done.8
  49.2 0.0 copy-done.9
  49.2 0.0 copy-start.4
  49.2 0.0 copy-start.5
  49.2 5.6 %all-to-all-done = bf16[16,16,128]{2,1,0:T(8,128)(2,1)S(1)} async-done(((bf16[16,16,128]{2,1,0:T(8,128)(2,1)}), bf16[16,16,128]{2,1,0:T(8,128)(2,1)S(1)}, u32[]{:S(2)}, u32[]{:S(2)}) %all-to-all-start) | async-done | bytes 65568 | tf_op jit(solution)/shard_map/all_to_all | solution.py:25
  54.8 0.0 copy-done.4
  54.8 0.0 copy-done.5
  54.8 0.0 copy-start.3
  54.8 0.3 project.1
  55.1 0.0 copy-start.1
  55.1 0.0 copy-start.2
  55.1 19.1 %all_to_all.40.parts_ref = bf16[16,8,512]{2,1,0:T(8,128)(2,1)S(1)} all-to-all(bf16[16,8,512]{2,1,0:T(8,128)(2,1)S(1)} %bitcast.44), channel_id=1, replica_groups=mesh['grp'=2,'kv'=16,'tp'=16] {'kv'}, dimensions={0} | all-to-all | bytes 262144 | tf_op jit(solution)/shard_map/all_to_all | solution.py:25
  74.2 0.0 copy-done.3
  74.2 1.2 cell.1
  75.5 6.7 %all-to-all-start.2 = ((bf16[16,8,128]{2,1,0:T(8,128)(2,1)}), bf16[16,8,128]{2,1,0:T(8,128)(2,1)S(1)}, u32[]{:S(2)}, u32[]{:S(2)}) async-start(bf16[16,8,128]{2,1,0:T(8,128)(2,1)} %get-tuple-element.26), calls=%async_computation.2 | async-start | bytes 65536 | tf_op jit(solution)/shard_map/all_to_all | solution.py:25
  82.2 0.0 copy-done.1
  82.2 0.0 copy-done.2
  82.2 0.0 copy-start.7
  82.2 0.3 pack.1.own_ref
  82.5 3.1 %collective-permute-start = (bf16[1376,256]{1,0:T(8,128)(2,1)S(1)}, bf16[1376,256]{1,0:T(8,128)(2,1)S(1)}, u32[]{:S(2)}, u32[]{:S(2)}) collective-permute-start(bf16[1376,256]{1,0:T(8,128)(2,1)S(1)} %pack.1.own_ref), channel_id=1, source_target_pairs={{0,16},{16,0},{32,48},{48,32},{64,80},{80,64},{96,112},{112,96},{1... | collective-permute-start | bytes 2113544 | tf_op jit(solution)/shard_map/ppermute | solution.py:363
  85.6 8.0 %all-to-all-done.2 = bf16[16,8,128]{2,1,0:T(8,128)(2,1)S(1)} async-done(((bf16[16,8,128]{2,1,0:T(8,128)(2,1)}), bf16[16,8,128]{2,1,0:T(8,128)(2,1)S(1)}, u32[]{:S(2)}, u32[]{:S(2)}) %all-to-all-start.2) | async-done | bytes 32800 | tf_op jit(solution)/shard_map/all_to_all | solution.py:25
  93.6 0.0 copy-done.7
  93.6 0.1 fusion
  93.8 0.1 copy.32
  93.9 12.4 %all_to_all.41.parts_ref = bf16[16,16,128]{2,1,0:T(8,128)(2,1)S(1)} all-to-all(bf16[16,16,128]{2,1,0:T(8,128)(2,1)S(1)} %bitcast.46), channel_id=1, replica_groups=mesh['grp'=2,'kv'=16,'tp'=16] {'tp'}, dimensions={0} | all-to-all | bytes 131072 | tf_op jit(solution)/shard_map/all_to_all | solution.py:25
  106.3 0.1 residual.1
  106.4 11.3 %all_to_all.42.x_ref = bf16[32,8,128]{2,1,0:T(8,128)(2,1)S(1)} all-to-all(bf16[32,8,128]{2,1,0:T(8,128)(2,1)S(1)} %get-tuple-element.28), channel_id=1, replica_groups={{0,1,2,3,4,5,6,7,8,9,10,11,12,13,14,15,16,17,18,19,20,21,22,23,24,25,26..., dimensions={0} | all-to-all | bytes 131072 | tf_op jit(solution)/shard_map/all_to_all | solution.py:25
  117.7 0.0 collective-permute-done.other_ref
  117.7 0.6 widen.1
  118.4 17.3 %all_to_all.43 = bf16[8,8,1408]{2,1,0:T(8,128)(2,1)S(1)} all-to-all(bf16[8,8,1408]{2,1,0:T(8,128)(2,1)S(1)} %bitcast.39), channel_id=1, replica_groups={{0,32,64,96,128,160,192,224},{16,48,80,112,144,176,208,240},{1,33,65,97..., dimensions={0} | all-to-all | bytes 360448 | tf_op jit(solution)/shard_map/all_to_all | solution.py:25
  135.7 0.2 fusion.8
  135.9 0.1 fusion.5
  136.0 18.1 %all_to_all.44 = bf16[16,8,688]{2,1,0:T(8,128)(2,1)S(1)} all-to-all(bf16[16,8,688]{2,1,0:T(8,128)(2,1)S(1)} %broadcast_in_dim.15), channel_id=1, replica_groups={{0,32,64,96,128,160,192,224,16,48,80,112,144,176,208,240},{1,33,65,97,1..., dimensions={0} | all-to-all | bytes 352256 | tf_op jit(solution)/shard_map/all_to_all | solution.py:25
  154.1 0.0 copy-done
  154.1 0.2 fusion.1
  154.3 0.1 copy.33
  154.4 14.6 %all_to_all.45.parts_ref = bf16[16,16,128]{2,1,0:T(8,128)(2,1)S(1)} all-to-all(bf16[16,16,128]{2,1,0:T(8,128)(2,1)S(1)} %bitcast.47), channel_id=1, replica_groups=mesh['grp'=2,'kv'=16,'tp'=16] {'tp'}, dimensions={0} | all-to-all | bytes 131072 | tf_op jit(solution)/shard_map/all_to_all | solution.py:25
  169.1 0.7 finish.1
  (9 shorter events, 0.1 us)
Async XLA Ops:
  0.6 153.5 %copy-start = (bf16[688,256]{1,0:T(8,128)(2,1)S(1)}, bf16[688,256]{1,0:T(8,128)(2,1)}, u32[]{:S(2)}) copy-start(bf16[688,256]{1,0:T(8,128)(2,1)} %param.37) | copy-start | bytes 1056772
  0.6 0.7 copy-start.6
  2.0 44.9 %copy-start.13 = (bf16[256]{0:T(256)(128)(2,1)S(1)}, bf16[256]{0:T(256)(128)(2,1)}, u32[]{:S(2)}) copy-start(bf16[256]{0:T(256)(128)(2,1)} %param.34) | copy-start | bytes 1540
  2.0 52.8 %all-to-all-start = ((bf16[16,16,128]{2,1,0:T(8,128)(2,1)}), bf16[16,16,128]{2,1,0:T(8,128)(2,1)S(1)}, u32[]{:S(2)}, u32[]{:S(2)}) async-start(bf16[16,16,128]{2,1,0:T(8,128)(2,1)} %get-tuple-element.22), calls=%async_computation | async-start | bytes 131072 | tf_op jit(solution)/shard_map/all_to_all | solution.py:25
  46.9 1.7 %copy-start.16 = (f32[8,1]{0,1:T(1,128)S(1)}, f32[8,1]{0,1:T(1,128)}, u32[]{:S(2)}) copy-start(f32[8,1]{0,1:T(1,128)} %param.31) | copy-start | bytes 100
  46.9 1.5 copy-start.15
  46.9 1.6 copy-start.11
  46.9 1.6 copy-start.12
  47.0 1.6 copy-start.10
  47.7 0.9 copy-start.14
  48.4 0.8 copy-start.8
  48.4 0.8 copy-start.9
  49.2 5.6 %copy-start.4 = (bf16[256,128]{1,0:T(8,128)(2,1)S(1)}, bf16[256,128]{1,0:T(8,128)(2,1)}, u32[]{:S(2)}) copy-start(bf16[256,128]{1,0:T(8,128)(2,1)} %value_ref.1) | copy-start | bytes 196612
  49.2 5.6 %copy-start.5 = (bf16[256,128]{1,0:T(8,128)(2,1)S(1)}, bf16[256,128]{1,0:T(8,128)(2,1)}, u32[]{:S(2)}) copy-start(bf16[256,128]{1,0:T(8,128)(2,1)} %ogate_ref.1) | copy-start | bytes 196612
  54.8 19.4 %copy-start.3 = (f32[8,1,64,128]{3,2,1,0:T(8,128)S(1)}, f32[8,1,64,128]{3,2,1,0:T(8,128)}, u32[]{:S(2)}) copy-start(f32[8,1,64,128]{3,2,1,0:T(8,128)} %param.29) | copy-start | bytes 786436
  55.1 27.1 %copy-start.1 = (bf16[256,688]{0,1:T(8,128)(2,1)S(1)}, bf16[256,688]{0,1:T(8,128)(2,1)}, u32[]{:S(2)}) copy-start(bf16[256,688]{0,1:T(8,128)(2,1)} %param.35) | copy-start | bytes 1056772
  55.1 27.1 %copy-start.2 = (bf16[256,688]{0,1:T(8,128)(2,1)S(1)}, bf16[256,688]{0,1:T(8,128)(2,1)}, u32[]{:S(2)}) copy-start(bf16[256,688]{0,1:T(8,128)(2,1)} %param.36) | copy-start | bytes 1056772
  75.5 18.2 %all-to-all-start.2 = ((bf16[16,8,128]{2,1,0:T(8,128)(2,1)}), bf16[16,8,128]{2,1,0:T(8,128)(2,1)S(1)}, u32[]{:S(2)}, u32[]{:S(2)}) async-start(bf16[16,8,128]{2,1,0:T(8,128)(2,1)} %get-tuple-element.26), calls=%async_computation.2 | async-start | bytes 65536 | tf_op jit(solution)/shard_map/all_to_all | solution.py:25
  82.2 11.4 %copy-start.7 = (bf16[128,256]{1,0:T(8,128)(2,1)S(1)}, bf16[128,256]{1,0:T(8,128)(2,1)}, u32[]{:S(2)}) copy-start(bf16[128,256]{1,0:T(8,128)(2,1)} %param.33) | copy-start | bytes 196612
  82.5 35.2 %collective-permute-start = (bf16[1376,256]{1,0:T(8,128)(2,1)S(1)}, bf16[1376,256]{1,0:T(8,128)(2,1)S(1)}, u32[]{:S(2)}, u32[]{:S(2)}) collective-permute-start(bf16[1376,256]{1,0:T(8,128)(2,1)S(1)} %pack.1.own_ref), channel_id=1, source_target_pairs={{0,16},{16,0},{32,48},{48,32},{64,80},{80,64},{96,112},{112,96},{1... | collective-permute-start | bytes 2113544 | tf_op jit(solution)/shard_map/ppermute | solution.py:363

commit v9 on v8

--- a/solution.py
+++ b/solution.py
@@ -1,11 +1,10 @@
-import functools
-
 import jax
 import jax.numpy as jnp
 from jax import lax
 from jax.experimental import pallas as pl
 from jax.experimental.pallas import tpu as pltpu
 from jax.sharding import PartitionSpec as P
+
 
 D = 4096
 DK = 64
@@ -215,9 +214,20 @@
     ]
     for copy in copies:
         copy.start()
-    total = parts_ref[0].astype(jnp.float32)
-    for k in range(1, parts_ref.shape[0]):
-        total += parts_ref[k].astype(jnp.float32)
+    blocks, half = parts_ref.shape[0] // 2, parts_ref.shape[2] // 2
+    sums = []
+    for place in range(2):
+        total = parts_ref[place * blocks].astype(jnp.float32)
+        for k in range(1, blocks):
+            total += parts_ref[place * blocks + k].astype(jnp.float32)
+        sums.append(total)
+    total = jnp.concatenate(
+        [
+            jnp.concatenate([one[:, :half] for one in sums], axis=1),
+            jnp.concatenate([one[:, half:] for one in sums], axis=1),
+        ],
+        axis=0,
+    )
     tokens[...] = (middle_ref[...].astype(jnp.float32) + total).astype(tokens.dtype)
     copies.append(pltpu.make_async_copy(tokens, out_ref, sems.at[count]))
     copies[count].start()
@@ -229,13 +239,13 @@
     return pl.pallas_call(
         finish_kernel,
         out_shape=(
-            jax.ShapeDtypeStruct(parts.shape[1:], parts.dtype),
+            jax.ShapeDtypeStruct(middle.shape, middle.dtype),
             *(jax.ShapeDtypeStruct(one.shape, one.dtype) for one in states),
         ),
         in_specs=[VMEM] * (2 + len(states)),
         out_specs=(ANY,) * (1 + len(states)),
         scratch_shapes=[
-            pltpu.VMEM(parts.shape[1:], parts.dtype),
+            pltpu.VMEM(middle.shape, middle.dtype),
             pltpu.SemaphoreType.DMA((1 + len(states),)),
         ],
         compiler_params=SMALL,
@@ -243,11 +253,12 @@
     )(parts, middle, *states)
 
 
-def pack_kernel(gate_ref, up_ref, out_ref, sems):
-    units = gate_ref.shape[0]
+def pack_kernel(*refs):
+    sources, out_ref, sems = refs[:-2], refs[-2], refs[-1]
+    units = sources[0].shape[0]
     copies = [
         pltpu.make_async_copy(source, out_ref.at[pl.ds(k * units, units)], sems.at[k])
-        for k, source in enumerate((gate_ref, up_ref))
+        for k, source in enumerate(sources)
     ]
     for copy in copies:
         copy.start()
@@ -255,23 +266,54 @@
         copy.wait()
 
 
-def pack(gate, up):
-    units, rows = gate.shape
+def pack(*arrays):
+    units, rows = arrays[0].shape
+    count = len(arrays)
     return pl.pallas_call(
         pack_kernel,
-        out_shape=jax.ShapeDtypeStruct((2 * units, rows), gate.dtype),
-        in_specs=[ANY, ANY],
+        out_shape=jax.ShapeDtypeStruct((count * units, rows), arrays[0].dtype),
+        in_specs=[ANY] * count,
         out_specs=VMEM,
-        scratch_shapes=[pltpu.SemaphoreType.DMA((2,))],
+        scratch_shapes=[pltpu.SemaphoreType.DMA((count,))],
         compiler_params=SMALL,
         name="pack",
-    )(gate, up)
+    )(*arrays)
+
+
+def lower_kernel(hidden_ref, own_ref, other_ref, out_ref):
+    units = hidden_ref.shape[1]
+    blocks, feats, _ = out_ref.shape
+    blocks //= 2
+    place = lax.rem(lax.axis_index("kv"), 2)
+    hidden = hidden_ref[...]
+
+    def product(weights_ref):
+        down = jnp.dot(
+            hidden, weights_ref[2 * units :, :], preferred_element_type=jnp.float32
+        ).T.reshape(blocks, 2, feats, hidden.shape[0])
+        return jnp.concatenate([down[:, 0], down[:, 1]], axis=2).astype(out_ref.dtype)
+
+    out_ref[pl.ds(place * blocks, blocks)] = product(own_ref)
+    out_ref[pl.ds((1 - place) * blocks, blocks)] = product(other_ref)
+
+
+def lower(hidden, own, other, count, feats):
+    return pl.pallas_call(
+        lower_kernel,
+        out_shape=jax.ShapeDtypeStruct(
+            (2 * count, feats // 2, 2 * hidden.shape[0]), jnp.bfloat16
+        ),
+        in_specs=[VMEM] * 3,
+        out_specs=VMEM,
+        compiler_params=SMALL,
+        name="lower",
+    )(hidden, own, other)
 
 
 def widen_kernel(x_ref, vectors_ref, gain_ref, own_ref, other_ref, out_ref):
     blocks = x_ref.shape[0] // 2
     half = x_ref.shape[2] // 2
-    units = own_ref.shape[0]
+    units = own_ref.shape[0] // 3 * 2
     cols = out_ref.shape[1]
     last = cols - LANES
     place = lax.rem(lax.axis_index("kv"), 2)
@@ -292,14 +334,14 @@
     ).astype(out_ref.dtype)
     filler = jnp.zeros((cols - units, own_ref.shape[1]), own_ref.dtype)
     rest = transposed_product(
-        own, jnp.concatenate([own_ref[last:, :], filler], axis=0)
-    ) + transposed_product(other, jnp.concatenate([other_ref[last:, :], filler], axis=0))
+        own, jnp.concatenate([own_ref[last:units, :], filler], axis=0)
+    ) + transposed_product(other, jnp.concatenate([other_ref[last:units, :], filler], axis=0))
     lane = lax.broadcasted_iota(jnp.int32, rest.shape, 1)
     out_ref[:, last:] = jnp.where(lane == units - last, squares, rest).astype(out_ref.dtype)
 
 
 def widen(x, vectors, other_gain, own, other):
-    cols = (own.shape[0] // LANES + 1) * LANES
+    cols = (own.shape[0] // 3 * 2 // LANES + 1) * LANES
     return pl.pallas_call(
         widen_kernel,
         out_shape=jax.ShapeDtypeStruct((x.shape[2] // 2, cols), jnp.bfloat16),
@@ -356,10 +398,10 @@
     parts, small = project(token_rows, vectors, small, w_both, w_value, w_ogate)
     arrived = exchanged(parts.reshape(n_kv, own_seqs, -1), "kv")
     states, other_gain, merged = cell(arrived, state_c, small, rows)
-    merged, gate, up = lax.optimization_barrier((merged, w_gate.T, w_up.T))
-    own_weights = pack(gate, up)
+    merged, gate, up, down = lax.optimization_barrier((merged, w_gate.T, w_up.T, w_down))
+    swap = [(k, k + 1 - 2 * (k % 2)) for k in range(n_kv)]
     merged_all = exchanged(merged, "kv").reshape(seqs, -1)
-    swap = [(k, k + 1 - 2 * (k % 2)) for k in range(n_kv)]
+    own_weights = pack(gate, up, down)
     other_weights = lax.ppermute(own_weights, "kv", swap)
     attn_part = jnp.dot(merged_all, w_out, preferred_element_type=jnp.float32)
     attn_part = attn_part.astype(jnp.bfloat16).T.reshape(n_tp, feats, seqs)
@@ -373,13 +415,12 @@
     gate_sum, up_sum, total = sums[:, :units], sums[:, units : 2 * units], sums[:, 2 * units]
     ffn_scale = lax.rsqrt(total / D + norm_eps)[:, None]
     hidden = (jax.nn.silu(ffn_scale * gate_sum) * (ffn_scale * up_sum)).astype(jnp.bfloat16)
-    hidden_all = exchanged(
-        jnp.broadcast_to(hidden[None], (n_kv, *hidden.shape)), "kv", [halves[0] + halves[1]]
-    ).reshape(seqs, units)
-    down_part = jnp.dot(hidden_all, w_down, preferred_element_type=jnp.float32)
-    down_part = down_part.astype(jnp.bfloat16).T.reshape(n_tp, feats, seqs)
+    hidden_half = exchanged(
+        jnp.broadcast_to(hidden[None], (n_kv // 2, *hidden.shape)), "kv", halves
+    ).reshape(seqs // 2, units)
+    down_part = lower(hidden_half, own_weights, other_weights, n_tp, feats)
     out_tokens, new_c, new_n, new_m = finish(
-        exchanged(down_part, "tp"), own_middle, *states
+        exchanged(down_part, ("kv", "tp"), pairs), own_middle, *states
     )
     new_n = new_n.reshape(own_seqs, 1, DK)
     return (out_tokens.T, new_c.reshape(state_c.shape), new_n, new_m.T)

time: 170 us -> 194 us (1.14)
  blocking collectives: 92.9 us -> 127 us
  waiting for transfers between devices: 13.6 us -> 0.9 us
  local copies, waits for them, and re-layouts: 1.69 us -> 7.63 us
  starting transfers between devices: 54.7 us -> 49.5 us
    all_to_all x6 -> x7, blocking collectives: 92.9 us -> 127 us  [exchanged(): lax.all_to_all(blocks, axis, split_axis=0, concat_axis=0, tiled=True, axi...]
    all_to_all x2 -> x1, waiting for transfers between devices: 13.6 us -> 0.89 us  [exchanged(): lax.all_to_all(blocks, axis, split_axis=0, concat_axis=0, tiled=True, axi...]
    all_to_all x2 -> x1, starting transfers between devices: 51.6 us -> 44.7 us  [exchanged(): lax.all_to_all(blocks, axis, split_axis=0, concat_axis=0, tiled=True, axi...]
    unnamed x34 -> x16, local copies, waits for them, and re-layouts: 1.32 us -> 3.42 us
  transfers between devices with their start and end apart: 3 -> 2, of which waited for: 2 -> 1; matrix products, arithmetic and copies ran while one was open for 0% -> 3% of each run, Pallas kernels for 0% -> 0%
where the time goes in v9:
time: 194 us; the launch traced here: 193 us
  blocking collectives  127 us (65%)
  starting transfers between devices  49.5 us (26%)
  local copies, waits for them, and re-layouts  7.63 us (4%)
  Pallas kernels  3.83 us (2%)
  between operations  2.08 us (1%)
  other arithmetic  1.94 us (1%)
    all_to_all x7, blocking collectives, exchanged(): lax.all_to_all(blocks, axis, split_axis=0, concat_axis=0, tiled=True, axi...  127 us
    all_to_all x1, starting transfers between devices, exchanged(): lax.all_to_all(blocks, axis, split_axis=0, concat_axis=0, tiled=True, axi...  44.7 us
    ppermute x1, starting transfers between devices, body(): other_weights = lax.ppermute(own_weights, 'kv', swap)  4.74 us
  transfers between devices with their start and end apart: 2, of which 1 were waited for; matrix products, arithmetic and copies ran while one was open for 3% of the time, Pallas kernels for 0%

profile of v9, /device:TPU:65, one launch (start us, length us, event | category | flops | bytes accessed | tf_op | source)
XLA Modules:
  0.0 193.4 jit_solution(14711587366430330136)
XLA Ops:
  0.6 0.0 copy-start
  0.6 0.0 copy-start.3
  0.7 0.0 copy-start.2
  0.7 0.0 copy-start.1
  0.7 0.0 copy-start.7
  0.7 0.8 copy-done.7
  1.5 0.6 spread.1
  2.1 44.7 %all-to-all-start = ((bf16[16,16,128]{2,1,0:T(8,128)(2,1)}), bf16[16,16,128]{2,1,0:T(8,128)(2,1)S(1)}, u32[]{:S(2)}, u32[]{:S(2)}) async-start(bf16[16,16,128]{2,1,0:T(8,128)(2,1)} %get-tuple-element.23), calls=%async_computation | async-start | bytes 131072 | tf_op jit(solution)/shard_map/all_to_all | solution.py:24
  46.8 0.7 broadcast_in_dim.14
  47.5 0.7 reshape.45
  49.5 0.7 broadcast_in_dim.6
  50.2 0.1 pad_convert_fusion
  50.3 0.7 maximum_convert_fusion.vectors_ref
  51.0 0.1 fusion.7
  51.0 0.7 pad.22
  51.7 0.7 pad.19
  52.4 0.7 concatenate.10.small_ref
  53.1 0.8 pad_maximum_fusion.both_ref
  53.9 0.9 all-to-all-done
  54.8 0.0 copy-start.5
  54.8 0.8 copy-done.5
  55.6 0.0 copy-start.6
  55.6 0.8 copy-done.6
  56.4 0.3 project.1
  56.7 19.0 %all_to_all.40.parts_ref = bf16[16,8,512]{2,1,0:T(8,128)(2,1)S(1)} all-to-all(bf16[16,8,512]{2,1,0:T(8,128)(2,1)S(1)} %bitcast.39), channel_id=1, replica_groups=mesh['grp'=2,'kv'=16,'tp'=16] {'kv'}, dimensions={0} | all-to-all | bytes 262144 | tf_op jit(solution)/shard_map/all_to_all | solution.py:24
  75.7 0.0 copy-start.4
  75.7 0.9 copy-done.4
  76.6 0.6 cell.1
  77.3 0.0 copy-done.3
  77.3 0.0 copy-done.2
  77.3 0.0 copy-done.1
  77.3 0.4 pack.1.own_ref
  77.7 4.7 %collective-permute-start = (bf16[2064,256]{1,0:T(8,128)(2,1)S(1)}, bf16[2064,256]{1,0:T(8,128)(2,1)S(1)}, u32[]{:S(2)}, u32[]{:S(2)}) collective-permute-start(bf16[2064,256]{1,0:T(8,128)(2,1)S(1)} %pack.1.own_ref), channel_id=1, source_target_pairs={{0,16},{16,0},{32,48},{48,32},{64,80},{80,64},{96,112},{112,96},{1... | collective-permute-start | bytes 3170312 | tf_op jit(solution)/shard_map/ppermute | solution.py:405
  82.5 25.7 %all_to_all.41 = bf16[16,8,128]{2,1,0:T(8,128)(2,1)S(1)} all-to-all(bf16[16,8,128]{2,1,0:T(8,128)(2,1)S(1)} %get-tuple-element.27), channel_id=1, replica_groups=mesh['grp'=2,'kv'=16,'tp'=16] {'kv'}, dimensions={0} | all-to-all | bytes 65536 | tf_op jit(solution)/shard_map/all_to_all | solution.py:24
  108.2 0.0 copy-done
  108.2 0.1 fusion
  108.3 0.1 copy.30
  108.5 16.0 %all_to_all.42.parts_ref = bf16[16,16,128]{2,1,0:T(8,128)(2,1)S(1)} all-to-all(bf16[16,16,128]{2,1,0:T(8,128)(2,1)S(1)} %bitcast.41), channel_id=1, replica_groups=mesh['grp'=2,'kv'=16,'tp'=16] {'tp'}, dimensions={0} | all-to-all | bytes 131072 | tf_op jit(solution)/shard_map/all_to_all | solution.py:24
  124.5 0.1 residual.1
  124.6 11.5 %all_to_all.43.x_ref = bf16[32,8,128]{2,1,0:T(8,128)(2,1)S(1)} all-to-all(bf16[32,8,128]{2,1,0:T(8,128)(2,1)S(1)} %get-tuple-element.29), channel_id=1, replica_groups={{0,1,2,3,4,5,6,7,8,9,10,11,12,13,14,15,16,17,18,19,20,21,22,23,24,25,26..., dimensions={0} | all-to-all | bytes 131072 | tf_op jit(solution)/shard_map/all_to_all | solution.py:24
  136.1 0.0 collective-permute-done.other_ref
  136.1 0.6 widen.1
  136.7 22.7 %all_to_all.44 = bf16[8,8,1408]{2,1,0:T(8,128)(2,1)S(1)} all-to-all(bf16[8,8,1408]{2,1,0:T(8,128)(2,1)S(1)} %bitcast.33), channel_id=1, replica_groups={{0,32,64,96,128,160,192,224},{16,48,80,112,144,176,208,240},{1,33,65,97..., dimensions={0} | all-to-all | bytes 360448 | tf_op jit(solution)/shard_map/all_to_all | solution.py:24
  159.4 0.2 fusion.6
  159.6 0.1 fusion.3
  159.7 18.1 %all_to_all.45 = bf16[8,8,688]{2,1,0:T(8,128)(2,1)S(1)} all-to-all(bf16[8,8,688]{2,1,0:T(8,128)(2,1)S(1)} %broadcast_in_dim.15), channel_id=1, replica_groups={{0,32,64,96,128,160,192,224},{16,48,80,112,144,176,208,240},{1,33,65,97..., dimensions={0} | all-to-all | bytes 176128 | tf_op jit(solution)/shard_map/all_to_all | solution.py:24
  177.9 0.4 lower.1
  178.3 14.4 %all_to_all.46.parts_ref = bf16[32,8,128]{2,1,0:T(8,128)(2,1)S(1)} all-to-all(bf16[32,8,128]{2,1,0:T(8,128)(2,1)S(1)} %lower.1), channel_id=1, replica_groups={{0,1,2,3,4,5,6,7,8,9,10,11,12,13,14,15,16,17,18,19,20,21,22,23,24,25,26..., dimensions={0} | all-to-all | bytes 131072 | tf_op jit(solution)/shard_map/all_to_all | solution.py:24
  192.7 0.7 finish.1
  (2 shorter events, 0.0 us)
Async XLA Ops:
  0.6 107.6 %copy-start = (bf16[128,256]{1,0:T(8,128)(2,1)S(1)}, bf16[128,256]{1,0:T(8,128)(2,1)}, u32[]{:S(2)}) copy-start(bf16[128,256]{1,0:T(8,128)(2,1)} %param.33) | copy-start | bytes 196612
  0.6 76.6 %copy-start.3 = (bf16[688,256]{1,0:T(8,128)(2,1)S(1)}, bf16[688,256]{1,0:T(8,128)(2,1)}, u32[]{:S(2)}) copy-start(bf16[688,256]{1,0:T(8,128)(2,1)} %refs_2_) | copy-start | bytes 1056772
  0.7 76.6 %copy-start.2 = (bf16[256,688]{0,1:T(8,128)(2,1)S(1)}, bf16[256,688]{0,1:T(8,128)(2,1)}, u32[]{:S(2)}) copy-start(bf16[256,688]{0,1:T(8,128)(2,1)} %param.36) | copy-start | bytes 1056772
  0.7 76.6 %copy-start.1 = (bf16[256,688]{0,1:T(8,128)(2,1)S(1)}, bf16[256,688]{0,1:T(8,128)(2,1)}, u32[]{:S(2)}) copy-start(bf16[256,688]{0,1:T(8,128)(2,1)} %param.35) | copy-start | bytes 1056772
  0.7 0.8 copy-start.7
  2.1 52.7 %all-to-all-start = ((bf16[16,16,128]{2,1,0:T(8,128)(2,1)}), bf16[16,16,128]{2,1,0:T(8,128)(2,1)S(1)}, u32[]{:S(2)}, u32[]{:S(2)}) async-start(bf16[16,16,128]{2,1,0:T(8,128)(2,1)} %get-tuple-element.23), calls=%async_computation | async-start | bytes 131072 | tf_op jit(solution)/shard_map/all_to_all | solution.py:24
  54.8 0.8 copy-start.5
  55.6 0.8 copy-start.6
  75.7 1.0 copy-start.4
  77.7 58.4 %collective-permute-start = (bf16[2064,256]{1,0:T(8,128)(2,1)S(1)}, bf16[2064,256]{1,0:T(8,128)(2,1)S(1)}, u32[]{:S(2)}, u32[]{:S(2)}) collective-permute-start(bf16[2064,256]{1,0:T(8,128)(2,1)S(1)} %pack.1.own_ref), channel_id=1, source_target_pairs={{0,16},{16,0},{32,48},{48,32},{64,80},{80,64},{96,112},{112,96},{1... | collective-permute-start | bytes 3170312 | tf_op jit(solution)/shard_map/ppermute | solution.py:405

commit v10 on v9

--- a/solution.py
+++ b/solution.py
@@ -1,10 +1,11 @@
+import functools
+
 import jax
 import jax.numpy as jnp
 from jax import lax
 from jax.experimental import pallas as pl
 from jax.experimental.pallas import tpu as pltpu
 from jax.sharding import PartitionSpec as P
-
 
 D = 4096
 DK = 64
@@ -289,7 +290,7 @@
 
     def product(weights_ref):
         down = jnp.dot(
-            hidden, weights_ref[2 * units :, :], preferred_element_type=jnp.float32
+            hidden, weights_ref[...], preferred_element_type=jnp.float32
         ).T.reshape(blocks, 2, feats, hidden.shape[0])
         return jnp.concatenate([down[:, 0], down[:, 1]], axis=2).astype(out_ref.dtype)
 
@@ -313,7 +314,7 @@
 def widen_kernel(x_ref, vectors_ref, gain_ref, own_ref, other_ref, out_ref):
     blocks = x_ref.shape[0] // 2
     half = x_ref.shape[2] // 2
-    units = own_ref.shape[0] // 3 * 2
+    units = own_ref.shape[0]
     cols = out_ref.shape[1]
     last = cols - LANES
     place = lax.rem(lax.axis_index("kv"), 2)
@@ -341,7 +342,7 @@
 
 
 def widen(x, vectors, other_gain, own, other):
-    cols = (own.shape[0] // 3 * 2 // LANES + 1) * LANES
+    cols = (own.shape[0] // LANES + 1) * LANES
     return pl.pallas_call(
         widen_kernel,
         out_shape=jax.ShapeDtypeStruct((x.shape[2] // 2, cols), jnp.bfloat16),
@@ -399,15 +400,17 @@
     arrived = exchanged(parts.reshape(n_kv, own_seqs, -1), "kv")
     states, other_gain, merged = cell(arrived, state_c, small, rows)
     merged, gate, up, down = lax.optimization_barrier((merged, w_gate.T, w_up.T, w_down))
+    own_weights = pack(gate, up)
+    merged_all = exchanged(merged, "kv").reshape(seqs, -1)
     swap = [(k, k + 1 - 2 * (k % 2)) for k in range(n_kv)]
-    merged_all = exchanged(merged, "kv").reshape(seqs, -1)
-    own_weights = pack(gate, up, down)
     other_weights = lax.ppermute(own_weights, "kv", swap)
+    other_down = lax.ppermute(down, "kv", swap)
     attn_part = jnp.dot(merged_all, w_out, preferred_element_type=jnp.float32)
     attn_part = attn_part.astype(jnp.bfloat16).T.reshape(n_tp, feats, seqs)
     own_middle, middle_copies = residual(exchanged(attn_part, "tp"), own_tokens)
     pairs = [[k * n_tp + t for t in range(2 * n_tp)] for k in range(0, n_kv, 2)]
     middle_rows = exchanged(middle_copies, ("kv", "tp"), pairs)
+    middle_rows, other_down = lax.optimization_barrier((middle_rows, other_down))
     partial = widen(middle_rows, vectors, other_gain, own_weights, other_weights)
     halves = [list(range(place, n_kv, 2)) for place in range(2)]
     arrived = exchanged(partial.reshape(n_kv // 2, own_seqs, -1), "kv", halves)
@@ -418,7 +421,7 @@
     hidden_half = exchanged(
         jnp.broadcast_to(hidden[None], (n_kv // 2, *hidden.shape)), "kv", halves
     ).reshape(seqs // 2, units)
-    down_part = lower(hidden_half, own_weights, other_weights, n_tp, feats)
+    down_part = lower(hidden_half, w_down, other_down, n_tp, feats)
     out_tokens, new_c, new_n, new_m = finish(
         exchanged(down_part, ("kv", "tp"), pairs), own_middle, *states
     )

time: 194 us -> 175 us (0.902)
  blocking collectives: 127 us -> 70.3 us
  waiting for transfers between devices: 0.9 us -> 27.2 us
  starting transfers between devices: 49.5 us -> 66.6 us
  local copies, waits for them, and re-layouts: 7.63 us -> 2.18 us
    all_to_all x7 -> x4, blocking collectives: 127 us -> 70.3 us  [exchanged(): lax.all_to_all(blocks, axis, split_axis=0, concat_axis=0, tiled=True, axi...]
    all_to_all x1 -> x4, waiting for transfers between devices: 0.89 us -> 27.2 us  [exchanged(): lax.all_to_all(blocks, axis, split_axis=0, concat_axis=0, tiled=True, axi...]
    all_to_all x1 -> x4, starting transfers between devices: 44.7 us -> 61.1 us  [exchanged(): lax.all_to_all(blocks, axis, split_axis=0, concat_axis=0, tiled=True, axi...]
    ppermute x0 -> x1, starting transfers between devices: none -> 2.21 us  [body(): other_down = lax.ppermute(down, 'kv', swap)]
    unnamed x16 -> x34, local copies, waits for them, and re-layouts: 3.42 us -> 1.31 us
  transfers between devices with their start and end apart: 2 -> 6, of which waited for: 1 -> 4; matrix products, arithmetic and copies ran while one was open for 3% -> 1% of each run, Pallas kernels for 0% -> 1%
where the time goes in v10:
time: 175 us; the launch traced here: 174 us
  blocking collectives  70.3 us (40%)
  starting transfers between devices  66.6 us (38%)
  waiting for transfers between devices  27.2 us (16%)
  Pallas kernels  4.93 us (3%)
  between operations  2.23 us (1%)
  local copies, waits for them, and re-layouts  2.18 us (1%)
    all_to_all x4, blocking collectives, exchanged(): lax.all_to_all(blocks, axis, split_axis=0, concat_axis=0, tiled=True, axi...  70.3 us
    all_to_all x4, starting transfers between devices, exchanged(): lax.all_to_all(blocks, axis, split_axis=0, concat_axis=0, tiled=True, axi...  61.1 us
    all_to_all x4, waiting for transfers between devices, exchanged(): lax.all_to_all(blocks, axis, split_axis=0, concat_axis=0, tiled=True, axi...  27.2 us
  transfers between devices with their start and end apart: 6, of which 4 were waited for; matrix products, arithmetic and copies ran while one was open for 1% of the time, Pallas kernels for 1%

profile of v10, /device:TPU:65, one launch (start us, length us, event | category | flops | bytes accessed | tf_op | source)
XLA Modules:
  0.0 174.1 jit_solution(3922415900039819288)
XLA Ops:
  0.6 0.0 copy-start
  0.6 0.0 copy-start.7
  0.7 0.7 copy-done.7
  1.4 0.6 spread.1
  2.0 44.9 %all-to-all-start = ((bf16[16,16,128]{2,1,0:T(8,128)(2,1)}), bf16[16,16,128]{2,1,0:T(8,128)(2,1)S(1)}, u32[]{:S(2)}, u32[]{:S(2)}) async-start(bf16[16,16,128]{2,1,0:T(8,128)(2,1)} %get-tuple-element.25), calls=%async_computation | async-start | bytes 131072 | tf_op jit(solution)/shard_map/all_to_all | solution.py:25
  46.9 0.0 copy-done.13
  46.9 0.0 copy-start.16
  46.9 0.0 copy-start.15
  46.9 0.0 copy-start.11
  46.9 0.0 copy-start.12
  46.9 0.1 reshape.45
  47.0 0.0 copy-start.10
  47.7 0.0 copy-start.14
  48.4 0.0 copy-done.15
  48.4 0.0 copy-start.8
  48.4 0.0 copy-start.9
  48.4 0.1 pad_convert_fusion
  48.5 0.0 copy-done.11
  48.5 0.0 copy-done.12
  48.5 0.1 fusion.7
  48.6 0.0 copy-done.16
  48.6 0.0 copy-done.10
  48.6 0.0 copy-done.14
  48.6 0.5 copy-done.8
  49.1 0.0 copy-done.9
  49.2 0.0 copy-start.5
  49.2 0.0 copy-start.6
  49.2 5.6 %all-to-all-done = bf16[16,16,128]{2,1,0:T(8,128)(2,1)S(1)} async-done(((bf16[16,16,128]{2,1,0:T(8,128)(2,1)}), bf16[16,16,128]{2,1,0:T(8,128)(2,1)S(1)}, u32[]{:S(2)}, u32[]{:S(2)}) %all-to-all-start) | async-done | bytes 65568 | tf_op jit(solution)/shard_map/all_to_all | solution.py:25
  54.8 0.0 copy-done.5
  54.8 0.0 copy-done.6
  54.8 0.0 copy-start.4
  54.8 0.3 project.1
  55.1 0.0 copy-start.2
  55.1 0.0 copy-start.3
  55.1 19.1 %all_to_all.40.parts_ref = bf16[16,8,512]{2,1,0:T(8,128)(2,1)S(1)} all-to-all(bf16[16,8,512]{2,1,0:T(8,128)(2,1)S(1)} %bitcast.39), channel_id=1, replica_groups=mesh['grp'=2,'kv'=16,'tp'=16] {'kv'}, dimensions={0} | all-to-all | bytes 262144 | tf_op jit(solution)/shard_map/all_to_all | solution.py:25
  74.2 0.0 copy-done.4
  74.2 1.2 cell.1
  75.4 6.7 %all-to-all-start.2 = ((bf16[16,8,128]{2,1,0:T(8,128)(2,1)}), bf16[16,8,128]{2,1,0:T(8,128)(2,1)S(1)}, u32[]{:S(2)}, u32[]{:S(2)}) async-start(bf16[16,8,128]{2,1,0:T(8,128)(2,1)} %get-tuple-element.29), calls=%async_computation.2 | async-start | bytes 65536 | tf_op jit(solution)/shard_map/all_to_all | solution.py:25
  82.2 0.0 copy-done.2
  82.2 0.0 copy-done.3
  82.2 0.3 pack.1.own_ref
  82.5 0.0 copy-start.1
  82.5 3.2 %collective-permute-start.1 = (bf16[1376,256]{1,0:T(8,128)(2,1)S(1)}, bf16[1376,256]{1,0:T(8,128)(2,1)S(1)}, u32[]{:S(2)}, u32[]{:S(2)}) collective-permute-start(bf16[1376,256]{1,0:T(8,128)(2,1)S(1)} %pack.1.own_ref), channel_id=1, source_target_pairs={{0,16},{16,0},{32,48},{48,32},{64,80},{80,64},{96,112},{112,96},{1... | collective-permute-start | bytes 2113544 | tf_op jit(solution)/shard_map/ppermute | solution.py:406
  85.7 7.9 %all-to-all-done.2 = bf16[16,8,128]{2,1,0:T(8,128)(2,1)S(1)} async-done(((bf16[16,8,128]{2,1,0:T(8,128)(2,1)}), bf16[16,8,128]{2,1,0:T(8,128)(2,1)S(1)}, u32[]{:S(2)}, u32[]{:S(2)}) %all-to-all-start.2) | async-done | bytes 32800 | tf_op jit(solution)/shard_map/all_to_all | solution.py:25
  93.6 0.0 copy-done
  93.6 0.1 fusion
  93.8 0.7 copy.30
  94.5 5.4 %all-to-all-start.3 = ((bf16[16,16,128]{2,1,0:T(8,128)(2,1)}), bf16[16,16,128]{2,1,0:T(8,128)(2,1)S(1)}, u32[]{:S(2)}, u32[]{:S(2)}) async-start(bf16[16,16,128]{2,1,0:T(8,128)(2,1)} %bitcast.16), calls=%async_computation.3 | async-start | bytes 131072 | tf_op jit(solution)/shard_map/all_to_all | solution.py:25
  99.9 0.0 copy-done.1
  99.9 2.2 %collective-permute-start = (bf16[688,256]{1,0:T(8,128)(2,1)S(1)}, bf16[688,256]{1,0:T(8,128)(2,1)S(1)}, u32[]{:S(2)}, u32[]{:S(2)}) collective-permute-start(bf16[688,256]{1,0:T(8,128)(2,1)S(1)} %copy-done.1), channel_id=1, source_target_pairs={{0,16},{16,0},{32,48},{48,32},{64,80},{80,64},{96,112},{112,96},{1... | collective-permute-start | bytes 1056776 | tf_op jit(solution)/shard_map/ppermute | solution.py:407
  102.1 5.7 %all-to-all-done.3.parts_ref = bf16[16,16,128]{2,1,0:T(8,128)(2,1)S(1)} async-done(((bf16[16,16,128]{2,1,0:T(8,128)(2,1)}), bf16[16,16,128]{2,1,0:T(8,128)(2,1)S(1)}, u32[]{:S(2)}, u32[]{:S(2)}) %all-to-all-start.3) | async-done | bytes 65568 | tf_op jit(solution)/shard_map/all_to_all | solution.py:25
  107.8 0.7 residual.1
  108.5 4.2 %all-to-all-start.4 = ((bf16[32,8,128]{2,1,0:T(8,128)(2,1)}), bf16[32,8,128]{2,1,0:T(8,128)(2,1)S(1)}, u32[]{:S(2)}, u32[]{:S(2)}) async-start(bf16[32,8,128]{2,1,0:T(8,128)(2,1)} %get-tuple-element.31), calls=%async_computation.4 | async-start | bytes 131072 | tf_op jit(solution)/shard_map/all_to_all | solution.py:25
  112.7 0.0 collective-permute-done.other_ref
  112.7 8.0 %all-to-all-done.4.x_ref = bf16[32,8,128]{2,1,0:T(8,128)(2,1)S(1)} async-done(((bf16[32,8,128]{2,1,0:T(8,128)(2,1)}), bf16[32,8,128]{2,1,0:T(8,128)(2,1)S(1)}, u32[]{:S(2)}, u32[]{:S(2)}) %all-to-all-start.4) | async-done | bytes 65568 | tf_op jit(solution)/shard_map/all_to_all | solution.py:25
  120.7 0.0 collective-permute-done.1.other_ref
  120.7 0.6 widen.1
  121.4 17.3 %all_to_all.41 = bf16[8,8,1408]{2,1,0:T(8,128)(2,1)S(1)} all-to-all(bf16[8,8,1408]{2,1,0:T(8,128)(2,1)S(1)} %bitcast.33), channel_id=1, replica_groups={{0,32,64,96,128,160,192,224},{16,48,80,112,144,176,208,240},{1,33,65,97..., dimensions={0} | all-to-all | bytes 360448 | tf_op jit(solution)/shard_map/all_to_all | solution.py:25
  138.7 0.2 fusion.6
  138.9 0.1 fusion.3
  139.0 17.8 %all_to_all.42 = bf16[8,8,688]{2,1,0:T(8,128)(2,1)S(1)} all-to-all(bf16[8,8,688]{2,1,0:T(8,128)(2,1)S(1)} %broadcast_in_dim.15), channel_id=1, replica_groups={{0,32,64,96,128,160,192,224},{16,48,80,112,144,176,208,240},{1,33,65,97..., dimensions={0} | all-to-all | bytes 176128 | tf_op jit(solution)/shard_map/all_to_all | solution.py:25
  156.8 0.4 lower.1
  157.2 16.2 %all_to_all.43.parts_ref = bf16[32,8,128]{2,1,0:T(8,128)(2,1)S(1)} all-to-all(bf16[32,8,128]{2,1,0:T(8,128)(2,1)S(1)} %lower.1), channel_id=1, replica_groups={{0,1,2,3,4,5,6,7,8,9,10,11,12,13,14,15,16,17,18,19,20,21,22,23,24,25,26..., dimensions={0} | all-to-all | bytes 131072 | tf_op jit(solution)/shard_map/all_to_all | solution.py:25
  173.3 0.7 finish.1
  (10 shorter events, 0.1 us)
Async XLA Ops:
  0.6 93.0 %copy-start = (bf16[128,256]{1,0:T(8,128)(2,1)S(1)}, bf16[128,256]{1,0:T(8,128)(2,1)}, u32[]{:S(2)}) copy-start(bf16[128,256]{1,0:T(8,128)(2,1)} %param.33) | copy-start | bytes 196612
  0.6 0.7 copy-start.7
  2.0 44.9 %copy-start.13 = (bf16[256]{0:T(256)(128)(2,1)S(1)}, bf16[256]{0:T(256)(128)(2,1)}, u32[]{:S(2)}) copy-start(bf16[256]{0:T(256)(128)(2,1)} %param.34) | copy-start | bytes 1540
  2.0 52.8 %all-to-all-start = ((bf16[16,16,128]{2,1,0:T(8,128)(2,1)}), bf16[16,16,128]{2,1,0:T(8,128)(2,1)S(1)}, u32[]{:S(2)}, u32[]{:S(2)}) async-start(bf16[16,16,128]{2,1,0:T(8,128)(2,1)} %get-tuple-element.25), calls=%async_computation | async-start | bytes 131072 | tf_op jit(solution)/shard_map/all_to_all | solution.py:25
  46.9 1.7 copy-start.16
  46.9 1.5 copy-start.15
  46.9 1.6 copy-start.11
  46.9 1.6 copy-start.12
  47.0 1.6 copy-start.10
  47.7 0.9 copy-start.14
  48.4 0.8 copy-start.8
  48.4 0.8 copy-start.9
  49.2 5.6 %copy-start.5 = (bf16[256,128]{1,0:T(8,128)(2,1)S(1)}, bf16[256,128]{1,0:T(8,128)(2,1)}, u32[]{:S(2)}) copy-start(bf16[256,128]{1,0:T(8,128)(2,1)} %value_ref.1) | copy-start | bytes 196612
  49.2 5.6 %copy-start.6 = (bf16[256,128]{1,0:T(8,128)(2,1)S(1)}, bf16[256,128]{1,0:T(8,128)(2,1)}, u32[]{:S(2)}) copy-start(bf16[256,128]{1,0:T(8,128)(2,1)} %ogate_ref.1) | copy-start | bytes 196612
  54.8 19.4 %copy-start.4 = (f32[8,1,64,128]{3,2,1,0:T(8,128)S(1)}, f32[8,1,64,128]{3,2,1,0:T(8,128)}, u32[]{:S(2)}) copy-start(f32[8,1,64,128]{3,2,1,0:T(8,128)} %param.29) | copy-start | bytes 786436
  55.1 27.1 %copy-start.2 = (bf16[256,688]{0,1:T(8,128)(2,1)S(1)}, bf16[256,688]{0,1:T(8,128)(2,1)}, u32[]{:S(2)}) copy-start(bf16[256,688]{0,1:T(8,128)(2,1)} %param.35) | copy-start | bytes 1056772
  55.1 27.1 %copy-start.3 = (bf16[256,688]{0,1:T(8,128)(2,1)S(1)}, bf16[256,688]{0,1:T(8,128)(2,1)}, u32[]{:S(2)}) copy-start(bf16[256,688]{0,1:T(8,128)(2,1)} %param.36) | copy-start | bytes 1056772
  75.4 18.2 %all-to-all-start.2 = ((bf16[16,8,128]{2,1,0:T(8,128)(2,1)}), bf16[16,8,128]{2,1,0:T(8,128)(2,1)S(1)}, u32[]{:S(2)}, u32[]{:S(2)}) async-start(bf16[16,8,128]{2,1,0:T(8,128)(2,1)} %get-tuple-element.29), calls=%async_computation.2 | async-start | bytes 65536 | tf_op jit(solution)/shard_map/all_to_all | solution.py:25
  82.5 17.4 %copy-start.1 = (bf16[688,256]{1,0:T(8,128)(2,1)S(1)}, bf16[688,256]{1,0:T(8,128)(2,1)}, u32[]{:S(2)}) copy-start(bf16[688,256]{1,0:T(8,128)(2,1)} %own_ref.1) | copy-start | bytes 1056772
  82.5 38.2 %collective-permute-start.1 = (bf16[1376,256]{1,0:T(8,128)(2,1)S(1)}, bf16[1376,256]{1,0:T(8,128)(2,1)S(1)}, u32[]{:S(2)}, u32[]{:S(2)}) collective-permute-start(bf16[1376,256]{1,0:T(8,128)(2,1)S(1)} %pack.1.own_ref), channel_id=1, source_target_pairs={{0,16},{16,0},{32,48},{48,32},{64,80},{80,64},{96,112},{112,96},{1... | collective-permute-start | bytes 2113544 | tf_op jit(solution)/shard_map/ppermute | solution.py:406
  94.5 13.3 %all-to-all-start.3 = ((bf16[16,16,128]{2,1,0:T(8,128)(2,1)}), bf16[16,16,128]{2,1,0:T(8,128)(2,1)S(1)}, u32[]{:S(2)}, u32[]{:S(2)}) async-start(bf16[16,16,128]{2,1,0:T(8,128)(2,1)} %bitcast.16), calls=%async_computation.3 | async-start | bytes 131072 | tf_op jit(solution)/shard_map/all_to_all | solution.py:25
  99.9 12.8 %collective-permute-start = (bf16[688,256]{1,0:T(8,128)(2,1)S(1)}, bf16[688,256]{1,0:T(8,128)(2,1)S(1)}, u32[]{:S(2)}, u32[]{:S(2)}) collective-permute-start(bf16[688,256]{1,0:T(8,128)(2,1)S(1)} %copy-done.1), channel_id=1, source_target_pairs={{0,16},{16,0},{32,48},{48,32},{64,80},{80,64},{96,112},{112,96},{1... | collective-permute-start | bytes 1056776 | tf_op jit(solution)/shard_map/ppermute | solution.py:407
  108.5 12.2 %all-to-all-start.4 = ((bf16[32,8,128]{2,1,0:T(8,128)(2,1)}), bf16[32,8,128]{2,1,0:T(8,128)(2,1)S(1)}, u32[]{:S(2)}, u32[]{:S(2)}) async-start(bf16[32,8,128]{2,1,0:T(8,128)(2,1)} %get-tuple-element.31), calls=%async_computation.4 | async-start | bytes 131072 | tf_op jit(solution)/shard_map/all_to_all | solution.py:25
